TPU v7x, 256 devices: a whole 4x4x8 slice. The times are simulated.
256 devices in a mesh: sp: 32 (over z, y), fs: 4 (over x), tp: 2 (over core).
Axes of the slice: x: 4, y: 4, z: 8, core: 2. Of those that a mesh axis runs over, the one named last changes fastest.
Arguments:
- tokens: bfloat16 [4, 4096, 2048], P('fs', ('sp', 'tp')), may hold values from -6 to 6
- norm_gain: float32 [2048], replicated, may hold values from 0.1 to 1.9
- drive_weight: bfloat16 [2048, 1024], P('fs', 'tp'), may hold values from -0.125 to 0.125
- query_weight: bfloat16 [2048, 1024], P('fs', 'tp'), may hold values from -1 to 1
- key_weight: bfloat16 [2048, 1024], P('fs', 'tp'), may hold values from -1 to 1
- value_weight: bfloat16 [2048, 1024], P('fs', 'tp'), may hold values from -0.5 to 0.5
- key_offset: bfloat16 [8, 4, 4096], P('tp', 'fs', 'sp'), may hold values from -16 to 0
- log_step: float32 [64], P('tp'), may hold values from -4.7 to -1.2
- lambda_real: float32 [64, 64], P('tp'), as said below
- lambda_imag: float32 [64, 64], P('tp'), may hold values from 1 to 201
- input_map: float32 [2, 64, 64, 16], P(None, 'tp'), may hold values from -2 to 2
- output_map: float32 [2, 64, 16, 64], P(None, 'tp'), may hold values from -0.5 to 0.5
- skip_gain: float32 [1024], P('tp'), may hold values from -5 to 5
- forget: float32 [64, 4, 4096], P('tp', 'fs', 'sp'), may hold values from -0.52 to 0
- initial_state: float32 [2, 4, 64, 64], P(None, 'fs', 'tp'), may hold values from -24 to 24
- scan_out_weight: bfloat16 [1024, 2048], P('tp', 'fs'), may hold values from -0.125 to 0.125
- attend_out_weight: bfloat16 [1024, 2048], P('tp', 'fs'), may hold values from -0.125 to 0.125
Outputs:
- layer_out: bfloat16 [4, 4096, 2048], P('fs', ('sp', 'tp'))
Inputs may be any that keep to these rules, and one draw needn't show every extreme that they name: lambda_real[g, n] * exp(log_step[g]) lies between -1/30 and 0 for every group g and state n.
All inputs are finite; a program needn't handle non-finite values.
Results may differ from a plain program's by a relative error of at most 0.009.
Values may be sent and summed in bfloat16 or wider, within the bound.
No kernel may reach another device: no remote copies, remote signals or barrier semaphores. Data moves between devices by JAX's collectives and lax.ppermute only.
A program may use at most 128 MiB of HBM per device.

v0:
```python
import math

import jax
import jax.numpy as jnp
from jax import lax
from jax.experimental import pallas as pl
from jax.experimental.pallas import tpu as pltpu
from jax.sharding import Mesh
from jax.sharding import PartitionSpec as P


HEAD_DIM = 128
BLOCK = 128
ROWS = 512
EXTRA = 16
MORE = 8
SP = ("z", "y")
SP_TP = ("z", "y", "c")
LOG2E = 1.4426950408889634
SCORE = HEAD_DIM ** (-0.5) * LOG2E
epsilon = 1e-06
f32 = jnp.float32
bf16 = jnp.bfloat16
INTERPRET = False


def staged(body, outs, arrays, scratch=(), flops=0, limit=20, lazy=False, raw=(), free=()):
    n, m = len(arrays), len(outs)
    kept = [i for i in range(n) if i not in raw]

    def kernel(*refs):
        src, dst = refs[:n], refs[n : n + m]
        refs = refs[n + m :]
        bufs = dict(zip(kept, refs[: len(kept)]))
        results = refs[len(kept) : len(kept) + m]
        sems, rest = refs[len(kept) + m], refs[len(kept) + m + 1 :]
        copies = {i: pltpu.make_async_copy(src[i], bufs[i], sems.at[i]) for i in kept}
        for i in kept:
            copies[i].start()
        leaving = {}

        def ready(*which):
            for i in which:
                copies[i].wait()

        def send(i):
            leaving[i] = pltpu.make_async_copy(results[i], dst[i], sems.at[n + i])
            leaving[i].start()

        ins = [bufs.get(i, src[i]) for i in range(n)]
        if lazy:
            body(ready, send, *ins, *results, *rest)
        else:
            ready(*kept)
            body(*ins, *results, *rest)
        for i in range(m):
            if i not in leaving:
                send(i)
        for i in range(m):
            leaving[i].wait()

    hbm = pl.BlockSpec(memory_space=pltpu.HBM)
    got = pl.pallas_call(
        kernel,
        out_shape=tuple(pltpu.HBM(o.shape, o.dtype) for o in outs),
        in_specs=[hbm] * n,
        out_specs=(hbm,) * m,
        scratch_shapes=[pltpu.VMEM(arrays[i].shape, arrays[i].dtype) for i in kept]
        + [pltpu.VMEM(o.shape, o.dtype) for o in outs]
        + [pltpu.SemaphoreType.DMA((n + m,))]
        + list(scratch),
        cost_estimate=pl.CostEstimate(flops=flops, transcendentals=0, bytes_accessed=1 << 20),
        compiler_params=pltpu.CompilerParams(vmem_limit_bytes=limit << 20),
        interpret=INTERPRET,
    )(*(a if i in free else pltpu.with_memory_space_constraint(a, pltpu.HBM) for i, a in enumerate(arrays)))
    return got if m > 1 else got[0]


def shape(dims, dtype):
    return jax.ShapeDtypeStruct(dims, dtype)


def split2(v):
    hi = v.astype(bf16)
    return hi, (v - hi.astype(f32)).astype(bf16)


def mm(a, b):
    return jnp.dot(a, b, preferred_element_type=f32)


def mm_t(a, b):
    return lax.dot_general(a, b, (((1,), (1,)), ((), ())), preferred_element_type=f32)


def norm_body(tok_ref, gain_ref, forget_ref, off_ref, out_ref):
    v = tok_ref[0].astype(f32)
    scale = lax.rsqrt(jnp.mean(v * v, axis=1, keepdims=True) + epsilon)
    normed = (v * scale * gain_ref[...]).astype(bf16)
    hi, lo = split2(forget_ref[...])
    hi, lo = hi.astype(f32), lo.astype(f32)
    off = off_ref[...].astype(f32)
    blank = jnp.zeros((6, BLOCK), f32)
    for k in range(4):
        out_ref[k, :64, :] = normed
        for j in range(16):
            row = hi[8 * k + j : 8 * k + j + 1] if j < 8 else lo[8 * k + j - 8 : 8 * k + j - 7]
            last = off[k : k + 1] if j == 0 else jnp.zeros((1, BLOCK), f32)
            tile = jnp.concatenate([row, last, blank], axis=0)
            out_ref[k, 64:, j * BLOCK : (j + 1) * BLOCK] = tile.astype(bf16)


def normalize(tokens, gain, forget, offset):
    return staged(
        norm_body,
        [shape((4, 64 + MORE, 2048), bf16)],
        [tokens, gain.reshape(1, -1), forget, offset],
        flops=10**6,
    )


def pack_body(k_ref, v_ref, q_ref, d_ref, kv_out, qd_out, kv_buf, qd_buf, sems):
    at = pl.ds(pl.multiple_of(lax.axis_index("y") * BLOCK, BLOCK), BLOCK)
    arrive = []
    for n, (ref, buf, h) in enumerate(
        ((k_ref, kv_buf, 0), (v_ref, kv_buf, 1), (q_ref, qd_buf, 0), (d_ref, qd_buf, 1))
    ):
        arrive.append(
            pltpu.make_async_copy(ref.at[:, at], buf.at[:, pl.ds(h * BLOCK, BLOCK)], sems.at[n])
        )
    for copy in arrive:
        copy.start()
    leave = []
    for part, (buf, out) in enumerate(((kv_buf, kv_out), (qd_buf, qd_out))):
        arrive[2 * part].wait()
        arrive[2 * part + 1].wait()
        for k in range(4):
            copy = pltpu.make_async_copy(buf, out.at[k], sems.at[4 + 4 * part + k])
            copy.start()
            leave.append(copy)
    for copy in leave:
        copy.wait()


def pack(*weights):
    anywhere = pl.BlockSpec(memory_space=pltpu.HBM)
    packed = pltpu.HBM((4, ROWS, 2 * BLOCK), bf16)
    return pl.pallas_call(
        pack_body,
        out_shape=(packed, packed),
        in_specs=[anywhere] * 4,
        out_specs=(anywhere, anywhere),
        scratch_shapes=[pltpu.VMEM((ROWS, 2 * BLOCK), bf16)] * 2 + [pltpu.SemaphoreType.DMA((12,))],
        interpret=INTERPRET,
        name="pack",
    )(*(pltpu.with_memory_space_constraint(a, pltpu.HBM) for a in weights))


def rows_copies(mine, theirs, rows, sems):
    c = lax.axis_index("c")
    copies = []
    for b in range(4):
        for part, ref in enumerate((mine, theirs)):
            at = pl.multiple_of(b * BLOCK + ((c + part) % 2) * 64, 64)
            copies.append(
                pltpu.make_async_copy(ref.at[b, pl.ds(0, 64)], rows.at[pl.ds(at, 64)], sems.at[2 * b + part])
            )
    return copies


ROWS_SCRATCH = [pltpu.VMEM((ROWS, 2048), bf16), pltpu.SemaphoreType.DMA((12,)), pltpu.VMEM((4, MORE, 2048), bf16)]


def kv_body(ready, send, mine, theirs, w_ref, kv_ref, rows, sems, more):
    copies = rows_copies(mine, theirs, rows, sems)
    for b in range(4):
        copies.append(
            pltpu.make_async_copy(mine.at[b, pl.ds(64, MORE)], more.at[b], sems.at[8 + b])
        )
    for copy in copies:
        copy.start()
    for copy in copies:
        copy.wait()
    ready(2)
    offs = [more[b].astype(f32)[1:2, :BLOCK] for b in range(4)]
    row0 = jnp.concatenate(offs[:2], axis=1)
    row1 = jnp.concatenate(offs[2:], axis=1)
    tail = jnp.concatenate([row0, row1, jnp.zeros((EXTRA - 2, 256), f32)], axis=0)
    kv_ref[ROWS:, :] = tail.astype(bf16)
    kv_ref[:ROWS, :] = mm(rows[...], w_ref[...]).astype(bf16)


def project_kv(mine, theirs, weights):
    return staged(
        kv_body,
        [shape((ROWS + EXTRA, 256), bf16)],
        [mine, theirs, weights],
        ROWS_SCRATCH,
        flops=2 * ROWS * 2048 * 256,
        lazy=True,
        raw=(0, 1),
        free=(0, 1, 2),
    )


SPAN = 256
TILE = 32
WIDE = SPAN + BLOCK


def chunk(q_ref, kv_ref, acc_ref, fall_ref, scr, diagonal):
    s_ref, soft_ref, r_ref, w_ref, tri_ref = scr
    j = lax.broadcasted_iota(jnp.int32, (SPAN, WIDE), 0)
    k = lax.broadcasted_iota(jnp.int32, (SPAN, WIDE), 1)
    tri_ref[...] = jnp.where((j > k) | (k >= SPAN), 1.0, 0.0).astype(bf16)
    offs = kv_ref[ROWS : ROWS + EXTRA, :].astype(f32)
    off = jnp.concatenate([offs[0:1], offs[1:2]], axis=1) * LOG2E
    s_ref[...] = mm_t(q_ref[...], kv_ref[:ROWS, :BLOCK])

    def visible(i):
        t = lax.broadcasted_iota(jnp.int32, (TILE, ROWS), 0) + i * TILE
        s = lax.broadcasted_iota(jnp.int32, (TILE, ROWS), 1)
        return s < t

    def first(i, _):
        at = pl.ds(pl.multiple_of(i * TILE, TILE), TILE)
        z = s_ref[at, :] * SCORE + off
        soft = jnp.maximum(z, 0.0) + jnp.log2(1.0 + jnp.exp2(-jnp.abs(z)))
        s_ref[at, :] = z - soft
        if diagonal:
            soft = jnp.where(visible(i), soft, 0.0)
        soft_ref[at, :] = soft.astype(bf16)
        return 0

    lax.fori_loop(0, ROWS // TILE, first, 0, unroll=2)
    for blk in range(2):
        r_ref[:, blk * WIDE : (blk + 1) * WIDE] = mm(
            soft_ref[:, blk * SPAN : (blk + 1) * SPAN], tri_ref[...]
        )

    def second(i, _):
        at = pl.ds(pl.multiple_of(i * TILE, TILE), TILE)
        fall1 = fall_ref[at, :]
        fall0 = fall1 + r_ref[at, WIDE + SPAN :]
        fall_ref[at, :] = fall0 + r_ref[at, SPAN:WIDE]
        behind = jnp.concatenate(
            [
                r_ref[at, :BLOCK] + fall0,
                r_ref[at, BLOCK:SPAN] + fall0,
                r_ref[at, WIDE : WIDE + BLOCK] + fall1,
                r_ref[at, WIDE + BLOCK : WIDE + SPAN] + fall1,
            ],
            axis=1,
        )
        w = jnp.exp2(s_ref[at, :] - behind)
        if diagonal:
            w = jnp.where(visible(i), w, 0.0)
        w_ref[at, :] = w.astype(bf16)
        return 0

    lax.fori_loop(0, ROWS // TILE, second, 0, unroll=2)
    acc_ref[...] += mm(w_ref[...], kv_ref[:ROWS, BLOCK:])


ATTEND_SCRATCH = [
    pltpu.VMEM((ROWS, ROWS), f32),
    pltpu.VMEM((ROWS, ROWS), bf16),
    pltpu.VMEM((ROWS, 2 * WIDE), f32),
    pltpu.VMEM((ROWS, ROWS), bf16),
    pltpu.VMEM((SPAN, WIDE), bf16),
]
PAIR = (shape((ROWS, BLOCK), f32), shape((ROWS, BLOCK), f32))
ATTEND_FLOPS = 8 * ROWS * ROWS * BLOCK


def attend_near(q, kv, up, down):
    def body(ready, send, q_ref, kv_ref, up_ref, down_ref, acc_ref, fall_ref, far_ref, low_ref, *scr):
        z = lax.axis_index("z")
        acc_ref[...] = jnp.zeros((ROWS, BLOCK), f32)
        fall_ref[...] = jnp.zeros((ROWS, BLOCK), f32)
        far_ref[...] = jnp.zeros((ROWS, BLOCK), f32)
        ready(0, 1)
        chunk(q_ref, kv_ref, acc_ref, fall_ref, scr, True)
        ready(2, 3)

        @pl.when(z >= 1)
        def _():
            chunk(q_ref, up_ref, acc_ref, fall_ref, scr, False)

        @pl.when(z >= 7)
        def _():
            low_ref[...] = jnp.zeros((ROWS, BLOCK), f32)
            chunk(q_ref, down_ref, far_ref, low_ref, scr, False)

    return staged(
        body,
        PAIR + PAIR[:1],
        [q, kv, up, down],
        [pltpu.VMEM((ROWS, BLOCK), f32)] + ATTEND_SCRATCH,
        flops=3 * ATTEND_FLOPS,
        lazy=True,
        free=(2, 3),
    )


def attend_middle(q, acc, fall, far, ups, downs):
    def body(
        ready, send, q_ref, acc_in, fall_in, far_in, up2, down2, up3, down3,
        acc_ref, fall_ref, far_ref, low_ref, *scr,
    ):
        z = lax.axis_index("z")
        ready(0, 1, 2, 3)
        acc_ref[...] = acc_in[...]
        fall_ref[...] = fall_in[...]
        for k, (up_ref, down_ref) in ((2, (up2, down2)), (3, (up3, down3))):
            ready(2 * k, 2 * k + 1)

            @pl.when(z >= k)
            def _(up_ref=up_ref):
                chunk(q_ref, up_ref, acc_ref, fall_ref, scr, False)

            before = far_in if k == 2 else far_ref

            @pl.when(z + k >= 8)
            def _(down_ref=down_ref, before=before):
                low_ref[...] = jnp.zeros((ROWS, BLOCK), f32)
                part_ref = acc_in
                part_ref[...] = jnp.zeros((ROWS, BLOCK), f32)
                chunk(q_ref, down_ref, part_ref, low_ref, scr, False)
                far_ref[...] = part_ref[...] + jnp.exp2(-low_ref[...]) * before[...]

            if k == 2:

                @pl.when(z + k < 8)
                def _():
                    far_ref[...] = far_in[...]

    return staged(
        body,
        PAIR + PAIR[:1],
        [q, acc, fall, far, ups[2], downs[2], ups[3], downs[3]],
        [pltpu.VMEM((ROWS, BLOCK), f32)] + ATTEND_SCRATCH,
        flops=4 * ATTEND_FLOPS,
        lazy=True,
        free=(4, 5, 6, 7),
    )


def attend_last(q, kv, acc, fall, far, scan_out):
    def body(q_ref, kv_ref, acc_ref, fall_ref, far_ref, scan_ref, out_ref, *scr):
        @pl.when(lax.axis_index("z") >= 4)
        def _():
            chunk(q_ref, kv_ref, acc_ref, fall_ref, scr, False)

        out_ref[:, :BLOCK] = scan_ref[...]
        out_ref[:, BLOCK:] = (acc_ref[...] + jnp.exp2(-fall_ref[...]) * far_ref[...]).astype(bf16)

    return staged(
        body,
        [shape((ROWS, 2 * BLOCK), bf16)],
        [q, kv, acc, fall, far, scan_out],
        ATTEND_SCRATCH,
        flops=ATTEND_FLOPS,
        free=(1,),
    )


N = 512


def cmul(ar, ai, br, bi):
    return ar * br - ai * bi, ar * bi + ai * br


def tables_body(
    in_ref, out_ref, lam_r_ref, lam_i_ref, step_ref, start_ref, skip_in,
    pow_ref, inv_ref, b_ref, ct_ref, init_ref, skip_ref,
):
    y = lax.axis_index("y")
    own = pl.ds(pl.multiple_of(y * 8, 8), 8)
    copy = (
        lax.broadcasted_iota(jnp.int32, (64, N), 1) % 64 == lax.broadcasted_iota(jnp.int32, (64, N), 0)
    ).astype(f32)

    def tiled(a, height):
        rows, width = a.shape
        r = lax.broadcasted_iota(jnp.int32, (rows, N), 0) // height
        k = lax.broadcasted_iota(jnp.int32, (rows, N), 1) // width
        spread = jnp.dot(a, copy, precision=lax.Precision.HIGHEST, preferred_element_type=f32)
        return jnp.where(r == k, spread, 0.0)

    def line(a):
        return jnp.sum(tiled(a, 1), axis=0, keepdims=True)

    lam_r, lam_i, step = line(lam_r_ref[own]), line(lam_i_ref[own]), jnp.exp(line(step_ref[own]))
    init_ref[0:1, :] = line(start_ref[0, 0, own])
    init_ref[1:2, :] = line(start_ref[1, 0, own])
    skip_ref[...] = skip_in[:, pl.ds(pl.multiple_of(y * BLOCK, BLOCK), BLOCK)]
    gain = lam_r * step
    turn = lam_i * step
    size = jnp.exp(gain)
    bar_r = size * jnp.cos(turn)
    bar_i = size * jnp.sin(turn)
    over = lam_r * lam_r + lam_i * lam_i
    less = bar_r - 1.0
    factor_r = (less * lam_r + bar_i * lam_i) / over
    factor_i = (bar_i * lam_r - less * lam_i) / over
    count = lax.broadcasted_iota(jnp.int32, (BLOCK, N), 0) + 1
    pr = jnp.ones((BLOCK, N), f32)
    pi = jnp.zeros((BLOCK, N), f32)
    sr, si = bar_r, bar_i
    for bit in range(8):
        on = ((count >> bit) & 1) == 1
        nr, ni = cmul(pr, pi, sr, si)
        pr, pi = jnp.where(on, nr, pr), jnp.where(on, ni, pi)
        if bit < 7:
            sr, si = cmul(sr, si, sr, si)
    back = jnp.exp(-2.0 * count.astype(f32) * gain)
    pow_ref[:BLOCK, :] = pr
    pow_ref[BLOCK:, :] = pi
    br, bi = cmul(pr * back, -pi * back, factor_r, factor_i)
    inv_ref[:BLOCK, :] = br
    inv_ref[BLOCK:, :] = bi
    for p in range(2):
        b_ref[:, p * N : (p + 1) * N] = tiled(in_ref[p, own].reshape(BLOCK, 64), 16).astype(bf16)
        sign = 1.0 if p == 0 else -1.0
        ct_ref[:, p * N : (p + 1) * N] = (sign * tiled(out_ref[p, own].reshape(BLOCK, 64), 16)).astype(bf16)


def scan_tables(*arrays):
    return staged(
        tables_body,
        (
            shape((2 * BLOCK, N), f32),
            shape((2 * BLOCK, N), f32),
            shape((BLOCK, 2 * N), bf16),
            shape((BLOCK, 2 * N), bf16),
            shape((2, N), f32),
            shape((1, BLOCK), f32),
        ),
        arrays,
        flops=10**9,
    )


def scan_body(
    ready, send, mine, theirs, w_ref, pow_ref, inv_ref, b_ref, ct_ref, skip_ref,
    q_ref, y_ref, ef_ref, hop_ref, sum_ref, all_rows, sems, more, u_ref, f_ref,
):
    copies = rows_copies(mine, theirs, all_rows, sems)
    for b in range(4):
        copies.append(
            pltpu.make_async_copy(mine.at[b, pl.ds(64, MORE)], more.at[b], sems.at[8 + b])
        )
    for copy in copies:
        copy.start()
    for copy in copies:
        copy.wait()
    ready(2)
    both = mm(all_rows[...], w_ref[...])
    q_ref[...] = both[:, :BLOCK].astype(bf16)
    u_ref[...] = both[:, BLOCK:].astype(bf16)
    send(0)
    for b in range(4):
        part = more[b].astype(f32)
        part = part[0:1, : 8 * BLOCK] + part[0:1, 8 * BLOCK :]
        f_ref[:, b * BLOCK : (b + 1) * BLOCK] = jnp.concatenate(
            [part[:, g * BLOCK : (g + 1) * BLOCK] for g in range(8)], axis=0
        )
    ready(3, 4, 5, 6, 7)
    row = lax.broadcasted_iota(jnp.int32, (BLOCK, BLOCK), 0)
    col = lax.broadcasted_iota(jnp.int32, (BLOCK, BLOCK), 1)
    low = (col <= row).astype(bf16)
    low32 = (col <= row).astype(f32)
    even = lax.broadcasted_iota(jnp.int32, (1, BLOCK), 1) < 64

    def block(b, state):
        carry_r, carry_i, hop_r, hop_i = state
        rows = pl.ds(pl.multiple_of(b * BLOCK, BLOCK), BLOCK)
        f = f_ref[:, rows]
        f_all = jnp.concatenate([jnp.broadcast_to(f[g : g + 1], (16, BLOCK)) for g in range(8)], axis=0)
        cum_f = lax.dot_general(
            low32, f_all, (((1,), (1,)), ((), ())), precision=lax.Precision.HIGHEST, preferred_element_type=f32
        )
        ef = jnp.exp(cum_f)
        ef_ref[rows, :] = ef
        u = u_ref[rows, :].astype(f32)
        drive = mm((u * jnp.exp(-cum_f)).astype(bf16), b_ref[...])
        dr, di = cmul(drive[:, :N], drive[:, N:], inv_ref[:BLOCK, :], inv_ref[BLOCK:, :])
        tr = mm(low, dr.astype(bf16)) + carry_r
        ti = mm(low, di.astype(bf16)) + carry_i
        st_r, st_i = cmul(pow_ref[:BLOCK, :], pow_ref[BLOCK:, :], tr, ti)
        out = mm_t(st_r.astype(bf16), ct_ref[:, :N]) + mm_t(st_i.astype(bf16), ct_ref[:, N:])
        y_ref[rows, :] = ef * out + skip_ref[...] * u
        total = jnp.exp(jnp.broadcast_to(jnp.sum(f, axis=1, keepdims=True), (8, BLOCK)))
        keep = jnp.concatenate(
            [jnp.where(even, total[2 * g : 2 * g + 1], total[2 * g + 1 : 2 * g + 2]) for g in range(4)], axis=1
        )
        hop_ref[pl.ds(pl.multiple_of(b * 8, 8), 8), :] = jnp.concatenate(
            [hop_r, hop_i, jnp.zeros((6, N), f32)], axis=0
        )
        nr, ni = cmul(hop_r, hop_i, pow_ref[BLOCK - 1 : BLOCK, :], pow_ref[2 * BLOCK - 1 :, :])
        return keep * st_r[BLOCK - 1 :, :], keep * st_i[BLOCK - 1 :, :], keep * nr, keep * ni

    zero = jnp.zeros((1, N), f32)
    carry_r, carry_i, hop_r, hop_i = lax.fori_loop(
        0, ROWS // BLOCK, block, (zero, zero, zero + 1.0, zero)
    )
    total = jnp.concatenate([carry_r, carry_i, hop_r, hop_i, jnp.zeros((4, N), f32)], axis=0)
    for k in range(8):
        sum_ref[k] = total


def scan_local(*arrays):
    return staged(
        scan_body,
        (
            shape((ROWS, BLOCK), bf16),
            shape((ROWS, BLOCK), f32),
            shape((ROWS, BLOCK), f32),
            shape((32, N), f32),
            shape((8, 8, N), f32),
        ),
        arrays,
        ROWS_SCRATCH + [pltpu.VMEM((ROWS, BLOCK), bf16), pltpu.VMEM((8, ROWS), f32)],
        flops=5 * 10**9,
        lazy=True,
        raw=(0, 1),
        free=(0, 1, 2),
    )


def finish_body(y_ref, ef_ref, pow_ref, hop_ref, all_ref, init_ref, ct_ref, out_ref):
    z = lax.axis_index("z")
    sr, si = init_ref[0:1, :], init_ref[1:2, :]
    for j in range(7):
        part = all_ref[j]
        nr, ni = cmul(part[2:3], part[3:4], sr, si)
        sr = jnp.where(j < z, nr + part[0:1], sr)
        si = jnp.where(j < z, ni + part[1:2], si)

    def block(b, _):
        rows = pl.ds(pl.multiple_of(b * BLOCK, BLOCK), BLOCK)
        hop = hop_ref[pl.ds(pl.multiple_of(b * 8, 8), 8), :]
        er, ei = cmul(hop[0:1], hop[1:2], sr, si)
        gr, gi = cmul(pow_ref[:BLOCK, :], pow_ref[BLOCK:, :], er, ei)
        more = mm_t(gr.astype(bf16), ct_ref[:, :N]) + mm_t(gi.astype(bf16), ct_ref[:, N:])
        v = y_ref[rows, :] + ef_ref[rows, :] * more
        inner = math.sqrt(2.0 / math.pi) * (v + 0.044715 * v * v * v)
        out_ref[rows, :] = (0.5 * v * (1.0 + jnp.tanh(inner))).astype(bf16)
        return 0

    lax.fori_loop(0, ROWS // BLOCK, block, 0)


def scan_finish(*arrays):
    return staged(finish_body, [shape((ROWS, BLOCK), bf16)], arrays, flops=2 * 10**9, free=(4,))


def out_body(recv_ref, own, up, down, far0, far1, keep_ref, send_ref, lhs_ref, sum_ref):
    x, c = lax.axis_index("x"), lax.axis_index("c")
    for k in range(4):
        lhs_ref[:, k * BLOCK : (k + 1) * BLOCK] = recv_ref[k, :, :BLOCK]
        lhs_ref[:, ROWS + k * BLOCK : ROWS + (k + 1) * BLOCK] = recv_ref[k, :, BLOCK:]
    for piece, step in ((own, 0), (up, 3), (down, 1), (None, 2)):
        if step == 2:
            total = mm(lhs_ref[:, :ROWS], far0[...]) + mm(lhs_ref[:, ROWS:], far1[...])
        else:
            total = mm(lhs_ref[...], piece[...])
        sum_ref[:, pl.ds(pl.multiple_of(((x + step) % 4) * ROWS, ROWS), ROWS)] = total
    keep_ref[...] = sum_ref[pl.ds(pl.multiple_of(c * 64, 64), 64), :]
    send_ref[...] = sum_ref[pl.ds(pl.multiple_of((1 - c) * 64, 64), 64), :].astype(bf16)


def project_out(recv, pieces):
    return staged(
        out_body,
        (shape((64, 2048), f32), shape((64, 2048), bf16)),
        [recv, *pieces],
        [pltpu.VMEM((BLOCK, 1024), bf16), pltpu.VMEM((BLOCK, 2048), f32)],
        flops=BLOCK * 1024 * 2048 * 2,
        free=range(6),
    )


def shift(a, axis, by):
    n = lax.axis_size(axis)
    return lax.ppermute(a, axis, [(i, (i + by) % n) for i in range(n)])


def ring4(a, axis, cut):
    up = shift(a, axis, 1)
    down = shift(a, axis, -1)
    far0 = shift(up[:cut], axis, 1)
    far1 = shift(down[cut:], axis, -1)
    return [a, up, down, far0, far1]


def after(a, b):
    return lax.optimization_barrier((a, b))[0]


def on_device(
    tokens,
    norm_gain,
    drive_weight,
    query_weight,
    key_weight,
    value_weight,
    key_offset,
    log_step,
    lambda_real,
    lambda_imag,
    input_map,
    output_map,
    skip_gain,
    forget,
    initial_state,
    scan_out_weight,
    attend_out_weight,
):
    def exchange(a, axis):
        return lax.all_to_all(a, axis, split_axis=0, concat_axis=0, tiled=True)

    kv_columns, qd_columns = pack(key_weight, value_weight, query_weight, drive_weight)
    w_kv = exchange(kv_columns, "x").reshape(2048, 2 * BLOCK)
    normed = normalize(tokens, norm_gain, forget[:, 0, :], key_offset[:, 0, :])
    mine = exchange(normed, "y")
    theirs = shift(mine, "c", 1)
    w_qd = exchange(after(qd_columns, w_kv), "x")
    tables = scan_tables(
        input_map.transpose(0, 1, 3, 2),
        output_map,
        lambda_real,
        lambda_imag,
        jnp.broadcast_to(log_step[:, None], lambda_real.shape),
        initial_state,
        skip_gain.reshape(1, -1),
    )
    out_rows = jnp.concatenate([scan_out_weight, attend_out_weight], axis=0)
    theirs, tables, out_rows = lax.optimization_barrier((theirs, tables, out_rows))
    power, inverse, b_map, c_map, init, skip = tables
    kv = project_kv(mine, theirs, w_kv)

    ups, downs = [kv], [kv]
    for k in range(1, 5):
        ups.append(shift(ups[-1], "z", 1))
        if k < 4:
            downs.append(shift(downs[-1], "z", -1))

    q, y_local, ef, hop, summary = scan_local(
        mine, theirs, w_qd.reshape(2048, 2 * BLOCK), power, inverse, b_map, c_map, skip
    )
    out_pieces = ring4(after(out_rows, q), "x", 512)
    everyone = exchange(summary, "z")
    acc, fall, far = attend_near(q, kv, ups[1], downs[1])
    scan_out = scan_finish(y_local, ef, power, hop, everyone, init, c_map)
    acc, fall, far = attend_middle(q, acc, fall, far, ups, downs)
    both = attend_last(q, ups[4], acc, fall, far, scan_out)
    recv = exchange(both.reshape(4, BLOCK, 2 * BLOCK), "y")
    keep, send = project_out(recv, out_pieces)
    return (keep + shift(send, "c", 1).astype(f32)).astype(bf16)[None]


def solution(mesh):
    split = Mesh(
        mesh.devices.reshape(8, 4, mesh.shape["fs"], mesh.shape["tp"]), ("z", "y", "x", "c")
    )
    in_specs = (
        P("x", SP_TP, None),
        P(),
        P("x", "c"),
        P("x", "c"),
        P("x", "c"),
        P("x", "c"),
        P("c", "x", SP),
        P("c"),
        P("c", None),
        P("c", None),
        P(None, "c", None, None),
        P(None, "c", None, None),
        P("c"),
        P("c", "x", SP),
        P(None, "x", "c", None),
        P("c", "x"),
        P("c", "x"),
    )
    out_specs = P("x", SP_TP, None)

    return jax.shard_map(
        on_device, mesh=split, in_specs=in_specs, out_specs=out_specs, check_vma=False
    )
```

profile of v0, /device:TPU:231, one launch (start us, length us, event | category | flops | bytes accessed | tf_op | source)
XLA Modules:
  0.0 148.4 jit_solution(1271265183248815103)
XLA Ops:
  0.0 2.2 %shard_map.163 = bf16[4,72,2048]{2,1,0:T(8,128)(2,1)} custom-call(bf16[1,64,2048]{2,1,0:T(8,128)(2,1)} %refs_0_.1, f32[1,2048]{1,0:T(1,128)} %bitcast.13, f32[32,128]{1,0:T(8,128)} %bitcast.12, bf16[4,128]{1,0:T(4,128)(2,1)} %bitcast.14), custom_call_target="tpu_custom_call" | custom-call | flops 1000000 | bytes 1048576 | tf_op jit(solution)/shard_map/pallas_call | solution.py:63
  2.2 4.2 %all-to-all-start = ((bf16[4,72,2048]{2,1,0:T(8,128)(2,1)}), bf16[4,72,2048]{2,1,0:T(8,128)(2,1)S(1)}, u32[]{:S(2)}, u32[]{:S(2)}) async-start(bf16[4,72,2048]{2,1,0:T(8,128)(2,1)} %shard_map.163), calls=%async_computation | async-start | bytes 2359296 | tf_op jit(solution)/shard_map/all_to_all | solution.py:623
  6.4 2.4 %pack.1 = (bf16[4,512,256]{2,1,0:T(8,128)(2,1)}, bf16[4,512,256]{2,1,0:T(8,128)(2,1)}) custom-call(bf16[512,512]{1,0:T(8,128)(2,1)} %k_ref.1, bf16[512,512]{1,0:T(8,128)(2,1)} %v_ref.1, bf16[512,512]{1,0:T(8,128)(2,1)} %q_ref.1, bf16[512,512]{1,0:T(8,128)(2,1)} %d_ref.1), custom_call_target="tpu_custom_call" | custom-call | tf_op jit(solution)/shard_map/pack/pallas_call | solution.py:148
  8.8 13.2 %all-to-all-done.refs_0_ = bf16[4,72,2048]{2,1,0:T(8,128)(2,1)S(1)} async-done(((bf16[4,72,2048]{2,1,0:T(8,128)(2,1)}), bf16[4,72,2048]{2,1,0:T(8,128)(2,1)S(1)}, u32[]{:S(2)}, u32[]{:S(2)}) %all-to-all-start) | async-done | bytes 1179680 | tf_op jit(solution)/shard_map/all_to_all | solution.py:623
  22.1 4.2 %all-to-all-start.1 = ((bf16[4,512,256]{2,1,0:T(8,128)(2,1)}), bf16[4,512,256]{2,1,0:T(8,128)(2,1)S(1)}, u32[]{:S(2)}, u32[]{:S(2)}) async-start(bf16[4,512,256]{2,1,0:T(8,128)(2,1)} %get-tuple-element.44), calls=%async_computation.1 | async-start | bytes 2097152 | tf_op jit(solution)/shard_map/all_to_all | solution.py:623
  26.3 0.0 copy-start.2
  26.3 2.4 %collective-permute-start = (bf16[4,72,2048]{2,1,0:T(8,128)(2,1)S(1)}, bf16[4,72,2048]{2,1,0:T(8,128)(2,1)}, u32[]{:S(2)}, u32[]{:S(2)}) collective-permute-start(bf16[4,72,2048]{2,1,0:T(8,128)(2,1)S(1)} %all-to-all-done.refs_0_), channel_id=1, source_target_pairs={{0,1},{1,0},{2,3},{3,2},{4,5},{5,4},{6,7},{7,6},{8,9},{9,8},{10,11... | collective-permute-start | bytes 3538952 | tf_op jit(solution)/shard_map/ppermute | solution.py:588
  28.6 8.9 %all-to-all-done.1 = bf16[4,512,256]{2,1,0:T(8,128)(2,1)S(1)} async-done(((bf16[4,512,256]{2,1,0:T(8,128)(2,1)}), bf16[4,512,256]{2,1,0:T(8,128)(2,1)S(1)}, u32[]{:S(2)}, u32[]{:S(2)}) %all-to-all-start.1) | async-done | bytes 1048608 | tf_op jit(solution)/shard_map/all_to_all | solution.py:623
  37.6 6.0 %all-to-all-start.2 = ((bf16[4,512,256]{2,1,0:T(8,128)(2,1)}), bf16[4,512,256]{2,1,0:T(8,128)(2,1)}, u32[]{:S(2)}, u32[]{:S(2)}) async-start(bf16[4,512,256]{2,1,0:T(8,128)(2,1)} %get-tuple-element.45), calls=%async_computation.2 | async-start | bytes 2097152 | tf_op jit(solution)/shard_map/all_to_all | solution.py:623
  43.6 0.0 copy-done.2
  43.6 0.7 broadcast_in_dim.4.refs_4_
  44.2 0.0 copy-start
  44.2 0.0 copy-start.1
  44.2 3.9 %shard_map.164 = (f32[256,512]{1,0:T(8,128)}, f32[256,512]{1,0:T(8,128)}, bf16[128,1024]{1,0:T(8,128)(2,1)}, bf16[128,1024]{1,0:T(8,128)(2,1)}, f32[2,512]{1,0:T(2,128)}, /*index=5*/f32[1,128]{1,0:T(1,128)}) custom-call(f32[2,32,16,64]{3,2,1,0:T(8,128)} %bitcast.15, f32[2,32,16,64]{3,2,1,0:T(8,128)} %refs_1_.1, f32[32,64]{1,0:T(8,128)} %refs_2_.1, ...), custom_call_target="tpu_custom_call" | custom-call | flops 1000000000 | bytes 1048576 | tf_op jit(solution)/shard_map/pallas_call | solution.py:63
  48.2 0.0 copy-done
  48.2 0.0 copy-done.1
  48.2 0.1 pad_maximum_fusion.refs_1_
  48.3 0.0 collective-permute-done.refs_1_
  48.3 5.6 %all-to-all-done.2 = bf16[4,512,256]{2,1,0:T(8,128)(2,1)} async-done(((bf16[4,512,256]{2,1,0:T(8,128)(2,1)}), bf16[4,512,256]{2,1,0:T(8,128)(2,1)}, u32[]{:S(2)}, u32[]{:S(2)}) %all-to-all-start.2) | async-done | bytes 1048608 | tf_op jit(solution)/shard_map/all_to_all | solution.py:623
  53.8 7.5 %shard_map.165 = (bf16[512,128]{1,0:T(8,128)(2,1)}, f32[512,128]{1,0:T(8,128)}, f32[512,128]{1,0:T(8,128)}, f32[32,512]{1,0:T(8,128)}, f32[8,8,512]{2,1,0:T(8,128)}) custom-call(bf16[4,72,2048]{2,1,0:T(8,128)(2,1)S(1)} %all-to-all-done.refs_0_, bf16[4,72,2048]{2,1,0:T(8,128)(2,1)} %collective-permute-done.refs_1_, bf16[2048,256]{1,0:T(8,128)(2,1)} %bitcast.6.refs_2_, ...), custom_call_target="tpu_custom_call" | custom-call | flops 5000000000 | bytes 1048576 | tf_op jit(solution)/shard_map/pallas_call | solution.py:63
  61.4 0.1 collective-permute-start.9
  61.5 2.7 %collective-permute-start.8 = (bf16[1024,512]{1,0:T(8,128)(2,1)S(1)}, bf16[1024,512]{1,0:T(8,128)(2,1)}, u32[]{:S(2)}, u32[]{:S(2)}) collective-permute-start(bf16[1024,512]{1,0:T(8,128)(2,1)S(1)} %pad_maximum_fusion.refs_1_), channel_id=1, source_target_pairs={{0,2},{2,4},{4,6},{6,0},{1,3},{3,5},{5,7},{7,1},{8,10},{10,12},{12... | collective-permute-start | bytes 3145736 | tf_op jit(solution)/shard_map/ppermute | solution.py:588
  64.1 2.9 %shard_map.166.refs_1_ = bf16[528,256]{1,0:T(8,128)(2,1)} custom-call(bf16[4,72,2048]{2,1,0:T(8,128)(2,1)S(1)} %all-to-all-done.refs_0_, bf16[4,72,2048]{2,1,0:T(8,128)(2,1)} %collective-permute-done.refs_1_, bf16[2048,256]{1,0:T(8,128)(2,1)S(1)} %bitcast.10), custom_call_target="tpu_custom_call" | custom-call | flops 536870912 | bytes 1048576 | tf_op jit(solution)/shard_map/pallas_call | solution.py:63
  67.0 0.1 collective-permute-start.1
  67.1 1.5 collective-permute-start.5
  68.6 4.5 %collective-permute-done.1.refs_2_ = bf16[528,256]{1,0:T(8,128)(2,1)S(1)} collective-permute-done((bf16[528,256]{1,0:T(8,128)(2,1)}, bf16[528,256]{1,0:T(8,128)(2,1)S(1)}, u32[]{:S(2)}, u32[]{:S(2)}) %collective-permute-start.1) | collective-permute-done | bytes 270368 | tf_op jit(solution)/shard_map/ppermute | solution.py:588
  73.0 1.2 collective-permute-start.2
  74.2 0.1 collective-permute-done.5.refs_3_
  74.3 0.2 collective-permute-start.6
  74.5 6.5 %collective-permute-done.2.refs_4_ = bf16[528,256]{1,0:T(8,128)(2,1)S(1)} collective-permute-done((bf16[528,256]{1,0:T(8,128)(2,1)S(1)}, bf16[528,256]{1,0:T(8,128)(2,1)S(1)}, u32[]{:S(2)}, u32[]{:S(2)}) %collective-permute-start.2) | collective-permute-done | bytes 270368 | tf_op jit(solution)/shard_map/ppermute | solution.py:588
  81.0 0.9 collective-permute-start.3
  82.0 5.8 %all-to-all-start.3 = ((f32[8,8,512]{2,1,0:T(8,128)}), f32[8,8,512]{2,1,0:T(8,128)S(1)}, u32[]{:S(2)}, u32[]{:S(2)}) async-start(f32[8,8,512]{2,1,0:T(8,128)} %get-tuple-element.61), calls=%async_computation.3 | async-start | bytes 262144 | tf_op jit(solution)/shard_map/all_to_all | solution.py:623
  87.8 0.0 collective-permute-done.6.refs_5_
  87.8 1.2 collective-permute-start.7
  89.0 0.4 collective-permute-done.3.refs_6_
  89.4 1.1 collective-permute-start.4
  90.5 0.0 collective-permute-done.9.refs_3_
  90.5 1.9 %slice.9 = bf16[512,512]{1,0:T(8,128)(2,1)} slice(bf16[1024,512]{1,0:T(8,128)(2,1)} %collective-permute-done.9.refs_3_), slice={[512:1024], [0:512]} | slice | bytes 1048576 | tf_op jit(solution)/shard_map/slice | solution.py:595
  92.4 0.0 collective-permute-start.11
  92.4 0.0 collective-permute-done.8.refs_2_
  92.4 1.9 %slice.8 = bf16[512,512]{1,0:T(8,128)(2,1)} slice(bf16[1024,512]{1,0:T(8,128)(2,1)} %collective-permute-done.8.refs_2_), slice={[0:512], [0:512]} | slice | bytes 1048576 | tf_op jit(solution)/shard_map/slice | solution.py:594
  94.3 2.7 %collective-permute-start.10 = (bf16[512,512]{1,0:T(8,128)(2,1)}, bf16[512,512]{1,0:T(8,128)(2,1)S(1)}, u32[]{:S(2)}, u32[]{:S(2)}) collective-permute-start(bf16[512,512]{1,0:T(8,128)(2,1)} %slice.8), channel_id=1, source_target_pairs={{0,2},{2,4},{4,6},{6,0},{1,3},{3,5},{5,7},{7,1},{8,10},{10,12},{12... | collective-permute-start | bytes 1572872 | tf_op jit(solution)/shard_map/ppermute | solution.py:588
  96.9 0.0 all-to-all-done.3.refs_4_
  97.0 3.1 %shard_map.169.refs_5_ = bf16[512,128]{1,0:T(8,128)(2,1)} custom-call(f32[512,128]{1,0:T(8,128)} %get-tuple-element.58.refs_0_, f32[512,128]{1,0:T(8,128)} %get-tuple-element.59.refs_1_, f32[256,512]{1,0:T(8,128)} %get-tuple-element.46.refs_3_.refs_2_, f32[32,512]{1,0:T(8,128)} %get-tuple-element.60.refs_3_, f32[8,8,512]{2,1,0:T(8,128)S(1)} %all-to-all-done.3.refs_4_, ...), custom_call_target="tpu_custom_call" | custom-call | flops 2000000000 | bytes 1048576 | tf_op jit(solution)/shard_map/pallas_call | solution.py:63
  100.1 7.4 %shard_map.167 = (f32[512,128]{1,0:T(8,128)}, f32[512,128]{1,0:T(8,128)}, f32[512,128]{1,0:T(8,128)}) custom-call(bf16[512,128]{1,0:T(8,128)(2,1)} %get-tuple-element.51.refs_0_, bf16[528,256]{1,0:T(8,128)(2,1)} %shard_map.166.refs_1_, bf16[528,256]{1,0:T(8,128)(2,1)S(1)} %collective-permute-done.1.refs_2_, bf16[528,256]{1,0:T(8,128)(2,1)S(1)} %collective-permute-done.5.refs_3_), custom_call_target="tpu_custom_call" | custom-call | flops 805306368 | bytes 1048576 | tf_op jit(solution)/shard_map/pallas_call | solution.py:63
  107.5 0.0 collective-permute-done.7.refs_7_
  107.5 9.4 %shard_map.168 = (f32[512,128]{1,0:T(8,128)}, f32[512,128]{1,0:T(8,128)}, f32[512,128]{1,0:T(8,128)}) custom-call(bf16[512,128]{1,0:T(8,128)(2,1)} %get-tuple-element.51.refs_0_, f32[512,128]{1,0:T(8,128)} %get-tuple-element.52.refs_1_, f32[512,128]{1,0:T(8,128)} %get-tuple-element.53.refs_2_, f32[512,128]{1,0:T(8,128)} %get-tuple-element.54.refs_3_, ...), custom_call_target="tpu_custom_call" | custom-call | flops 1073741824 | bytes 1048576 | tf_op jit(solution)/shard_map/pallas_call | solution.py:63
  117.0 0.0 collective-permute-done.4.refs_1_
  117.0 3.8 %shard_map.170 = bf16[512,256]{1,0:T(8,128)(2,1)} custom-call(bf16[512,128]{1,0:T(8,128)(2,1)} %get-tuple-element.51.refs_0_, bf16[528,256]{1,0:T(8,128)(2,1)S(1)} %collective-permute-done.4.refs_1_, f32[512,128]{1,0:T(8,128)} %get-tuple-element.55.refs_2_, f32[512,128]{1,0:T(8,128)} %get-tuple-element.56.refs_3_, f32[512,128]{1,0:T(8,128)} %get-tuple-element.57.refs_4_, ...), custom_call_target="tpu_custom_call" | custom-call | flops 268435456 | bytes 1048576 | tf_op jit(solution)/shard_map/pallas_call | solution.py:63
  120.8 8.9 %all_to_all.25.refs_0_ = bf16[4,128,256]{2,1,0:T(8,128)(2,1)S(1)} all-to-all(bf16[4,128,256]{2,1,0:T(8,128)(2,1)} %bitcast.11), channel_id=1, replica_groups=mesh['z'=8,'y'=4,'x'=4,'c'=2] {'y'}, dimensions={0} | all-to-all | bytes 524288 | tf_op jit(solution)/shard_map/all_to_all | solution.py:623
  129.7 0.0 collective-permute-done.11.refs_5_
  129.7 0.0 collective-permute-done.10.refs_4_
  129.7 3.3 %shard_map.171 = (f32[64,2048]{1,0:T(8,128)}, bf16[64,2048]{1,0:T(8,128)(2,1)}) custom-call(bf16[4,128,256]{2,1,0:T(8,128)(2,1)S(1)} %all_to_all.25.refs_0_, bf16[1024,512]{1,0:T(8,128)(2,1)S(1)} %pad_maximum_fusion.refs_1_, bf16[1024,512]{1,0:T(8,128)(2,1)} %collective-permute-done.8.refs_2_, bf16[1024,512]{1,0:T(8,128)(2,1)} %collective-permute-done.9.refs_3_, ...), custom_call_target="tpu_custom_call" | custom-call | flops 536870912 | bytes 1048576 | tf_op jit(solution)/shard_map/pallas_call | solution.py:63
  133.1 12.1 %collective-permute-start.12 = (bf16[64,2048]{1,0:T(8,128)(2,1)}, bf16[64,2048]{1,0:T(8,128)(2,1)S(1)}, u32[]{:S(2)}, u32[]{:S(2)}) collective-permute-start(bf16[64,2048]{1,0:T(8,128)(2,1)} %get-tuple-element.66), channel_id=1, source_target_pairs={{0,1},{1,0},{2,3},{3,2},{4,5},{5,4},{6,7},{7,6},{8,9},{9,8},{10,11... | collective-permute-start | bytes 786440 | tf_op jit(solution)/shard_map/ppermute | solution.py:588
  145.2 1.4 collective-permute-done.12
  146.6 1.8 %fusion = bf16[1,64,2048]{2,1,0:T(8,128)(2,1)} fusion(f32[64,2048]{1,0:T(8,128)} %get-tuple-element.65, bf16[64,2048]{1,0:T(8,128)(2,1)S(1)} %collective-permute-done.12), kind=kLoop, calls=%fused_computation.2 | loop fusion | flops 393216 | bytes 1048576 | tf_op jit(solution)/shard_map/broadcast_in_dim | solution.py:662
Async XLA Ops:
  2.2 19.8 %all-to-all-start = ((bf16[4,72,2048]{2,1,0:T(8,128)(2,1)}), bf16[4,72,2048]{2,1,0:T(8,128)(2,1)S(1)}, u32[]{:S(2)}, u32[]{:S(2)}) async-start(bf16[4,72,2048]{2,1,0:T(8,128)(2,1)} %shard_map.163), calls=%async_computation | async-start | bytes 2359296 | tf_op jit(solution)/shard_map/all_to_all | solution.py:623
  22.1 15.5 %all-to-all-start.1 = ((bf16[4,512,256]{2,1,0:T(8,128)(2,1)}), bf16[4,512,256]{2,1,0:T(8,128)(2,1)S(1)}, u32[]{:S(2)}, u32[]{:S(2)}) async-start(bf16[4,512,256]{2,1,0:T(8,128)(2,1)} %get-tuple-element.44), calls=%async_computation.1 | async-start | bytes 2097152 | tf_op jit(solution)/shard_map/all_to_all | solution.py:623
  26.3 17.3 %copy-start.2 = (f32[32]{0:T(128)S(1)}, f32[32]{0:T(128)}, u32[]{:S(2)}) copy-start(f32[32]{0:T(128)} %param.24) | copy-start | bytes 388
  26.3 22.0 %collective-permute-start = (bf16[4,72,2048]{2,1,0:T(8,128)(2,1)S(1)}, bf16[4,72,2048]{2,1,0:T(8,128)(2,1)}, u32[]{:S(2)}, u32[]{:S(2)}) collective-permute-start(bf16[4,72,2048]{2,1,0:T(8,128)(2,1)S(1)} %all-to-all-done.refs_0_), channel_id=1, source_target_pairs={{0,1},{1,0},{2,3},{3,2},{4,5},{5,4},{6,7},{7,6},{8,9},{9,8},{10,11... | collective-permute-start | bytes 3538952 | tf_op jit(solution)/shard_map/ppermute | solution.py:588
  37.6 16.3 %all-to-all-start.2 = ((bf16[4,512,256]{2,1,0:T(8,128)(2,1)}), bf16[4,512,256]{2,1,0:T(8,128)(2,1)}, u32[]{:S(2)}, u32[]{:S(2)}) async-start(bf16[4,512,256]{2,1,0:T(8,128)(2,1)} %get-tuple-element.45), calls=%async_computation.2 | async-start | bytes 2097152 | tf_op jit(solution)/shard_map/all_to_all | solution.py:623
  44.2 3.9 %copy-start = (bf16[512,512]{1,0:T(8,128)(2,1)S(1)}, bf16[512,512]{1,0:T(8,128)(2,1)}, u32[]{:S(2)}) copy-start(bf16[512,512]{1,0:T(8,128)(2,1)} %param.33) | copy-start | bytes 1572868
  44.2 3.9 %copy-start.1 = (bf16[512,512]{1,0:T(8,128)(2,1)S(1)}, bf16[512,512]{1,0:T(8,128)(2,1)}, u32[]{:S(2)}) copy-start(bf16[512,512]{1,0:T(8,128)(2,1)} %param.32) | copy-start | bytes 1572868
  61.4 29.1 %collective-permute-start.9 = (bf16[1024,512]{1,0:T(8,128)(2,1)S(1)}, bf16[1024,512]{1,0:T(8,128)(2,1)}, u32[]{:S(2)}, u32[]{:S(2)}) collective-permute-start(bf16[1024,512]{1,0:T(8,128)(2,1)S(1)} %pad_maximum_fusion.refs_1_), channel_id=1, source_target_pairs={{0,6},{2,0},{4,2},{6,4},{1,7},{3,1},{5,3},{7,5},{8,14},{10,8},{12,... | collective-permute-start | bytes 3145736 | tf_op jit(solution)/shard_map/ppermute | solution.py:588
  61.5 30.9 %collective-permute-start.8 = (bf16[1024,512]{1,0:T(8,128)(2,1)S(1)}, bf16[1024,512]{1,0:T(8,128)(2,1)}, u32[]{:S(2)}, u32[]{:S(2)}) collective-permute-start(bf16[1024,512]{1,0:T(8,128)(2,1)S(1)} %pad_maximum_fusion.refs_1_), channel_id=1, source_target_pairs={{0,2},{2,4},{4,6},{6,0},{1,3},{3,5},{5,7},{7,1},{8,10},{10,12},{12... | collective-permute-start | bytes 3145736 | tf_op jit(solution)/shard_map/ppermute | solution.py:588
  67.0 6.0 %collective-permute-start.1 = (bf16[528,256]{1,0:T(8,128)(2,1)}, bf16[528,256]{1,0:T(8,128)(2,1)S(1)}, u32[]{:S(2)}, u32[]{:S(2)}) collective-permute-start(bf16[528,256]{1,0:T(8,128)(2,1)} %shard_map.166.refs_1_), channel_id=1, source_target_pairs={{0,32},{32,64},{64,96},{96,128},{128,160},{160,192},{192,224},{224... | collective-permute-start | bytes 811016 | tf_op jit(solution)/shard_map/ppermute | solution.py:588
  67.1 7.2 %collective-permute-start.5 = (bf16[528,256]{1,0:T(8,128)(2,1)}, bf16[528,256]{1,0:T(8,128)(2,1)S(1)}, u32[]{:S(2)}, u32[]{:S(2)}) collective-permute-start(bf16[528,256]{1,0:T(8,128)(2,1)} %shard_map.166.refs_1_), channel_id=1, source_target_pairs={{0,224},{32,0},{64,32},{96,64},{128,96},{160,128},{192,160},{224,1... | collective-permute-start | bytes 811016 | tf_op jit(solution)/shard_map/ppermute | solution.py:588
  73.0 8.0 %collective-permute-start.2 = (bf16[528,256]{1,0:T(8,128)(2,1)S(1)}, bf16[528,256]{1,0:T(8,128)(2,1)S(1)}, u32[]{:S(2)}, u32[]{:S(2)}) collective-permute-start(bf16[528,256]{1,0:T(8,128)(2,1)S(1)} %collective-permute-done.1.refs_2_), channel_id=1, source_target_pairs={{0,32},{32,64},{64,96},{96,128},{128,160},{160,192},{192,224},{224... | collective-permute-start | bytes 811016 | tf_op jit(solution)/shard_map/ppermute | solution.py:588
  74.3 13.5 %collective-permute-start.6 = (bf16[528,256]{1,0:T(8,128)(2,1)S(1)}, bf16[528,256]{1,0:T(8,128)(2,1)}, u32[]{:S(2)}, u32[]{:S(2)}) collective-permute-start(bf16[528,256]{1,0:T(8,128)(2,1)S(1)} %collective-permute-done.5.refs_3_), channel_id=1, source_target_pairs={{0,224},{32,0},{64,32},{96,64},{128,96},{160,128},{192,160},{224,1... | collective-permute-start | bytes 811016 | tf_op jit(solution)/shard_map/ppermute | solution.py:588
  81.0 8.3 %collective-permute-start.3 = (bf16[528,256]{1,0:T(8,128)(2,1)S(1)}, bf16[528,256]{1,0:T(8,128)(2,1)}, u32[]{:S(2)}, u32[]{:S(2)}) collective-permute-start(bf16[528,256]{1,0:T(8,128)(2,1)S(1)} %collective-permute-done.2.refs_4_), channel_id=1, source_target_pairs={{0,32},{32,64},{64,96},{96,128},{128,160},{160,192},{192,224},{224... | collective-permute-start | bytes 811016 | tf_op jit(solution)/shard_map/ppermute | solution.py:588
  82.0 15.0 %all-to-all-start.3 = ((f32[8,8,512]{2,1,0:T(8,128)}), f32[8,8,512]{2,1,0:T(8,128)S(1)}, u32[]{:S(2)}, u32[]{:S(2)}) async-start(f32[8,8,512]{2,1,0:T(8,128)} %get-tuple-element.61), calls=%async_computation.3 | async-start | bytes 262144 | tf_op jit(solution)/shard_map/all_to_all | solution.py:623
  87.8 19.7 %collective-permute-start.7 = (bf16[528,256]{1,0:T(8,128)(2,1)}, bf16[528,256]{1,0:T(8,128)(2,1)}, u32[]{:S(2)}, u32[]{:S(2)}) collective-permute-start(bf16[528,256]{1,0:T(8,128)(2,1)} %collective-permute-done.6.refs_5_), channel_id=1, source_target_pairs={{0,224},{32,0},{64,32},{96,64},{128,96},{160,128},{192,160},{224,1... | collective-permute-start | bytes 811016 | tf_op jit(solution)/shard_map/ppermute | solution.py:588
  89.4 27.6 %collective-permute-start.4 = (bf16[528,256]{1,0:T(8,128)(2,1)}, bf16[528,256]{1,0:T(8,128)(2,1)S(1)}, u32[]{:S(2)}, u32[]{:S(2)}) collective-permute-start(bf16[528,256]{1,0:T(8,128)(2,1)} %collective-permute-done.3.refs_6_), channel_id=1, source_target_pairs={{0,32},{32,64},{64,96},{96,128},{128,160},{160,192},{192,224},{224... | collective-permute-start | bytes 811016 | tf_op jit(solution)/shard_map/ppermute | solution.py:588
  92.4 37.4 %collective-permute-start.11 = (bf16[512,512]{1,0:T(8,128)(2,1)}, bf16[512,512]{1,0:T(8,128)(2,1)S(1)}, u32[]{:S(2)}, u32[]{:S(2)}) collective-permute-start(bf16[512,512]{1,0:T(8,128)(2,1)} %slice.9), channel_id=1, source_target_pairs={{0,6},{2,0},{4,2},{6,4},{1,7},{3,1},{5,3},{7,5},{8,14},{10,8},{12,... | collective-permute-start | bytes 1572872 | tf_op jit(solution)/shard_map/ppermute | solution.py:588
  94.3 35.5 %collective-permute-start.10 = (bf16[512,512]{1,0:T(8,128)(2,1)}, bf16[512,512]{1,0:T(8,128)(2,1)S(1)}, u32[]{:S(2)}, u32[]{:S(2)}) collective-permute-start(bf16[512,512]{1,0:T(8,128)(2,1)} %slice.8), channel_id=1, source_target_pairs={{0,2},{2,4},{4,6},{6,0},{1,3},{3,5},{5,7},{7,1},{8,10},{10,12},{12... | collective-permute-start | bytes 1572872 | tf_op jit(solution)/shard_map/ppermute | solution.py:588
  133.1 13.5 %collective-permute-start.12 = (bf16[64,2048]{1,0:T(8,128)(2,1)}, bf16[64,2048]{1,0:T(8,128)(2,1)S(1)}, u32[]{:S(2)}, u32[]{:S(2)}) collective-permute-start(bf16[64,2048]{1,0:T(8,128)(2,1)} %get-tuple-element.66), channel_id=1, source_target_pairs={{0,1},{1,0},{2,3},{3,2},{4,5},{5,4},{6,7},{7,6},{8,9},{9,8},{10,11... | collective-permute-start | bytes 786440 | tf_op jit(solution)/shard_map/ppermute | solution.py:588
where the time goes:
time: 149 us; the launch traced here: 148 us
  starting transfers between devices  46.3 us (31%)
  Pallas kernels  46.1 us (31%)
  waiting for transfers between devices  40.6 us (27%)
  blocking collectives  8.91 us (6%)
  local copies, waits for them, and re-layouts  4.45 us (3%)
  other arithmetic  1.86 us (1%)
    pallas_call x9, Pallas kernels, staged(): pl.pallas_call(kernel, out_shape=tuple((pltpu.HBM(o.shape, o.dtype) for o...  43.7 us
    all_to_all x4, waiting for transfers between devices, exchange(): return lax.all_to_all(a, axis, split_axis=0, concat_axis=0, tiled=True)  27.8 us
    ppermute x13, starting transfers between devices, shift(): return lax.ppermute(a, axis, [(i, (i + by) % n) for i in range(n)])  26.1 us
    all_to_all x4, starting transfers between devices, exchange(): return lax.all_to_all(a, axis, split_axis=0, concat_axis=0, tiled=True)  20.2 us
    ppermute x13, waiting for transfers between devices, shift(): return lax.ppermute(a, axis, [(i, (i + by) % n) for i in range(n)])  12.9 us
    all_to_all x1, blocking collectives, exchange(): return lax.all_to_all(a, axis, split_axis=0, concat_axis=0, tiled=True)  8.91 us
  transfers between devices with their start and end apart: 17, of which 8 were waited for; matrix products, arithmetic and copies ran while one was open for 3% of the time, Pallas kernels for 22%

commit v1 on v0

v1 whole, which is shorter than its diff:
```python
import math

import jax
import jax.numpy as jnp
from jax import lax
from jax.experimental import pallas as pl
from jax.experimental.pallas import tpu as pltpu
from jax.sharding import Mesh
from jax.sharding import PartitionSpec as P


HEAD_DIM = 128
BLOCK = 128
ROWS = 512
EXTRA = 16
MORE = 8
SP = ("z", "y")
SP_TP = ("z", "y", "c")
LOG2E = 1.4426950408889634
SCORE = HEAD_DIM ** (-0.5) * LOG2E
epsilon = 1e-06
f32 = jnp.float32
bf16 = jnp.bfloat16
INTERPRET = False


def staged(body, outs, arrays, scratch=(), flops=0, limit=20, lazy=False, raw=(), free=(), vin=(), vout=(), alias=()):
    n, m = len(arrays), len(outs)
    kept = [i for i in range(n) if i not in raw]

    def kernel(*refs):
        nv, mv = len(vin), len(vout)
        src, near_in = refs[:n], refs[n : n + nv]
        refs = refs[n + nv :]
        dst, near_out = refs[:m], refs[m : m + mv]
        refs = refs[m + mv :]
        bufs = dict(zip(kept, refs[: len(kept)]))
        results = refs[len(kept) : len(kept) + m]
        sems, rest = refs[len(kept) + m], refs[len(kept) + m + 1 :]
        copies = {i: pltpu.make_async_copy(src[i], bufs[i], sems.at[i]) for i in kept}
        for i in kept:
            copies[i].start()
        leaving = {}

        def ready(*which):
            for i in which:
                copies[i].wait()

        def send(i):
            leaving[i] = pltpu.make_async_copy(results[i], dst[i], sems.at[n + i])
            leaving[i].start()

        ins = [bufs.get(i, src[i]) for i in range(n)]
        if lazy:
            body(ready, send, *ins, *near_in, *results, *near_out, *rest)
        else:
            ready(*kept)
            body(*ins, *near_in, *results, *near_out, *rest)
        for i in range(m):
            if i not in leaving:
                send(i)
        for i in range(m):
            leaving[i].wait()

    hbm = pl.BlockSpec(memory_space=pltpu.HBM)
    near = pl.BlockSpec(memory_space=pltpu.VMEM)
    got = pl.pallas_call(
        kernel,
        out_shape=tuple(pltpu.HBM(o.shape, o.dtype) for o in outs) + tuple(vout),
        in_specs=[hbm] * n + [near] * len(vin),
        out_specs=(hbm,) * m + (near,) * len(vout),
        input_output_aliases={n + i: m + o for i, o in alias},
        scratch_shapes=[pltpu.VMEM(arrays[i].shape, arrays[i].dtype) for i in kept]
        + [pltpu.VMEM(o.shape, o.dtype) for o in outs]
        + [pltpu.SemaphoreType.DMA((n + m,))]
        + list(scratch),
        cost_estimate=pl.CostEstimate(flops=flops, transcendentals=0, bytes_accessed=1 << 20),
        compiler_params=pltpu.CompilerParams(vmem_limit_bytes=limit << 20),
        interpret=INTERPRET,
    )(*(a if i in free else pltpu.with_memory_space_constraint(a, pltpu.HBM) for i, a in enumerate(arrays)), *vin)
    return got if len(got) > 1 else got[0]


def shape(dims, dtype):
    return jax.ShapeDtypeStruct(dims, dtype)


def split2(v):
    hi = v.astype(bf16)
    return hi, (v - hi.astype(f32)).astype(bf16)


def mm(a, b):
    return jnp.dot(a, b, preferred_element_type=f32)


def mm_t(a, b):
    return lax.dot_general(a, b, (((1,), (1,)), ((), ())), preferred_element_type=f32)


def norm_body(
    ready, send, tok_ref, gain_ref, forget_ref, off_ref, k_ref, v_ref, q_ref, d_ref, out_ref, a_ref, b_ref, sems
):
    at = pl.ds(pl.multiple_of(lax.axis_index("y") * BLOCK, BLOCK), BLOCK)
    copies = []
    for n, (ref, to, h) in enumerate(((k_ref, a_ref, 0), (v_ref, a_ref, 1), (q_ref, b_ref, 0), (d_ref, b_ref, 1))):
        copies.append(pltpu.make_async_copy(ref.at[:, at], to.at[:, pl.ds(h * BLOCK, BLOCK)], sems.at[n]))
    for copy in copies:
        copy.start()
    ready(0, 1, 2, 3)
    v = tok_ref[0].astype(f32)
    scale = lax.rsqrt(jnp.mean(v * v, axis=1, keepdims=True) + epsilon)
    normed = (v * scale * gain_ref[...]).astype(bf16)
    hi, lo = split2(forget_ref[...])
    hi, lo = hi.astype(f32), lo.astype(f32)
    off = off_ref[...].astype(f32)
    blank = jnp.zeros((6, BLOCK), f32)
    for k in range(4):
        out_ref[k, :64, :] = normed
        for j in range(16):
            row = hi[8 * k + j : 8 * k + j + 1] if j < 8 else lo[8 * k + j - 8 : 8 * k + j - 7]
            last = off[k : k + 1] if j == 0 else jnp.zeros((1, BLOCK), f32)
            tile = jnp.concatenate([row, last, blank], axis=0)
            out_ref[k, 64:, j * BLOCK : (j + 1) * BLOCK] = tile.astype(bf16)
    send(0)
    for copy in copies:
        copy.wait()


def normalize(tokens, gain, forget, offset, *weights):
    return staged(
        norm_body,
        [shape((4, 64 + MORE, 2048), bf16), shape((ROWS, 256), bf16), shape((ROWS, 256), bf16)],
        [tokens, gain.reshape(1, -1), forget, offset, *weights],
        [pltpu.SemaphoreType.DMA((4,))],
        flops=10**6,
        lazy=True,
        raw=(4, 5, 6, 7),
    )


SPAN = 256
TILE = 32
WIDE = SPAN + BLOCK


def chunk(q_ref, kv_ref, acc_ref, fall_ref, scr, diagonal):
    s_ref, soft_ref, r_ref, w_ref, tri_ref = scr
    j = lax.broadcasted_iota(jnp.int32, (SPAN, WIDE), 0)
    k = lax.broadcasted_iota(jnp.int32, (SPAN, WIDE), 1)
    tri_ref[...] = jnp.where((j > k) | (k >= SPAN), 1.0, 0.0).astype(bf16)
    offs = kv_ref[ROWS : ROWS + EXTRA, :].astype(f32)
    off = jnp.concatenate([offs[0:1], offs[1:2]], axis=1) * LOG2E
    s_ref[...] = mm_t(q_ref[...], kv_ref[:ROWS, :BLOCK])

    def visible(i):
        t = lax.broadcasted_iota(jnp.int32, (TILE, ROWS), 0) + i * TILE
        s = lax.broadcasted_iota(jnp.int32, (TILE, ROWS), 1)
        return s < t

    def first(i, _):
        at = pl.ds(pl.multiple_of(i * TILE, TILE), TILE)
        z = s_ref[at, :] * SCORE + off
        soft = jnp.maximum(z, 0.0) + jnp.log2(1.0 + jnp.exp2(-jnp.abs(z)))
        s_ref[at, :] = z - soft
        if diagonal:
            soft = jnp.where(visible(i), soft, 0.0)
        soft_ref[at, :] = soft.astype(bf16)
        return 0

    lax.fori_loop(0, ROWS // TILE, first, 0, unroll=2)
    for blk in range(2):
        r_ref[:, blk * WIDE : (blk + 1) * WIDE] = mm(
            soft_ref[:, blk * SPAN : (blk + 1) * SPAN], tri_ref[...]
        )

    def second(i, _):
        at = pl.ds(pl.multiple_of(i * TILE, TILE), TILE)
        fall1 = fall_ref[at, :]
        fall0 = fall1 + r_ref[at, WIDE + SPAN :]
        fall_ref[at, :] = fall0 + r_ref[at, SPAN:WIDE]
        behind = jnp.concatenate(
            [
                r_ref[at, :BLOCK] + fall0,
                r_ref[at, BLOCK:SPAN] + fall0,
                r_ref[at, WIDE : WIDE + BLOCK] + fall1,
                r_ref[at, WIDE + BLOCK : WIDE + SPAN] + fall1,
            ],
            axis=1,
        )
        w = jnp.exp2(s_ref[at, :] - behind)
        if diagonal:
            w = jnp.where(visible(i), w, 0.0)
        w_ref[at, :] = w.astype(bf16)
        return 0

    lax.fori_loop(0, ROWS // TILE, second, 0, unroll=2)
    acc_ref[...] += mm(w_ref[...], kv_ref[:ROWS, BLOCK:])


ATTEND_SCRATCH = [
    pltpu.VMEM((ROWS, ROWS), f32),
    pltpu.VMEM((ROWS, ROWS), bf16),
    pltpu.VMEM((ROWS, 2 * WIDE), f32),
    pltpu.VMEM((ROWS, ROWS), bf16),
    pltpu.VMEM((SPAN, WIDE), bf16),
]
PAIR = (shape((ROWS, BLOCK), f32), shape((ROWS, BLOCK), f32))
ATTEND_FLOPS = 8 * ROWS * ROWS * BLOCK


def zero(ref):
    ref[...] = jnp.zeros(ref.shape, ref.dtype)


def attend_near(q, kv, up, down):
    def body(ready, send, kv_ref, up_ref, down_ref, q_ref, acc_ref, fall_ref, far_ref, low_ref, *scr):
        z = lax.axis_index("z")
        zero(acc_ref)
        zero(fall_ref)
        zero(far_ref)
        ready(0)
        chunk(q_ref, kv_ref, acc_ref, fall_ref, scr, True)
        ready(1, 2)

        @pl.when(z >= 1)
        def _():
            chunk(q_ref, up_ref, acc_ref, fall_ref, scr, False)

        @pl.when(z >= 7)
        def _():
            zero(low_ref)
            chunk(q_ref, down_ref, far_ref, low_ref, scr, False)

    return staged(
        body,
        (),
        [kv, up, down],
        [pltpu.VMEM((ROWS, BLOCK), f32)] + ATTEND_SCRATCH,
        flops=3 * ATTEND_FLOPS,
        lazy=True,
        free=(1, 2),
        vin=(q,),
        vout=PAIR + PAIR[:1],
    )


def attend_step(q, acc, fall, far, up, down, k):
    def body(ready, send, up_ref, down_ref, q_ref, _a, _b, _c, acc_ref, fall_ref, far_ref, low_ref, part_ref, *scr):
        z = lax.axis_index("z")
        ready(0, 1)

        @pl.when(z >= k)
        def _():
            chunk(q_ref, up_ref, acc_ref, fall_ref, scr, False)

        @pl.when(z + k >= 8)
        def _():
            zero(low_ref)
            zero(part_ref)
            chunk(q_ref, down_ref, part_ref, low_ref, scr, False)
            far_ref[...] = part_ref[...] + jnp.exp2(-low_ref[...]) * far_ref[...]

    return staged(
        body,
        (),
        [up, down],
        [pltpu.VMEM((ROWS, BLOCK), f32)] * 2 + ATTEND_SCRATCH,
        flops=2 * ATTEND_FLOPS,
        lazy=True,
        free=(0, 1),
        vin=(q, acc, fall, far),
        vout=PAIR + PAIR[:1],
        alias=((1, 0), (2, 1), (3, 2)),
    )


def attend_last(q, acc, fall, far, ups, downs, y, ef, power, hop, init, c_map):
    def body(
        ready, send, up4, y_ref, ef_ref, pow_ref, hop_ref, init_ref, ct_ref, *refs,
    ):
        heads = refs[:6]
        refs = refs[6:]
        q_ref, acc_in, fall_in, far_ref, out_ref, acc_ref, fall_ref, g_ref, head_ref, head_sem = refs[:10]
        scr = refs[10:]
        tails = [
            pltpu.make_async_copy(ref.at[pl.ds(ROWS + EXTRA, EXTRA)], head_ref.at[n], head_sem.at[n])
            for n, ref in enumerate(heads)
        ]
        for copy in tails:
            copy.start()
        acc_ref[...] = acc_in[...]
        fall_ref[...] = fall_in[...]
        ready(0)

        @pl.when(lax.axis_index("z") >= 4)
        def _():
            chunk(q_ref, up4, acc_ref, fall_ref, scr, False)

        for copy in tails:
            copy.wait()
        ready(1, 2, 3, 4, 5, 6)
        out_ref[:, BLOCK:] = (acc_ref[...] + jnp.exp2(-fall_ref[...]) * far_ref[...]).astype(bf16)

        def chunks(z):
            for n, k in enumerate((1, 2, 3)):
                yield head_ref[n], z + k >= 8
            yield up4[ROWS + EXTRA :, :], z >= 4
            for n, k in ((3, 3), (4, 2), (5, 1)):
                yield head_ref[n], z >= k

        out_ref[:, :BLOCK] = finish(chunks, y_ref, ef_ref, pow_ref, hop_ref, init_ref, ct_ref, g_ref)

    return staged(
        body,
        [shape((ROWS, 2 * BLOCK), bf16)],
        [ups[4], y, ef, power, hop, init, c_map, downs[1], downs[2], downs[3], ups[3], ups[2], ups[1]],
        [
            pltpu.VMEM((ROWS, BLOCK), f32),
            pltpu.VMEM((ROWS, BLOCK), f32),
            pltpu.VMEM((ROWS, 2 * N), bf16),
            pltpu.VMEM((6, EXTRA, 256), bf16),
            pltpu.SemaphoreType.DMA((6,)),
        ]
        + ATTEND_SCRATCH,
        flops=2 * ATTEND_FLOPS,
        lazy=True,
        raw=range(7, 13),
        free=(0,) + tuple(range(7, 13)),
        vin=(q, acc, fall, far),
    )


N = 512


def cmul(ar, ai, br, bi):
    return ar * br - ai * bi, ar * bi + ai * br


def tables_body(
    in_ref, out_ref, lam_r_ref, lam_i_ref, step_ref, start_ref, skip_in,
    pow_ref, inv_ref, b_ref, ct_ref, init_ref, skip_ref,
):
    y = lax.axis_index("y")
    own = pl.ds(pl.multiple_of(y * 8, 8), 8)
    copy = (
        lax.broadcasted_iota(jnp.int32, (64, N), 1) % 64 == lax.broadcasted_iota(jnp.int32, (64, N), 0)
    ).astype(f32)

    def tiled(a, height):
        rows, width = a.shape
        r = lax.broadcasted_iota(jnp.int32, (rows, N), 0) // height
        k = lax.broadcasted_iota(jnp.int32, (rows, N), 1) // width
        spread = jnp.dot(a, copy, precision=lax.Precision.HIGHEST, preferred_element_type=f32)
        return jnp.where(r == k, spread, 0.0)

    def line(a):
        return jnp.sum(tiled(a, 1), axis=0, keepdims=True)

    lam_r, lam_i, step = line(lam_r_ref[own]), line(lam_i_ref[own]), jnp.exp(line(step_ref[own]))
    init_ref[0:1, :] = line(start_ref[0, 0, own])
    init_ref[1:2, :] = line(start_ref[1, 0, own])
    skip_ref[...] = skip_in[:, pl.ds(pl.multiple_of(y * BLOCK, BLOCK), BLOCK)]
    gain = lam_r * step
    turn = lam_i * step
    size = jnp.exp(gain)
    bar_r = size * jnp.cos(turn)
    bar_i = size * jnp.sin(turn)
    over = lam_r * lam_r + lam_i * lam_i
    less = bar_r - 1.0
    factor_r = (less * lam_r + bar_i * lam_i) / over
    factor_i = (bar_i * lam_r - less * lam_i) / over
    count = lax.broadcasted_iota(jnp.int32, (BLOCK, N), 0) + 1
    pr = jnp.ones((BLOCK, N), f32)
    pi = jnp.zeros((BLOCK, N), f32)
    sr, si = bar_r, bar_i
    for bit in range(8):
        on = ((count >> bit) & 1) == 1
        nr, ni = cmul(pr, pi, sr, si)
        pr, pi = jnp.where(on, nr, pr), jnp.where(on, ni, pi)
        if bit < 7:
            sr, si = cmul(sr, si, sr, si)
    back = jnp.exp(-2.0 * count.astype(f32) * gain)
    pow_ref[:BLOCK, :] = pr
    pow_ref[BLOCK:, :] = pi
    br, bi = cmul(pr * back, -pi * back, factor_r, factor_i)
    inv_ref[:BLOCK, :] = br
    inv_ref[BLOCK:, :] = bi
    for p in range(2):
        b_ref[:, p * N : (p + 1) * N] = tiled(in_ref[p, own].reshape(BLOCK, 64), 16).astype(bf16)
        sign = 1.0 if p == 0 else -1.0
        ct_ref[:, p * N : (p + 1) * N] = (sign * tiled(out_ref[p, own].reshape(BLOCK, 64), 16)).astype(bf16)


def scan_tables(*arrays):
    return staged(
        tables_body,
        (
            shape((2 * BLOCK, N), f32),
            shape((2 * BLOCK, N), f32),
            shape((BLOCK, 2 * N), bf16),
            shape((BLOCK, 2 * N), bf16),
            shape((2, N), f32),
            shape((1, BLOCK), f32),
        ),
        arrays,
        flops=10**9,
    )


DEEP = ROWS + 2 * EXTRA


def project_body(
    ready, send, mine, theirs, a0, a3, a1, a2, b0, b3, b1, b2, pow_ref, inv_ref, b_ref, ct_ref, skip_ref,
    kv_ref, y_ref, ef_ref, hop_ref, q_ref,
    rows, sems, more, u_ref, f_ref, x_ref, st_ref, w_ref,
):
    c = lax.axis_index("c")
    x = lax.axis_index("x")
    copies = []
    for n, (step, ref) in enumerate(((0, a0), (3, a3), (1, a1), (2, a2), (0, b0), (3, b3), (1, b1), (2, b2))):
        at = pl.multiple_of(((x + step) % 4) * ROWS, ROWS)
        to = w_ref.at[pl.ds(at, ROWS), pl.ds(256 * (n // 4), 256)]
        copies.append(pltpu.make_async_copy(ref, to, sems.at[12 + n]))
    for b in range(4):
        for part, ref in enumerate((mine, theirs)):
            at = pl.multiple_of(b * BLOCK + ((c + part) % 2) * 64, 64)
            copies.append(
                pltpu.make_async_copy(ref.at[b, pl.ds(0, 64)], rows.at[pl.ds(at, 64)], sems.at[2 * b + part])
            )
    for b in range(4):
        copies.append(
            pltpu.make_async_copy(mine.at[b, pl.ds(64, MORE)], more.at[b], sems.at[8 + b])
        )
    for copy in copies:
        copy.start()
    for copy in copies:
        copy.wait()
    both = mm(rows[...], w_ref[...])
    kv_ref[:ROWS, :] = both[:, :256].astype(bf16)
    q_ref[...] = both[:, 256:384].astype(bf16)
    u_ref[...] = both[:, 384:].astype(bf16)
    offs = [more[b].astype(f32)[1:2, :BLOCK] for b in range(4)]
    row0 = jnp.concatenate(offs[:2], axis=1)
    row1 = jnp.concatenate(offs[2:], axis=1)
    tail = jnp.concatenate([row0, row1, jnp.zeros((EXTRA - 2, 256), f32)], axis=0)
    kv_ref[ROWS : ROWS + EXTRA, :] = tail.astype(bf16)
    for b in range(4):
        part = more[b].astype(f32)
        part = part[0:1, : 8 * BLOCK] + part[0:1, 8 * BLOCK :]
        f_ref[:, b * BLOCK : (b + 1) * BLOCK] = jnp.concatenate(
            [part[:, g * BLOCK : (g + 1) * BLOCK] for g in range(8)], axis=0
        )
    ready(10, 11, 12, 13, 14)
    row = lax.broadcasted_iota(jnp.int32, (BLOCK, BLOCK), 0)
    col = lax.broadcasted_iota(jnp.int32, (BLOCK, BLOCK), 1)
    low = (col <= row).astype(bf16)
    low32 = (col <= row).astype(f32)
    even = lax.broadcasted_iota(jnp.int32, (1, BLOCK), 1) < 64
    keeps = []
    blocks = [slice(b * BLOCK, (b + 1) * BLOCK) for b in range(4)]
    for at in blocks:
        f = f_ref[:, at]
        f_all = jnp.concatenate([jnp.broadcast_to(f[g : g + 1], (16, BLOCK)) for g in range(8)], axis=0)
        cum_f = lax.dot_general(
            low32, f_all, (((1,), (1,)), ((), ())), precision=lax.Precision.HIGHEST, preferred_element_type=f32
        )
        ef_ref[at, :] = jnp.exp(cum_f)
        x_ref[at, :BLOCK] = u_ref[at, :].astype(f32) * jnp.exp(-cum_f)
        total = jnp.exp(jnp.broadcast_to(jnp.sum(f, axis=1, keepdims=True), (8, BLOCK)))
        keeps.append(
            jnp.concatenate(
                [jnp.where(even, total[2 * g : 2 * g + 1], total[2 * g + 1 : 2 * g + 2]) for g in range(4)],
                axis=1,
            )
        )
    x_ref[...] = mm(x_ref[:, :BLOCK].astype(bf16), b_ref[...])
    carry_r = jnp.zeros((1, N), f32)
    carry_i = jnp.zeros((1, N), f32)
    hop_r = jnp.ones((1, N), f32)
    hop_i = jnp.zeros((1, N), f32)
    end_r, end_i = pow_ref[BLOCK - 1 : BLOCK, :], pow_ref[2 * BLOCK - 1 :, :]
    hops = []
    for at, keep in zip(blocks, keeps):
        dr, di = cmul(x_ref[at, :N], x_ref[at, N:], inv_ref[:BLOCK, :], inv_ref[BLOCK:, :])
        tr = mm(low, dr.astype(bf16)) + carry_r
        ti = mm(low, di.astype(bf16)) + carry_i
        st_r, st_i = cmul(pow_ref[:BLOCK, :], pow_ref[BLOCK:, :], tr, ti)
        st_ref[at, :N] = st_r.astype(bf16)
        st_ref[at, N:] = st_i.astype(bf16)
        carry_r, carry_i = keep * st_r[BLOCK - 1 :, :], keep * st_i[BLOCK - 1 :, :]
        hops += [hop_r, hop_i]
        nr, ni = cmul(hop_r, hop_i, end_r, end_i)
        hop_r, hop_i = keep * nr, keep * ni
    hop_ref[...] = jnp.concatenate(hops, axis=0)
    hi, lo = split2(jnp.concatenate([carry_r, carry_i, hop_r, hop_i], axis=0))
    hi, lo = hi.astype(f32), lo.astype(f32)
    kv_ref[ROWS + EXTRA :, :] = jnp.concatenate(
        [hi[:, :256], hi[:, 256:], lo[:, :256], lo[:, 256:]], axis=0
    ).astype(bf16)
    send(0)
    y_ref[...] = ef_ref[...] * mm_t(st_ref[...], ct_ref[...]) + skip_ref[...] * u_ref[...].astype(f32)


def project(*arrays):
    return staged(
        project_body,
        (
            shape((DEEP, 256), bf16),
            shape((ROWS, BLOCK), f32),
            shape((ROWS, BLOCK), f32),
            shape((8, N), f32),
        ),
        arrays,
        [
            pltpu.VMEM((ROWS, 2048), bf16),
            pltpu.SemaphoreType.DMA((20,)),
            pltpu.VMEM((4, MORE, 2048), bf16),
            pltpu.VMEM((ROWS, BLOCK), bf16),
            pltpu.VMEM((8, ROWS), f32),
            pltpu.VMEM((ROWS, 2 * N), f32),
            pltpu.VMEM((ROWS, 2 * N), bf16),
            pltpu.VMEM((2048, ROWS), bf16),
        ],
        flops=3 * 10**9,
        lazy=True,
        raw=range(10),
        free=range(10),
        vout=(shape((ROWS, BLOCK), bf16),),
        limit=32,
    )


def finish(chunks, y_ref, ef_ref, pow_ref, hop_ref, init_ref, ct_ref, g_ref):
    z = lax.axis_index("z")
    sr, si = init_ref[0:1, :], init_ref[1:2, :]
    for ref, active in chunks(z):
        part = ref.astype(f32)
        part = part[:8] + part[8:]
        part = jnp.concatenate([part[:4], part[4:]], axis=1)
        nr, ni = cmul(part[2:3], part[3:4], sr, si)
        sr = jnp.where(active, nr + part[0:1], sr)
        si = jnp.where(active, ni + part[1:2], si)
    for b in range(ROWS // BLOCK):
        at = slice(b * BLOCK, (b + 1) * BLOCK)
        er, ei = cmul(hop_ref[2 * b : 2 * b + 1, :], hop_ref[2 * b + 1 : 2 * b + 2, :], sr, si)
        gr, gi = cmul(pow_ref[:BLOCK, :], pow_ref[BLOCK:, :], er, ei)
        g_ref[at, :N] = gr.astype(bf16)
        g_ref[at, N:] = gi.astype(bf16)
    v = y_ref[...] + ef_ref[...] * mm_t(g_ref[...], ct_ref[...])
    inner = math.sqrt(2.0 / math.pi) * (v + 0.044715 * v * v * v)
    return (0.5 * v * (1.0 + jnp.tanh(inner))).astype(bf16)


def out_body(recv_ref, own, up, down, far0, far1, keep_ref, send_ref, lhs_ref, sum_ref):
    x, c = lax.axis_index("x"), lax.axis_index("c")
    for k in range(4):
        lhs_ref[:, k * BLOCK : (k + 1) * BLOCK] = recv_ref[k, :, :BLOCK]
        lhs_ref[:, ROWS + k * BLOCK : ROWS + (k + 1) * BLOCK] = recv_ref[k, :, BLOCK:]
    for piece, step in ((own, 0), (up, 3), (down, 1), (None, 2)):
        if step == 2:
            total = mm(lhs_ref[:, :ROWS], far0[...]) + mm(lhs_ref[:, ROWS:], far1[...])
        else:
            total = mm(lhs_ref[...], piece[...])
        sum_ref[:, pl.ds(pl.multiple_of(((x + step) % 4) * ROWS, ROWS), ROWS)] = total
    keep_ref[...] = sum_ref[pl.ds(pl.multiple_of(c * 64, 64), 64), :]
    send_ref[...] = sum_ref[pl.ds(pl.multiple_of((1 - c) * 64, 64), 64), :].astype(bf16)


def project_out(recv, pieces):
    return staged(
        out_body,
        (shape((64, 2048), f32), shape((64, 2048), bf16)),
        [recv, *pieces],
        [pltpu.VMEM((BLOCK, 1024), bf16), pltpu.VMEM((BLOCK, 2048), f32)],
        flops=BLOCK * 1024 * 2048 * 2,
        free=range(6),
    )


def shift(a, axis, by):
    n = lax.axis_size(axis)
    return lax.ppermute(a, axis, [(i, (i + by) % n) for i in range(n)])


def ring4(a, axis, cut):
    up = shift(a, axis, 1)
    down = shift(a, axis, -1)
    far0 = shift(up[:cut], axis, 1)
    far1 = shift(down[cut:], axis, -1)
    return [a, up, down, far0, far1]


def after(a, b):
    return lax.optimization_barrier((a, b))[0]


def on_device(
    tokens,
    norm_gain,
    drive_weight,
    query_weight,
    key_weight,
    value_weight,
    key_offset,
    log_step,
    lambda_real,
    lambda_imag,
    input_map,
    output_map,
    skip_gain,
    forget,
    initial_state,
    scan_out_weight,
    attend_out_weight,
):
    def exchange(a, axis):
        return lax.all_to_all(a, axis, split_axis=0, concat_axis=0, tiled=True)

    normed, w_a, w_b = normalize(
        tokens,
        norm_gain,
        forget[:, 0, :],
        key_offset[:, 0, :],
        key_weight,
        value_weight,
        query_weight,
        drive_weight,
    )
    a_up = shift(w_a, "x", 1)
    b_down = shift(w_b, "x", -1)
    b_up = shift(w_b, "x", 1)
    a_down = shift(w_a, "x", -1)
    a_far = shift(a_up, "x", 1)
    b_far = shift(b_down, "x", -1)
    weights = (w_a, a_up, a_down, a_far, w_b, b_up, b_down, b_far)
    mine = exchange(normed, "y")
    theirs = shift(mine, "c", 1)
    tables = scan_tables(
        input_map.transpose(0, 1, 3, 2),
        output_map,
        lambda_real,
        lambda_imag,
        jnp.broadcast_to(log_step[:, None], lambda_real.shape),
        initial_state,
        skip_gain.reshape(1, -1),
    )
    out_rows = jnp.concatenate([scan_out_weight, attend_out_weight], axis=0)
    theirs, tables, out_rows = lax.optimization_barrier((theirs, tables, out_rows))
    power, inverse, b_map, c_map, init, skip = tables
    kv, y_local, ef, hop, q = project(
        mine, theirs, *weights, power, inverse, b_map, c_map, skip
    )
    ups, downs = [kv], [kv]
    for k in range(1, 5):
        ups.append(shift(ups[-1], "z", 1))
        if k < 4:
            downs.append(shift(downs[-1], "z", -1))
    out_pieces = ring4(after(out_rows, kv), "x", 512)
    acc, fall, far = attend_near(q, kv, ups[1], downs[1])
    for k in (2, 3):
        acc, fall, far = attend_step(q, acc, fall, far, ups[k], downs[k], k)
    both = attend_last(q, acc, fall, far, ups, downs, y_local, ef, power, hop, init, c_map)
    recv = exchange(both.reshape(4, BLOCK, 2 * BLOCK), "y")
    keep, send = project_out(recv, out_pieces)
    return (keep + shift(send, "c", 1).astype(f32)).astype(bf16)[None]


def solution(mesh):
    split = Mesh(
        mesh.devices.reshape(8, 4, mesh.shape["fs"], mesh.shape["tp"]), ("z", "y", "x", "c")
    )
    in_specs = (
        P("x", SP_TP, None),
        P(),
        P("x", "c"),
        P("x", "c"),
        P("x", "c"),
        P("x", "c"),
        P("c", "x", SP),
        P("c"),
        P("c", None),
        P("c", None),
        P(None, "c", None, None),
        P(None, "c", None, None),
        P("c"),
        P("c", "x", SP),
        P(None, "x", "c", None),
        P("c", "x"),
        P("c", "x"),
    )
    out_specs = P("x", SP_TP, None)

    return jax.shard_map(on_device, mesh=split, in_specs=in_specs, out_specs=out_specs, check_vma=False)
```

time: 149 us -> 116 us (0.78)
  blocking collectives: 8.91 us -> 28.9 us
  starting transfers between devices: 46.3 us -> 28.2 us
  waiting for transfers between devices: 40.6 us -> 24.4 us
  Pallas kernels: 46.1 us -> 31.4 us
  local copies, waits for them, and re-layouts: 4.45 us -> 0.76 us
    all_to_all x4 -> x0, waiting for transfers between devices: 27.8 us -> none  [exchange(): return lax.all_to_all(a, axis, split_axis=0, concat_axis=0, tiled=True)]
    all_to_all x4 -> x0, starting transfers between devices: 20.2 us -> none  [exchange(): return lax.all_to_all(a, axis, split_axis=0, concat_axis=0, tiled=True)]
    all_to_all x1 -> x2, blocking collectives: 8.91 us -> 28.9 us  [exchange(): return lax.all_to_all(a, axis, split_axis=0, concat_axis=0, tiled=True)]
    pallas_call x9 -> x8, Pallas kernels: 43.7 us -> 31.4 us  [staged(): pl.pallas_call(kernel, out_shape=tuple((pltpu.HBM(o.shape, o.dtype) for o...]
    ppermute x13 -> x19, waiting for transfers between devices: 12.9 us -> 24.4 us  [shift(): return lax.ppermute(a, axis, [(i, (i + by) % n) for i in range(n)])]
    pallas_call x1 -> x0, Pallas kernels: 2.39 us -> none  [pack(): pl.pallas_call(pack_body, out_shape=(packed, packed), in_specs=[anywhere]...]
    ppermute x13 -> x19, starting transfers between devices: 26.1 us -> 28.2 us  [shift(): return lax.ppermute(a, axis, [(i, (i + by) % n) for i in range(n)])]
    slice x1, local copies, waits for them, and re-layouts: 1.89 us -> 0.03 us  [ring4(): far1 = shift(down[cut:], axis, -1)]
  transfers between devices with their start and end apart: 17 -> 19, of which waited for: 8 -> 9; matrix products, arithmetic and copies ran while one was open for 3% -> 1% of each run, Pallas kernels for 22% -> 18%
where the time goes in v1:
time: 116 us
  Pallas kernels  31.4 us (27%)
  blocking collectives  28.9 us (25%)
  starting transfers between devices  28.2 us (24%)
  waiting for transfers between devices  24.4 us (21%)
  other arithmetic  1.87 us (2%)
    pallas_call x8, Pallas kernels, staged(): pl.pallas_call(kernel, out_shape=tuple((pltpu.HBM(o.shape, o.dtype) for o...  31.4 us
    all_to_all x2, blocking collectives, exchange(): return lax.all_to_all(a, axis, split_axis=0, concat_axis=0, tiled=True)  28.9 us
    ppermute x19, starting transfers between devices, shift(): return lax.ppermute(a, axis, [(i, (i + by) % n) for i in range(n)])  28.2 us
    ppermute x19, waiting for transfers between devices, shift(): return lax.ppermute(a, axis, [(i, (i + by) % n) for i in range(n)])  24.4 us
  transfers between devices with their start and end apart: 19, of which 9 were waited for; matrix products, arithmetic and copies ran while one was open for 1% of the time, Pallas kernels for 18%

profile of v1, /device:TPU:231, one launch (start us, length us, event | category | flops | bytes accessed | tf_op | source)
XLA Modules:
  0.0 115.7 jit_solution(4216976160931462239)
XLA Ops:
  0.0 2.4 %shard_map.163 = (bf16[4,72,2048]{2,1,0:T(8,128)(2,1)}, bf16[512,256]{1,0:T(8,128)(2,1)}, bf16[512,256]{1,0:T(8,128)(2,1)}) custom-call(bf16[1,64,2048]{2,1,0:T(8,128)(2,1)} %refs_0_.1, f32[1,2048]{1,0:T(1,128)} %bitcast.10, f32[32,128]{1,0:T(8,128)} %bitcast.9, bf16[4,128]{1,0:T(4,128)(2,1)} %bitcast.11, bf16[512,512]{1,0:T(8,128)(2,1)} %refs_4_.1, ...), custom_call_target="tpu_custom_call" | custom-call | flops 1000000 | bytes 1048576 | tf_op jit(solution)/shard_map/pallas_call | solution.py:67
  2.5 0.0 copy-start
  2.5 0.0 copy-start.1
  2.5 0.0 copy-start.4
  2.5 20.0 %all_to_all.10.refs_0_ = bf16[4,72,2048]{2,1,0:T(8,128)(2,1)S(1)} all-to-all(bf16[4,72,2048]{2,1,0:T(8,128)(2,1)} %get-tuple-element.39), channel_id=1, replica_groups=mesh['z'=8,'y'=4,'x'=4,'c'=2] {'y'}, dimensions={0} | all-to-all | bytes 2359296 | tf_op jit(solution)/shard_map/all_to_all | solution.py:620
  22.5 1.8 %collective-permute-start = (bf16[4,72,2048]{2,1,0:T(8,128)(2,1)S(1)}, bf16[4,72,2048]{2,1,0:T(8,128)(2,1)S(1)}, u32[]{:S(2)}, u32[]{:S(2)}) collective-permute-start(bf16[4,72,2048]{2,1,0:T(8,128)(2,1)S(1)} %all_to_all.10.refs_0_), channel_id=1, source_target_pairs={{0,1},{1,0},{2,3},{3,2},{4,5},{5,4},{6,7},{7,6},{8,9},{9,8},{10,11... | collective-permute-start | bytes 3538952 | tf_op jit(solution)/shard_map/ppermute | solution.py:585
  24.3 0.0 copy-done
  24.3 0.2 collective-permute-start.1
  24.5 0.0 copy-done.1
  24.5 1.3 %collective-permute-start.5 = (bf16[512,256]{1,0:T(8,128)(2,1)S(1)}, bf16[512,256]{1,0:T(8,128)(2,1)S(1)}, u32[]{:S(2)}, u32[]{:S(2)}) collective-permute-start(bf16[512,256]{1,0:T(8,128)(2,1)S(1)} %copy-done.1), channel_id=1, source_target_pairs={{0,6},{2,0},{4,2},{6,4},{1,7},{3,1},{5,3},{7,5},{8,14},{10,8},{12,... | collective-permute-start | bytes 786440 | tf_op jit(solution)/shard_map/ppermute | solution.py:585
  25.7 0.5 collective-permute-start.2
  26.3 2.1 %collective-permute-start.4 = (bf16[512,256]{1,0:T(8,128)(2,1)S(1)}, bf16[512,256]{1,0:T(8,128)(2,1)S(1)}, u32[]{:S(2)}, u32[]{:S(2)}) collective-permute-start(bf16[512,256]{1,0:T(8,128)(2,1)S(1)} %copy-done.1), channel_id=1, source_target_pairs={{0,2},{2,4},{4,6},{6,0},{1,3},{3,5},{5,7},{7,1},{8,10},{10,12},{12... | collective-permute-start | bytes 786440 | tf_op jit(solution)/shard_map/ppermute | solution.py:585
  28.4 3.7 %collective-permute-done.1.refs_3_ = bf16[512,256]{1,0:T(8,128)(2,1)S(1)} collective-permute-done((bf16[512,256]{1,0:T(8,128)(2,1)S(1)}, bf16[512,256]{1,0:T(8,128)(2,1)S(1)}, u32[]{:S(2)}, u32[]{:S(2)}) %collective-permute-start.1) | collective-permute-done | bytes 262176 | tf_op jit(solution)/shard_map/ppermute | solution.py:585
  32.1 1.4 %collective-permute-start.3 = (bf16[512,256]{1,0:T(8,128)(2,1)S(1)}, bf16[512,256]{1,0:T(8,128)(2,1)S(1)}, u32[]{:S(2)}, u32[]{:S(2)}) collective-permute-start(bf16[512,256]{1,0:T(8,128)(2,1)S(1)} %collective-permute-done.1.refs_3_), channel_id=1, source_target_pairs={{0,2},{2,4},{4,6},{6,0},{1,3},{3,5},{5,7},{7,1},{8,10},{10,12},{12... | collective-permute-start | bytes 786440 | tf_op jit(solution)/shard_map/ppermute | solution.py:585
  33.5 0.0 collective-permute-done.5.refs_8_
  33.5 0.1 collective-permute-start.6
  33.6 0.0 copy-done.4
  33.6 0.7 broadcast_in_dim.4.refs_4_
  34.3 0.0 copy-start.2
  34.3 0.0 copy-start.3
  34.3 3.9 %shard_map.164 = (f32[256,512]{1,0:T(8,128)}, f32[256,512]{1,0:T(8,128)}, bf16[128,1024]{1,0:T(8,128)(2,1)}, bf16[128,1024]{1,0:T(8,128)(2,1)}, f32[2,512]{1,0:T(2,128)}, /*index=5*/f32[1,128]{1,0:T(1,128)}) custom-call(f32[2,32,16,64]{3,2,1,0:T(8,128)} %bitcast.12, f32[2,32,16,64]{3,2,1,0:T(8,128)} %refs_1_.1, f32[32,64]{1,0:T(8,128)} %refs_2_.1, ...), custom_call_target="tpu_custom_call" | custom-call | flops 1000000000 | bytes 1048576 | tf_op jit(solution)/shard_map/pallas_call | solution.py:67
  38.2 0.0 copy-done.2
  38.2 0.0 copy-done.3
  38.2 0.1 pad_maximum_fusion.refs_1_
  38.3 0.0 collective-permute-done.refs_1_
  38.3 0.6 collective-permute-done.2.refs_4_
  38.9 0.0 collective-permute-done.4.refs_7_
  38.9 4.5 %collective-permute-done.3.refs_5_ = bf16[512,256]{1,0:T(8,128)(2,1)S(1)} collective-permute-done((bf16[512,256]{1,0:T(8,128)(2,1)S(1)}, bf16[512,256]{1,0:T(8,128)(2,1)S(1)}, u32[]{:S(2)}, u32[]{:S(2)}) %collective-permute-start.3) | collective-permute-done | bytes 262176 | tf_op jit(solution)/shard_map/ppermute | solution.py:585
  43.4 1.1 collective-permute-done.6.refs_9_
  44.5 5.5 %shard_map.165 = (bf16[544,256]{1,0:T(8,128)(2,1)}, f32[512,128]{1,0:T(8,128)}, f32[512,128]{1,0:T(8,128)}, f32[8,512]{1,0:T(8,128)}, bf16[512,128]{1,0:T(8,128)(2,1)S(1)}) custom-call(bf16[4,72,2048]{2,1,0:T(8,128)(2,1)S(1)} %all_to_all.10.refs_0_, bf16[4,72,2048]{2,1,0:T(8,128)(2,1)S(1)} %collective-permute-done.refs_1_, bf16[512,256]{1,0:T(8,128)(2,1)S(1)} %copy-done, ...), custom_call_target="tpu_custom_call" | custom-call | flops 3000000000 | bytes 1048576 | tf_op jit(solution)/shard_map/pallas_call | solution.py:67
  50.1 0.1 collective-permute-start.15
  50.2 2.6 %collective-permute-start.14 = (bf16[1024,512]{1,0:T(8,128)(2,1)S(1)}, bf16[1024,512]{1,0:T(8,128)(2,1)S(1)}, u32[]{:S(2)}, u32[]{:S(2)}) collective-permute-start(bf16[1024,512]{1,0:T(8,128)(2,1)S(1)} %pad_maximum_fusion.refs_1_), channel_id=1, source_target_pairs={{0,2},{2,4},{4,6},{6,0},{1,3},{3,5},{5,7},{7,1},{8,10},{10,12},{12... | collective-permute-start | bytes 3145736 | tf_op jit(solution)/shard_map/ppermute | solution.py:585
  52.8 0.0 collective-permute-start.7
  52.8 1.5 %collective-permute-start.11 = (bf16[544,256]{1,0:T(8,128)(2,1)}, bf16[544,256]{1,0:T(8,128)(2,1)S(1)}, u32[]{:S(2)}, u32[]{:S(2)}) collective-permute-start(bf16[544,256]{1,0:T(8,128)(2,1)} %get-tuple-element.54.refs_0_), channel_id=1, source_target_pairs={{0,224},{32,0},{64,32},{96,64},{128,96},{160,128},{192,160},{224,1... | collective-permute-start | bytes 835592 | tf_op jit(solution)/shard_map/ppermute | solution.py:585
  54.3 5.3 %collective-permute-done.7.refs_1_.refs_12_ = bf16[544,256]{1,0:T(8,128)(2,1)S(1)} collective-permute-done((bf16[544,256]{1,0:T(8,128)(2,1)}, bf16[544,256]{1,0:T(8,128)(2,1)S(1)}, u32[]{:S(2)}, u32[]{:S(2)}) %collective-permute-start.7) | collective-permute-done | bytes 278560 | tf_op jit(solution)/shard_map/ppermute | solution.py:585
  59.5 1.5 %collective-permute-start.8 = (bf16[544,256]{1,0:T(8,128)(2,1)S(1)}, bf16[544,256]{1,0:T(8,128)(2,1)S(1)}, u32[]{:S(2)}, u32[]{:S(2)}) collective-permute-start(bf16[544,256]{1,0:T(8,128)(2,1)S(1)} %collective-permute-done.7.refs_1_.refs_12_), channel_id=1, source_target_pairs={{0,32},{32,64},{64,96},{96,128},{128,160},{160,192},{192,224},{224... | collective-permute-start | bytes 835592 | tf_op jit(solution)/shard_map/ppermute | solution.py:585
  61.0 0.0 collective-permute-done.11.refs_2_.refs_7_
  61.0 0.0 collective-permute-start.12
  61.0 4.2 %collective-permute-done.8.refs_0_.refs_11_ = bf16[544,256]{1,0:T(8,128)(2,1)S(1)} collective-permute-done((bf16[544,256]{1,0:T(8,128)(2,1)S(1)}, bf16[544,256]{1,0:T(8,128)(2,1)S(1)}, u32[]{:S(2)}, u32[]{:S(2)}) %collective-permute-start.8) | collective-permute-done | bytes 278560 | tf_op jit(solution)/shard_map/ppermute | solution.py:585
  65.2 2.9 %collective-permute-start.9 = (bf16[544,256]{1,0:T(8,128)(2,1)S(1)}, bf16[544,256]{1,0:T(8,128)(2,1)S(1)}, u32[]{:S(2)}, u32[]{:S(2)}) collective-permute-start(bf16[544,256]{1,0:T(8,128)(2,1)S(1)} %collective-permute-done.8.refs_0_.refs_11_), channel_id=1, source_target_pairs={{0,32},{32,64},{64,96},{96,128},{128,160},{160,192},{192,224},{224... | collective-permute-start | bytes 835592 | tf_op jit(solution)/shard_map/ppermute | solution.py:585
  68.2 0.0 collective-permute-done.12.refs_1_.refs_8_
  68.2 0.0 collective-permute-start.13
  68.2 3.5 %collective-permute-done.9.refs_0_.refs_10_ = bf16[544,256]{1,0:T(8,128)(2,1)S(1)} collective-permute-done((bf16[544,256]{1,0:T(8,128)(2,1)S(1)}, bf16[544,256]{1,0:T(8,128)(2,1)S(1)}, u32[]{:S(2)}, u32[]{:S(2)}) %collective-permute-start.9) | collective-permute-done | bytes 278560 | tf_op jit(solution)/shard_map/ppermute | solution.py:585
  71.7 3.1 %collective-permute-start.10 = (bf16[544,256]{1,0:T(8,128)(2,1)S(1)}, bf16[544,256]{1,0:T(8,128)(2,1)S(1)}, u32[]{:S(2)}, u32[]{:S(2)}) collective-permute-start(bf16[544,256]{1,0:T(8,128)(2,1)S(1)} %collective-permute-done.9.refs_0_.refs_10_), channel_id=1, source_target_pairs={{0,32},{32,64},{64,96},{96,128},{128,160},{160,192},{192,224},{224... | collective-permute-start | bytes 835592 | tf_op jit(solution)/shard_map/ppermute | solution.py:585
  74.8 0.1 collective-permute-done.15.refs_3_
  75.0 0.1 collective-permute-start.17
  75.0 0.0 collective-permute-done.14.refs_2_
  75.1 2.7 %collective-permute-start.16 = (bf16[512,512]{1,0:T(8,128)(2,1)S(1)}, bf16[512,512]{1,0:T(8,128)(2,1)S(1)}, u32[]{:S(2)}, u32[]{:S(2)}) collective-permute-start(bf16[512,512]{1,0:T(8,128)(2,1)S(1)} %slice.8), channel_id=1, source_target_pairs={{0,2},{2,4},{4,6},{6,0},{1,3},{3,5},{5,7},{7,1},{8,10},{10,12},{12... | collective-permute-start | bytes 1572872 | tf_op jit(solution)/shard_map/ppermute | solution.py:585
  77.8 6.4 %shard_map.166 = (f32[512,128]{1,0:T(8,128)S(1)}, f32[512,128]{1,0:T(8,128)S(1)}, f32[512,128]{1,0:T(8,128)S(1)}) custom-call(bf16[544,256]{1,0:T(8,128)(2,1)} %get-tuple-element.54.refs_0_, bf16[544,256]{1,0:T(8,128)(2,1)S(1)} %collective-permute-done.7.refs_1_.refs_12_, bf16[544,256]{1,0:T(8,128)(2,1)S(1)} %collective-permute-done.11.refs_2_.refs_7_, ...), custom_call_target="tpu_custom_call" | custom-call | flops 805306368 | bytes 1048576 | tf_op jit(solution)/shard_map/pallas_call | solution.py:67
  84.3 3.7 %shard_map.167 = (f32[512,128]{1,0:T(8,128)S(1)}, f32[512,128]{1,0:T(8,128)S(1)}, f32[512,128]{1,0:T(8,128)S(1)}) custom-call(bf16[544,256]{1,0:T(8,128)(2,1)S(1)} %collective-permute-done.8.refs_0_.refs_11_, bf16[544,256]{1,0:T(8,128)(2,1)S(1)} %collective-permute-done.12.refs_1_.refs_8_, ...), custom_call_target="tpu_custom_call", output_to_operand_aliasing={{0}: (3, {}), {1}: (4, {}), {2}: (5, {})} | custom-call | flops 536870912 | bytes 1048576 | tf_op jit(solution)/shard_map/pallas_call | solution.py:67
  88.0 0.0 collective-permute-done.13.refs_1_.refs_9_
  88.0 3.9 %shard_map.168 = (f32[512,128]{1,0:T(8,128)S(1)}, f32[512,128]{1,0:T(8,128)S(1)}, f32[512,128]{1,0:T(8,128)S(1)}) custom-call(bf16[544,256]{1,0:T(8,128)(2,1)S(1)} %collective-permute-done.9.refs_0_.refs_10_, bf16[544,256]{1,0:T(8,128)(2,1)S(1)} %collective-permute-done.13.refs_1_.refs_9_, ...), custom_call_target="tpu_custom_call", output_to_operand_aliasing={{0}: (3, {}), {1}: (4, {}), {2}: (5, {})} | custom-call | flops 536870912 | bytes 1048576 | tf_op jit(solution)/shard_map/pallas_call | solution.py:67
  91.9 0.0 collective-permute-done.10.refs_0_
  91.9 3.4 %shard_map.169 = bf16[512,256]{1,0:T(8,128)(2,1)} custom-call(bf16[544,256]{1,0:T(8,128)(2,1)S(1)} %collective-permute-done.10.refs_0_, f32[512,128]{1,0:T(8,128)} %get-tuple-element.55.refs_1_, f32[512,128]{1,0:T(8,128)} %get-tuple-element.56.refs_2_, f32[256,512]{1,0:T(8,128)} %get-tuple-element.49.refs_10_.refs_3_, f32[8,512]{1,0:T(8,128)} %get-tuple-element.57.refs_4_, ...), custom_call_target="tpu_custom_call" | custom-call | flops 536870912 | bytes 1048576 | tf_op jit(solution)/shard_map/pallas_call | solution.py:67
  95.4 8.9 %all_to_all.11.refs_0_ = bf16[4,128,256]{2,1,0:T(8,128)(2,1)S(1)} all-to-all(bf16[4,128,256]{2,1,0:T(8,128)(2,1)} %bitcast.8), channel_id=1, replica_groups=mesh['z'=8,'y'=4,'x'=4,'c'=2] {'y'}, dimensions={0} | all-to-all | bytes 524288 | tf_op jit(solution)/shard_map/all_to_all | solution.py:620
  104.3 0.0 collective-permute-done.17.refs_5_
  104.3 0.0 collective-permute-done.16.refs_4_
  104.3 2.0 %shard_map.170 = (f32[64,2048]{1,0:T(8,128)}, bf16[64,2048]{1,0:T(8,128)(2,1)}) custom-call(bf16[4,128,256]{2,1,0:T(8,128)(2,1)S(1)} %all_to_all.11.refs_0_, bf16[1024,512]{1,0:T(8,128)(2,1)S(1)} %pad_maximum_fusion.refs_1_, bf16[1024,512]{1,0:T(8,128)(2,1)S(1)} %collective-permute-done.14.refs_2_, bf16[1024,512]{1,0:T(8,128)(2,1)S(1)} %collective-permute-done.15.refs_3_, ...), custom_call_target="tpu_custom_call" | custom-call | flops 536870912 | bytes 1048576 | tf_op jit(solution)/shard_map/pallas_call | solution.py:67
  106.3 6.2 %collective-permute-start.18 = (bf16[64,2048]{1,0:T(8,128)(2,1)}, bf16[64,2048]{1,0:T(8,128)(2,1)S(1)}, u32[]{:S(2)}, u32[]{:S(2)}) collective-permute-start(bf16[64,2048]{1,0:T(8,128)(2,1)} %get-tuple-element.72), channel_id=1, source_target_pairs={{0,1},{1,0},{2,3},{3,2},{4,5},{5,4},{6,7},{7,6},{8,9},{9,8},{10,11... | collective-permute-start | bytes 786440 | tf_op jit(solution)/shard_map/ppermute | solution.py:585
  112.5 1.4 %collective-permute-done.18 = bf16[64,2048]{1,0:T(8,128)(2,1)S(1)} collective-permute-done((bf16[64,2048]{1,0:T(8,128)(2,1)}, bf16[64,2048]{1,0:T(8,128)(2,1)S(1)}, u32[]{:S(2)}, u32[]{:S(2)}) %collective-permute-start.18) | collective-permute-done | bytes 262176 | tf_op jit(solution)/shard_map/ppermute | solution.py:585
  113.9 1.8 %fusion = bf16[1,64,2048]{2,1,0:T(8,128)(2,1)} fusion(f32[64,2048]{1,0:T(8,128)} %get-tuple-element.71, bf16[64,2048]{1,0:T(8,128)(2,1)S(1)} %collective-permute-done.18), kind=kLoop, calls=%fused_computation.2 | loop fusion | flops 393216 | bytes 1048576 | tf_op jit(solution)/shard_map/broadcast_in_dim | solution.py:668
  (2 shorter events, 0.1 us)
Async XLA Ops:
  2.5 21.8 %copy-start = (bf16[512,256]{1,0:T(8,128)(2,1)S(1)}, bf16[512,256]{1,0:T(8,128)(2,1)}, u32[]{:S(2)}) copy-start(bf16[512,256]{1,0:T(8,128)(2,1)} %get-tuple-element.47.refs_2_) | copy-start | bytes 786436
  2.5 22.0 %copy-start.1 = (bf16[512,256]{1,0:T(8,128)(2,1)S(1)}, bf16[512,256]{1,0:T(8,128)(2,1)}, u32[]{:S(2)}) copy-start(bf16[512,256]{1,0:T(8,128)(2,1)} %get-tuple-element.48.refs_6_) | copy-start | bytes 786436
  2.5 31.1 %copy-start.4 = (f32[32]{0:T(128)S(1)}, f32[32]{0:T(128)}, u32[]{:S(2)}) copy-start(f32[32]{0:T(128)} %param.24) | copy-start | bytes 388
  22.5 15.8 %collective-permute-start = (bf16[4,72,2048]{2,1,0:T(8,128)(2,1)S(1)}, bf16[4,72,2048]{2,1,0:T(8,128)(2,1)S(1)}, u32[]{:S(2)}, u32[]{:S(2)}) collective-permute-start(bf16[4,72,2048]{2,1,0:T(8,128)(2,1)S(1)} %all_to_all.10.refs_0_), channel_id=1, source_target_pairs={{0,1},{1,0},{2,3},{3,2},{4,5},{5,4},{6,7},{7,6},{8,9},{9,8},{10,11... | collective-permute-start | bytes 3538952 | tf_op jit(solution)/shard_map/ppermute | solution.py:585
  24.3 7.9 %collective-permute-start.1 = (bf16[512,256]{1,0:T(8,128)(2,1)S(1)}, bf16[512,256]{1,0:T(8,128)(2,1)S(1)}, u32[]{:S(2)}, u32[]{:S(2)}) collective-permute-start(bf16[512,256]{1,0:T(8,128)(2,1)S(1)} %copy-done), channel_id=1, source_target_pairs={{0,2},{2,4},{4,6},{6,0},{1,3},{3,5},{5,7},{7,1},{8,10},{10,12},{12... | collective-permute-start | bytes 786440 | tf_op jit(solution)/shard_map/ppermute | solution.py:585
  24.5 9.1 %collective-permute-start.5 = (bf16[512,256]{1,0:T(8,128)(2,1)S(1)}, bf16[512,256]{1,0:T(8,128)(2,1)S(1)}, u32[]{:S(2)}, u32[]{:S(2)}) collective-permute-start(bf16[512,256]{1,0:T(8,128)(2,1)S(1)} %copy-done.1), channel_id=1, source_target_pairs={{0,6},{2,0},{4,2},{6,4},{1,7},{3,1},{5,3},{7,5},{8,14},{10,8},{12,... | collective-permute-start | bytes 786440 | tf_op jit(solution)/shard_map/ppermute | solution.py:585
  25.7 13.1 %collective-permute-start.2 = (bf16[512,256]{1,0:T(8,128)(2,1)S(1)}, bf16[512,256]{1,0:T(8,128)(2,1)S(1)}, u32[]{:S(2)}, u32[]{:S(2)}) collective-permute-start(bf16[512,256]{1,0:T(8,128)(2,1)S(1)} %copy-done), channel_id=1, source_target_pairs={{0,6},{2,0},{4,2},{6,4},{1,7},{3,1},{5,3},{7,5},{8,14},{10,8},{12,... | collective-permute-start | bytes 786440 | tf_op jit(solution)/shard_map/ppermute | solution.py:585
  26.3 12.6 %collective-permute-start.4 = (bf16[512,256]{1,0:T(8,128)(2,1)S(1)}, bf16[512,256]{1,0:T(8,128)(2,1)S(1)}, u32[]{:S(2)}, u32[]{:S(2)}) collective-permute-start(bf16[512,256]{1,0:T(8,128)(2,1)S(1)} %copy-done.1), channel_id=1, source_target_pairs={{0,2},{2,4},{4,6},{6,0},{1,3},{3,5},{5,7},{7,1},{8,10},{10,12},{12... | collective-permute-start | bytes 786440 | tf_op jit(solution)/shard_map/ppermute | solution.py:585
  32.1 11.2 %collective-permute-start.3 = (bf16[512,256]{1,0:T(8,128)(2,1)S(1)}, bf16[512,256]{1,0:T(8,128)(2,1)S(1)}, u32[]{:S(2)}, u32[]{:S(2)}) collective-permute-start(bf16[512,256]{1,0:T(8,128)(2,1)S(1)} %collective-permute-done.1.refs_3_), channel_id=1, source_target_pairs={{0,2},{2,4},{4,6},{6,0},{1,3},{3,5},{5,7},{7,1},{8,10},{10,12},{12... | collective-permute-start | bytes 786440 | tf_op jit(solution)/shard_map/ppermute | solution.py:585
  33.5 11.0 %collective-permute-start.6 = (bf16[512,256]{1,0:T(8,128)(2,1)S(1)}, bf16[512,256]{1,0:T(8,128)(2,1)S(1)}, u32[]{:S(2)}, u32[]{:S(2)}) collective-permute-start(bf16[512,256]{1,0:T(8,128)(2,1)S(1)} %collective-permute-done.5.refs_8_), channel_id=1, source_target_pairs={{0,6},{2,0},{4,2},{6,4},{1,7},{3,1},{5,3},{7,5},{8,14},{10,8},{12,... | collective-permute-start | bytes 786440 | tf_op jit(solution)/shard_map/ppermute | solution.py:585
  34.3 3.9 %copy-start.2 = (bf16[512,512]{1,0:T(8,128)(2,1)S(1)}, bf16[512,512]{1,0:T(8,128)(2,1)}, u32[]{:S(2)}) copy-start(bf16[512,512]{1,0:T(8,128)(2,1)} %param.33) | copy-start | bytes 1572868
  34.3 3.9 %copy-start.3 = (bf16[512,512]{1,0:T(8,128)(2,1)S(1)}, bf16[512,512]{1,0:T(8,128)(2,1)}, u32[]{:S(2)}) copy-start(bf16[512,512]{1,0:T(8,128)(2,1)} %param.32) | copy-start | bytes 1572868
  50.1 24.9 %collective-permute-start.15 = (bf16[1024,512]{1,0:T(8,128)(2,1)S(1)}, bf16[1024,512]{1,0:T(8,128)(2,1)S(1)}, u32[]{:S(2)}, u32[]{:S(2)}) collective-permute-start(bf16[1024,512]{1,0:T(8,128)(2,1)S(1)} %pad_maximum_fusion.refs_1_), channel_id=1, source_target_pairs={{0,6},{2,0},{4,2},{6,4},{1,7},{3,1},{5,3},{7,5},{8,14},{10,8},{12,... | collective-permute-start | bytes 3145736 | tf_op jit(solution)/shard_map/ppermute | solution.py:585
  50.2 24.9 %collective-permute-start.14 = (bf16[1024,512]{1,0:T(8,128)(2,1)S(1)}, bf16[1024,512]{1,0:T(8,128)(2,1)S(1)}, u32[]{:S(2)}, u32[]{:S(2)}) collective-permute-start(bf16[1024,512]{1,0:T(8,128)(2,1)S(1)} %pad_maximum_fusion.refs_1_), channel_id=1, source_target_pairs={{0,2},{2,4},{4,6},{6,0},{1,3},{3,5},{5,7},{7,1},{8,10},{10,12},{12... | collective-permute-start | bytes 3145736 | tf_op jit(solution)/shard_map/ppermute | solution.py:585
  52.8 6.7 %collective-permute-start.7 = (bf16[544,256]{1,0:T(8,128)(2,1)}, bf16[544,256]{1,0:T(8,128)(2,1)S(1)}, u32[]{:S(2)}, u32[]{:S(2)}) collective-permute-start(bf16[544,256]{1,0:T(8,128)(2,1)} %get-tuple-element.54.refs_0_), channel_id=1, source_target_pairs={{0,32},{32,64},{64,96},{96,128},{128,160},{160,192},{192,224},{224... | collective-permute-start | bytes 835592 | tf_op jit(solution)/shard_map/ppermute | solution.py:585
  52.8 8.2 %collective-permute-start.11 = (bf16[544,256]{1,0:T(8,128)(2,1)}, bf16[544,256]{1,0:T(8,128)(2,1)S(1)}, u32[]{:S(2)}, u32[]{:S(2)}) collective-permute-start(bf16[544,256]{1,0:T(8,128)(2,1)} %get-tuple-element.54.refs_0_), channel_id=1, source_target_pairs={{0,224},{32,0},{64,32},{96,64},{128,96},{160,128},{192,160},{224,1... | collective-permute-start | bytes 835592 | tf_op jit(solution)/shard_map/ppermute | solution.py:585
  59.5 5.7 %collective-permute-start.8 = (bf16[544,256]{1,0:T(8,128)(2,1)S(1)}, bf16[544,256]{1,0:T(8,128)(2,1)S(1)}, u32[]{:S(2)}, u32[]{:S(2)}) collective-permute-start(bf16[544,256]{1,0:T(8,128)(2,1)S(1)} %collective-permute-done.7.refs_1_.refs_12_), channel_id=1, source_target_pairs={{0,32},{32,64},{64,96},{96,128},{128,160},{160,192},{192,224},{224... | collective-permute-start | bytes 835592 | tf_op jit(solution)/shard_map/ppermute | solution.py:585
  61.0 7.1 %collective-permute-start.12 = (bf16[544,256]{1,0:T(8,128)(2,1)S(1)}, bf16[544,256]{1,0:T(8,128)(2,1)S(1)}, u32[]{:S(2)}, u32[]{:S(2)}) collective-permute-start(bf16[544,256]{1,0:T(8,128)(2,1)S(1)} %collective-permute-done.11.refs_2_.refs_7_), channel_id=1, source_target_pairs={{0,224},{32,0},{64,32},{96,64},{128,96},{160,128},{192,160},{224,1... | collective-permute-start | bytes 835592 | tf_op jit(solution)/shard_map/ppermute | solution.py:585
  65.2 6.4 %collective-permute-start.9 = (bf16[544,256]{1,0:T(8,128)(2,1)S(1)}, bf16[544,256]{1,0:T(8,128)(2,1)S(1)}, u32[]{:S(2)}, u32[]{:S(2)}) collective-permute-start(bf16[544,256]{1,0:T(8,128)(2,1)S(1)} %collective-permute-done.8.refs_0_.refs_11_), channel_id=1, source_target_pairs={{0,32},{32,64},{64,96},{96,128},{128,160},{160,192},{192,224},{224... | collective-permute-start | bytes 835592 | tf_op jit(solution)/shard_map/ppermute | solution.py:585
  68.2 19.8 %collective-permute-start.13 = (bf16[544,256]{1,0:T(8,128)(2,1)S(1)}, bf16[544,256]{1,0:T(8,128)(2,1)S(1)}, u32[]{:S(2)}, u32[]{:S(2)}) collective-permute-start(bf16[544,256]{1,0:T(8,128)(2,1)S(1)} %collective-permute-done.12.refs_1_.refs_8_), channel_id=1, source_target_pairs={{0,224},{32,0},{64,32},{96,64},{128,96},{160,128},{192,160},{224,1... | collective-permute-start | bytes 835592 | tf_op jit(solution)/shard_map/ppermute | solution.py:585
  71.7 20.3 %collective-permute-start.10 = (bf16[544,256]{1,0:T(8,128)(2,1)S(1)}, bf16[544,256]{1,0:T(8,128)(2,1)S(1)}, u32[]{:S(2)}, u32[]{:S(2)}) collective-permute-start(bf16[544,256]{1,0:T(8,128)(2,1)S(1)} %collective-permute-done.9.refs_0_.refs_10_), channel_id=1, source_target_pairs={{0,32},{32,64},{64,96},{96,128},{128,160},{160,192},{192,224},{224... | collective-permute-start | bytes 835592 | tf_op jit(solution)/shard_map/ppermute | solution.py:585
  75.0 29.3 %collective-permute-start.17 = (bf16[512,512]{1,0:T(8,128)(2,1)S(1)}, bf16[512,512]{1,0:T(8,128)(2,1)S(1)}, u32[]{:S(2)}, u32[]{:S(2)}) collective-permute-start(bf16[512,512]{1,0:T(8,128)(2,1)S(1)} %slice.9), channel_id=1, source_target_pairs={{0,6},{2,0},{4,2},{6,4},{1,7},{3,1},{5,3},{7,5},{8,14},{10,8},{12,... | collective-permute-start | bytes 1572872 | tf_op jit(solution)/shard_map/ppermute | solution.py:585
  75.1 29.2 %collective-permute-start.16 = (bf16[512,512]{1,0:T(8,128)(2,1)S(1)}, bf16[512,512]{1,0:T(8,128)(2,1)S(1)}, u32[]{:S(2)}, u32[]{:S(2)}) collective-permute-start(bf16[512,512]{1,0:T(8,128)(2,1)S(1)} %slice.8), channel_id=1, source_target_pairs={{0,2},{2,4},{4,6},{6,0},{1,3},{3,5},{5,7},{7,1},{8,10},{10,12},{12... | collective-permute-start | bytes 1572872 | tf_op jit(solution)/shard_map/ppermute | solution.py:585
  106.3 7.6 %collective-permute-start.18 = (bf16[64,2048]{1,0:T(8,128)(2,1)}, bf16[64,2048]{1,0:T(8,128)(2,1)S(1)}, u32[]{:S(2)}, u32[]{:S(2)}) collective-permute-start(bf16[64,2048]{1,0:T(8,128)(2,1)} %get-tuple-element.72), channel_id=1, source_target_pairs={{0,1},{1,0},{2,3},{3,2},{4,5},{5,4},{6,7},{7,6},{8,9},{9,8},{10,11... | collective-permute-start | bytes 786440 | tf_op jit(solution)/shard_map/ppermute | solution.py:585

commit v2 on v1

--- a/solution.py
+++ b/solution.py
@@ -213,36 +213,14 @@
     ref[...] = jnp.zeros(ref.shape, ref.dtype)
 
 
-def attend_near(q, kv, up, down):
-    def body(ready, send, kv_ref, up_ref, down_ref, q_ref, acc_ref, fall_ref, far_ref, low_ref, *scr):
-        z = lax.axis_index("z")
+def attend_own(q, kv):
+    def body(kv_ref, q_ref, acc_ref, fall_ref, far_ref, *scr):
         zero(acc_ref)
         zero(fall_ref)
         zero(far_ref)
-        ready(0)
         chunk(q_ref, kv_ref, acc_ref, fall_ref, scr, True)
-        ready(1, 2)
-
-        @pl.when(z >= 1)
-        def _():
-            chunk(q_ref, up_ref, acc_ref, fall_ref, scr, False)
-
-        @pl.when(z >= 7)
-        def _():
-            zero(low_ref)
-            chunk(q_ref, down_ref, far_ref, low_ref, scr, False)
-
-    return staged(
-        body,
-        (),
-        [kv, up, down],
-        [pltpu.VMEM((ROWS, BLOCK), f32)] + ATTEND_SCRATCH,
-        flops=3 * ATTEND_FLOPS,
-        lazy=True,
-        free=(1, 2),
-        vin=(q,),
-        vout=PAIR + PAIR[:1],
-    )
+
+    return staged(body, (), [kv], ATTEND_SCRATCH, flops=ATTEND_FLOPS, vin=(q,), vout=PAIR + PAIR[:1])
 
 
 def attend_step(q, acc, fall, far, up, down, k):
@@ -281,8 +259,9 @@
     ):
         heads = refs[:6]
         refs = refs[6:]
-        q_ref, acc_in, fall_in, far_ref, out_ref, acc_ref, fall_ref, g_ref, head_ref, head_sem = refs[:10]
-        scr = refs[10:]
+        q_ref, acc_in, fall_in, far_ref, *parts = refs[:8]
+        out_ref, acc_ref, fall_ref, g_ref, head_ref, head_sem = refs[8:14]
+        scr = refs[14:]
         tails = [
             pltpu.make_async_copy(ref.at[pl.ds(ROWS + EXTRA, EXTRA)], head_ref.at[n], head_sem.at[n])
             for n, ref in enumerate(heads)
@@ -310,12 +289,16 @@
                 yield head_ref[n], z >= k
 
         out_ref[:, :BLOCK] = finish(chunks, y_ref, ef_ref, pow_ref, hop_ref, init_ref, ct_ref, g_ref)
+        mine = lax.axis_index("y")
+        for k, part in enumerate(parts):
+            part[...] = out_ref[pl.ds(pl.multiple_of(((mine + k) % 4) * BLOCK, BLOCK), BLOCK), :]
 
     return staged(
         body,
-        [shape((ROWS, 2 * BLOCK), bf16)],
+        [],
         [ups[4], y, ef, power, hop, init, c_map, downs[1], downs[2], downs[3], ups[3], ups[2], ups[1]],
         [
+            pltpu.VMEM((ROWS, 2 * BLOCK), bf16),
             pltpu.VMEM((ROWS, BLOCK), f32),
             pltpu.VMEM((ROWS, BLOCK), f32),
             pltpu.VMEM((ROWS, 2 * N), bf16),
@@ -328,6 +311,7 @@
         raw=range(7, 13),
         free=(0,) + tuple(range(7, 13)),
         vin=(q, acc, fall, far),
+        vout=(shape((BLOCK, 2 * BLOCK), bf16),) * 4,
     )
 
 
@@ -420,6 +404,7 @@
     c = lax.axis_index("c")
     x = lax.axis_index("x")
     copies = []
+    both = None
     for n, (step, ref) in enumerate(((0, a0), (3, a3), (1, a1), (2, a2), (0, b0), (3, b3), (1, b1), (2, b2))):
         at = pl.multiple_of(((x + step) % 4) * ROWS, ROWS)
         to = w_ref.at[pl.ds(at, ROWS), pl.ds(256 * (n // 4), 256)]
@@ -554,16 +539,17 @@
     return (0.5 * v * (1.0 + jnp.tanh(inner))).astype(bf16)
 
 
-def out_body(recv_ref, own, up, down, far0, far1, keep_ref, send_ref, lhs_ref, sum_ref):
-    x, c = lax.axis_index("x"), lax.axis_index("c")
-    for k in range(4):
-        lhs_ref[:, k * BLOCK : (k + 1) * BLOCK] = recv_ref[k, :, :BLOCK]
-        lhs_ref[:, ROWS + k * BLOCK : ROWS + (k + 1) * BLOCK] = recv_ref[k, :, BLOCK:]
-    for piece, step in ((own, 0), (up, 3), (down, 1), (None, 2)):
-        if step == 2:
-            total = mm(lhs_ref[:, :ROWS], far0[...]) + mm(lhs_ref[:, ROWS:], far1[...])
-        else:
-            total = mm(lhs_ref[...], piece[...])
+def out_body(
+    ready, send, a0, a3, a1, a2, b0, b1, b3, b2, r0, r3, r1, r2, send_ref, keep_ref, lhs_ref, sum_ref
+):
+    x, y, c = lax.axis_index("x"), lax.axis_index("y"), lax.axis_index("c")
+    for step, ref in ((0, r0), (3, r3), (1, r1), (2, r2)):
+        at = pl.multiple_of(((y + step) % 4) * BLOCK, BLOCK)
+        lhs_ref[:, pl.ds(at, BLOCK)] = ref[:, :BLOCK]
+        lhs_ref[:, pl.ds(ROWS + at, BLOCK)] = ref[:, BLOCK:]
+    ready(*range(8))
+    for step, scan_w, attend_w in ((0, a0, b0), (3, a3, b3), (1, a1, b1), (2, a2, b2)):
+        total = mm(lhs_ref[:, :ROWS], scan_w[...]) + mm(lhs_ref[:, ROWS:], attend_w[...])
         sum_ref[:, pl.ds(pl.multiple_of(((x + step) % 4) * ROWS, ROWS), ROWS)] = total
     keep_ref[...] = sum_ref[pl.ds(pl.multiple_of(c * 64, 64), 64), :]
     send_ref[...] = sum_ref[pl.ds(pl.multiple_of((1 - c) * 64, 64), 64), :].astype(bf16)
@@ -572,25 +558,20 @@
 def project_out(recv, pieces):
     return staged(
         out_body,
-        (shape((64, 2048), f32), shape((64, 2048), bf16)),
-        [recv, *pieces],
+        [shape((64, 2048), bf16)],
+        list(pieces),
         [pltpu.VMEM((BLOCK, 1024), bf16), pltpu.VMEM((BLOCK, 2048), f32)],
         flops=BLOCK * 1024 * 2048 * 2,
-        free=range(6),
+        lazy=True,
+        free=(1, 2, 3, 5, 6, 7),
+        vin=tuple(recv),
+        vout=(shape((64, 2048), f32),),
     )
 
 
 def shift(a, axis, by):
     n = lax.axis_size(axis)
     return lax.ppermute(a, axis, [(i, (i + by) % n) for i in range(n)])
-
-
-def ring4(a, axis, cut):
-    up = shift(a, axis, 1)
-    down = shift(a, axis, -1)
-    far0 = shift(up[:cut], axis, 1)
-    far1 = shift(down[cut:], axis, -1)
-    return [a, up, down, far0, far1]
 
 
 def after(a, b):
@@ -638,17 +619,17 @@
     weights = (w_a, a_up, a_down, a_far, w_b, b_up, b_down, b_far)
     mine = exchange(normed, "y")
     theirs = shift(mine, "c", 1)
+    wide = jnp.broadcast_to(log_step[:, None], lambda_real.shape)
     tables = scan_tables(
         input_map.transpose(0, 1, 3, 2),
         output_map,
         lambda_real,
         lambda_imag,
-        jnp.broadcast_to(log_step[:, None], lambda_real.shape),
+        wide,
         initial_state,
         skip_gain.reshape(1, -1),
     )
-    out_rows = jnp.concatenate([scan_out_weight, attend_out_weight], axis=0)
-    theirs, tables, out_rows = lax.optimization_barrier((theirs, tables, out_rows))
+    theirs, tables = lax.optimization_barrier((theirs, tables))
     power, inverse, b_map, c_map, init, skip = tables
     kv, y_local, ef, hop, q = project(
         mine, theirs, *weights, power, inverse, b_map, c_map, skip
@@ -658,13 +639,21 @@
         ups.append(shift(ups[-1], "z", 1))
         if k < 4:
             downs.append(shift(downs[-1], "z", -1))
-    out_pieces = ring4(after(out_rows, kv), "x", 512)
-    acc, fall, far = attend_near(q, kv, ups[1], downs[1])
-    for k in (2, 3):
+    out_pieces = []
+    for w, way in ((scan_out_weight, 1), (attend_out_weight, -1)):
+        w = after(w, kv)
+        first = shift(w, "x", way)
+        second = shift(w, "x", -way)
+        far_piece = shift(first, "x", way)
+        out_pieces += [w, first, second, far_piece]
+    acc, fall, far = attend_own(q, kv)
+    for k in (1, 2, 3):
         acc, fall, far = attend_step(q, acc, fall, far, ups[k], downs[k], k)
     both = attend_last(q, acc, fall, far, ups, downs, y_local, ef, power, hop, init, c_map)
-    recv = exchange(both.reshape(4, BLOCK, 2 * BLOCK), "y")
-    keep, send = project_out(recv, out_pieces)
+    got = [both[0]]
+    for k in (1, 3, 2):
+        got.append(shift(both[k], "y", k))
+    send, keep = project_out(got, out_pieces)
     return (keep + shift(send, "c", 1).astype(f32)).astype(bf16)[None]
 
 

time: 116 us -> 110 us (0.948)
  the two profiles are of different devices: /device:TPU:231 before, /device:TPU:225 now
where the time goes in v2:
time: 110 us
  Pallas kernels  31.6 us (29%)
  starting transfers between devices  31.2 us (28%)
  waiting for transfers between devices  25.8 us (23%)
  blocking collectives  20 us (18%)
    pallas_call x9, Pallas kernels, staged(): pl.pallas_call(kernel, out_shape=tuple((pltpu.HBM(o.shape, o.dtype) for o...  31.6 us
    ppermute x24, starting transfers between devices, shift(): return lax.ppermute(a, axis, [(i, (i + by) % n) for i in range(n)])  31.2 us
    ppermute x24, waiting for transfers between devices, shift(): return lax.ppermute(a, axis, [(i, (i + by) % n) for i in range(n)])  25.8 us
    all_to_all x1, blocking collectives, exchange(): return lax.all_to_all(a, axis, split_axis=0, concat_axis=0, tiled=True)  20 us
  transfers between devices with their start and end apart: 24, of which 10 were waited for; matrix products, arithmetic and copies ran while one was open for 1% of the time, Pallas kernels for 19%

profile of v2, /device:TPU:225, one launch (start us, length us, event | category | flops | bytes accessed | tf_op | source)
XLA Modules:
  0.0 110.2 jit_solution(3975547013505381644)
XLA Ops:
  0.0 2.5 %shard_map.163 = (bf16[4,72,2048]{2,1,0:T(8,128)(2,1)}, bf16[512,256]{1,0:T(8,128)(2,1)}, bf16[512,256]{1,0:T(8,128)(2,1)}) custom-call(bf16[1,64,2048]{2,1,0:T(8,128)(2,1)} %refs_0_.1, f32[1,2048]{1,0:T(1,128)} %bitcast.8, f32[32,128]{1,0:T(8,128)} %bitcast.7, bf16[4,128]{1,0:T(4,128)(2,1)} %bitcast.9, bf16[512,512]{1,0:T(8,128)(2,1)} %refs_4_.1, ...), custom_call_target="tpu_custom_call" | custom-call | flops 1000000 | bytes 1048576 | tf_op jit(solution)/shard_map/pallas_call | solution.py:67
  2.5 0.0 copy-start
  2.5 0.0 copy-start.4
  2.5 20.0 %all_to_all.5.refs_0_ = bf16[4,72,2048]{2,1,0:T(8,128)(2,1)S(1)} all-to-all(bf16[4,72,2048]{2,1,0:T(8,128)(2,1)} %get-tuple-element.46), channel_id=1, replica_groups=mesh['z'=8,'y'=4,'x'=4,'c'=2] {'y'}, dimensions={0} | all-to-all | bytes 2359296 | tf_op jit(solution)/shard_map/all_to_all | solution.py:601
  22.5 1.8 %collective-permute-start = (bf16[4,72,2048]{2,1,0:T(8,128)(2,1)S(1)}, bf16[4,72,2048]{2,1,0:T(8,128)(2,1)S(1)}, u32[]{:S(2)}, u32[]{:S(2)}) collective-permute-start(bf16[4,72,2048]{2,1,0:T(8,128)(2,1)S(1)} %all_to_all.5.refs_0_), channel_id=1, source_target_pairs={{0,1},{1,0},{2,3},{3,2},{4,5},{5,4},{6,7},{7,6},{8,9},{9,8},{10,11... | collective-permute-start | bytes 3538952 | tf_op jit(solution)/shard_map/ppermute | solution.py:574
  24.3 1.2 %collective-permute-start.1 = (bf16[512,256]{1,0:T(8,128)(2,1)S(1)}, bf16[512,256]{1,0:T(8,128)(2,1)S(1)}, u32[]{:S(2)}, u32[]{:S(2)}) collective-permute-start(bf16[512,256]{1,0:T(8,128)(2,1)S(1)} %copy-done), channel_id=1, source_target_pairs={{0,2},{2,4},{4,6},{6,0},{1,3},{3,5},{5,7},{7,1},{8,10},{10,12},{12... | collective-permute-start | bytes 786440 | tf_op jit(solution)/shard_map/ppermute | solution.py:574
  25.5 1.5 %collective-permute-start.5 = (bf16[512,256]{1,0:T(8,128)(2,1)S(1)}, bf16[512,256]{1,0:T(8,128)(2,1)S(1)}, u32[]{:S(2)}, u32[]{:S(2)}) collective-permute-start(bf16[512,256]{1,0:T(8,128)(2,1)S(1)} %copy-done.1), channel_id=1, source_target_pairs={{0,6},{2,0},{4,2},{6,4},{1,7},{3,1},{5,3},{7,5},{8,14},{10,8},{12,... | collective-permute-start | bytes 786440 | tf_op jit(solution)/shard_map/ppermute | solution.py:574
  27.0 1.3 %collective-permute-start.2 = (bf16[512,256]{1,0:T(8,128)(2,1)S(1)}, bf16[512,256]{1,0:T(8,128)(2,1)S(1)}, u32[]{:S(2)}, u32[]{:S(2)}) collective-permute-start(bf16[512,256]{1,0:T(8,128)(2,1)S(1)} %copy-done), channel_id=1, source_target_pairs={{0,6},{2,0},{4,2},{6,4},{1,7},{3,1},{5,3},{7,5},{8,14},{10,8},{12,... | collective-permute-start | bytes 786440 | tf_op jit(solution)/shard_map/ppermute | solution.py:574
  28.2 0.2 collective-permute-start.4
  28.4 4.9 %collective-permute-done.1.refs_3_ = bf16[512,256]{1,0:T(8,128)(2,1)S(1)} collective-permute-done((bf16[512,256]{1,0:T(8,128)(2,1)S(1)}, bf16[512,256]{1,0:T(8,128)(2,1)S(1)}, u32[]{:S(2)}, u32[]{:S(2)}) %collective-permute-start.1) | collective-permute-done | bytes 262176 | tf_op jit(solution)/shard_map/ppermute | solution.py:574
  33.4 0.0 collective-permute-start.3
  33.4 0.0 collective-permute-done.5.refs_8_
  33.4 2.7 %collective-permute-start.6 = (bf16[512,256]{1,0:T(8,128)(2,1)S(1)}, bf16[512,256]{1,0:T(8,128)(2,1)S(1)}, u32[]{:S(2)}, u32[]{:S(2)}) collective-permute-start(bf16[512,256]{1,0:T(8,128)(2,1)S(1)} %collective-permute-done.5.refs_8_), channel_id=1, source_target_pairs={{0,6},{2,0},{4,2},{6,4},{1,7},{3,1},{5,3},{7,5},{8,14},{10,8},{12,... | collective-permute-start | bytes 786440 | tf_op jit(solution)/shard_map/ppermute | solution.py:574
  36.0 0.7 broadcast_in_dim.4.refs_4_
  36.7 3.8 %shard_map.164 = (f32[256,512]{1,0:T(8,128)}, f32[256,512]{1,0:T(8,128)}, bf16[128,1024]{1,0:T(8,128)(2,1)}, bf16[128,1024]{1,0:T(8,128)(2,1)}, f32[2,512]{1,0:T(2,128)}, /*index=5*/f32[1,128]{1,0:T(1,128)}) custom-call(f32[2,32,16,64]{3,2,1,0:T(8,128)} %bitcast.10, f32[2,32,16,64]{3,2,1,0:T(8,128)} %refs_1_.1, f32[32,64]{1,0:T(8,128)} %refs_2_.1, ...), custom_call_target="tpu_custom_call" | custom-call | flops 1000000000 | bytes 1048576 | tf_op jit(solution)/shard_map/pallas_call | solution.py:67
  40.5 0.0 collective-permute-done.refs_1_
  40.5 0.0 copy-start.3
  40.5 0.0 copy-start.2
  40.6 0.0 collective-permute-done.2.refs_4_
  40.6 0.0 collective-permute-done.4.refs_7_
  40.6 4.0 %collective-permute-done.3.refs_5_ = bf16[512,256]{1,0:T(8,128)(2,1)S(1)} collective-permute-done((bf16[512,256]{1,0:T(8,128)(2,1)S(1)}, bf16[512,256]{1,0:T(8,128)(2,1)S(1)}, u32[]{:S(2)}, u32[]{:S(2)}) %collective-permute-start.3) | collective-permute-done | bytes 262176 | tf_op jit(solution)/shard_map/ppermute | solution.py:574
  44.6 0.0 collective-permute-done.6.refs_9_
  44.6 5.6 %shard_map.165 = (bf16[544,256]{1,0:T(8,128)(2,1)}, f32[512,128]{1,0:T(8,128)}, f32[512,128]{1,0:T(8,128)}, f32[8,512]{1,0:T(8,128)}, bf16[512,128]{1,0:T(8,128)(2,1)S(1)}) custom-call(bf16[4,72,2048]{2,1,0:T(8,128)(2,1)S(1)} %all_to_all.5.refs_0_, bf16[4,72,2048]{2,1,0:T(8,128)(2,1)S(1)} %collective-permute-done.refs_1_, bf16[512,256]{1,0:T(8,128)(2,1)S(1)} %copy-done, ...), custom_call_target="tpu_custom_call" | custom-call | flops 3000000000 | bytes 1048576 | tf_op jit(solution)/shard_map/pallas_call | solution.py:67
  50.2 0.1 collective-permute-start.13
  50.3 1.5 %collective-permute-start.17 = (bf16[544,256]{1,0:T(8,128)(2,1)}, bf16[544,256]{1,0:T(8,128)(2,1)S(1)}, u32[]{:S(2)}, u32[]{:S(2)}) collective-permute-start(bf16[544,256]{1,0:T(8,128)(2,1)} %get-tuple-element.61.refs_0_), channel_id=1, source_target_pairs={{0,224},{32,0},{64,32},{96,64},{128,96},{160,128},{192,160},{224,1... | collective-permute-start | bytes 835592 | tf_op jit(solution)/shard_map/ppermute | solution.py:574
  51.7 2.4 %collective-permute-start.10 = (bf16[512,512]{1,0:T(8,128)(2,1)S(1)}, bf16[512,512]{1,0:T(8,128)(2,1)S(1)}, u32[]{:S(2)}, u32[]{:S(2)}) collective-permute-start(bf16[512,512]{1,0:T(8,128)(2,1)S(1)} %copy-done.3), channel_id=1, source_target_pairs={{0,6},{2,0},{4,2},{6,4},{1,7},{3,1},{5,3},{7,5},{8,14},{10,8},{12,... | collective-permute-start | bytes 1572872 | tf_op jit(solution)/shard_map/ppermute | solution.py:574
  54.1 3.7 %collective-permute-done.13.refs_0_.refs_12_ = bf16[544,256]{1,0:T(8,128)(2,1)S(1)} collective-permute-done((bf16[544,256]{1,0:T(8,128)(2,1)}, bf16[544,256]{1,0:T(8,128)(2,1)S(1)}, u32[]{:S(2)}, u32[]{:S(2)}) %collective-permute-start.13) | collective-permute-done | bytes 278560 | tf_op jit(solution)/shard_map/ppermute | solution.py:574
  57.8 1.5 %collective-permute-start.14 = (bf16[544,256]{1,0:T(8,128)(2,1)S(1)}, bf16[544,256]{1,0:T(8,128)(2,1)S(1)}, u32[]{:S(2)}, u32[]{:S(2)}) collective-permute-start(bf16[544,256]{1,0:T(8,128)(2,1)S(1)} %collective-permute-done.13.refs_0_.refs_12_), channel_id=1, source_target_pairs={{0,32},{32,64},{64,96},{96,128},{128,160},{160,192},{192,224},{224... | collective-permute-start | bytes 835592 | tf_op jit(solution)/shard_map/ppermute | solution.py:574
  59.3 0.6 collective-permute-start.7
  60.0 0.0 collective-permute-done.17.refs_1_.refs_7_
  60.0 0.0 collective-permute-start.18
  60.0 4.4 %collective-permute-done.14.refs_0_.refs_11_ = bf16[544,256]{1,0:T(8,128)(2,1)S(1)} collective-permute-done((bf16[544,256]{1,0:T(8,128)(2,1)S(1)}, bf16[544,256]{1,0:T(8,128)(2,1)S(1)}, u32[]{:S(2)}, u32[]{:S(2)}) %collective-permute-start.14) | collective-permute-done | bytes 278560 | tf_op jit(solution)/shard_map/ppermute | solution.py:574
  64.3 3.0 %collective-permute-start.15 = (bf16[544,256]{1,0:T(8,128)(2,1)S(1)}, bf16[544,256]{1,0:T(8,128)(2,1)S(1)}, u32[]{:S(2)}, u32[]{:S(2)}) collective-permute-start(bf16[544,256]{1,0:T(8,128)(2,1)S(1)} %collective-permute-done.14.refs_0_.refs_11_), channel_id=1, source_target_pairs={{0,32},{32,64},{64,96},{96,128},{128,160},{160,192},{192,224},{224... | collective-permute-start | bytes 835592 | tf_op jit(solution)/shard_map/ppermute | solution.py:574
  67.3 0.0 collective-permute-done.18.refs_1_.refs_8_
  67.3 0.0 collective-permute-start.19
  67.3 0.7 collective-permute-start.11
  68.0 0.0 collective-permute-done.10.refs_5_
  68.0 2.0 %collective-permute-start.8 = (bf16[512,512]{1,0:T(8,128)(2,1)S(1)}, bf16[512,512]{1,0:T(8,128)(2,1)S(1)}, u32[]{:S(2)}, u32[]{:S(2)}) collective-permute-start(bf16[512,512]{1,0:T(8,128)(2,1)S(1)} %copy-done.2), channel_id=1, source_target_pairs={{0,6},{2,0},{4,2},{6,4},{1,7},{3,1},{5,3},{7,5},{8,14},{10,8},{12,... | collective-permute-start | bytes 1572872 | tf_op jit(solution)/shard_map/ppermute | solution.py:574
  70.0 2.3 %collective-permute-done.7.refs_1_ = bf16[512,512]{1,0:T(8,128)(2,1)S(1)} collective-permute-done((bf16[512,512]{1,0:T(8,128)(2,1)S(1)}, bf16[512,512]{1,0:T(8,128)(2,1)S(1)}, u32[]{:S(2)}, u32[]{:S(2)}) %collective-permute-start.7) | collective-permute-done | bytes 524320 | tf_op jit(solution)/shard_map/ppermute | solution.py:574
  72.3 0.6 collective-permute-start.12
  72.9 0.0 collective-permute-done.15.refs_0_.refs_10_
  72.9 0.9 collective-permute-start.9
  73.8 0.4 collective-permute-done.19.refs_1_.refs_9_
  74.2 0.2 collective-permute-start.16
  74.5 2.9 %shard_map.166 = (f32[512,128]{1,0:T(8,128)S(1)}, f32[512,128]{1,0:T(8,128)S(1)}, f32[512,128]{1,0:T(8,128)S(1)}) custom-call(bf16[544,256]{1,0:T(8,128)(2,1)} %get-tuple-element.61.refs_0_, bf16[512,128]{1,0:T(8,128)(2,1)S(1)} %get-tuple-element.68.refs_1_.refs_2_.refs_13_), custom_call_target="tpu_custom_call" | custom-call | flops 268435456 | bytes 1048576 | tf_op jit(solution)/shard_map/pallas_call | solution.py:67
  77.4 3.7 %shard_map.167 = (f32[512,128]{1,0:T(8,128)S(1)}, f32[512,128]{1,0:T(8,128)S(1)}, f32[512,128]{1,0:T(8,128)S(1)}) custom-call(bf16[544,256]{1,0:T(8,128)(2,1)S(1)} %collective-permute-done.13.refs_0_.refs_12_, bf16[544,256]{1,0:T(8,128)(2,1)S(1)} %collective-permute-done.17.refs_1_.refs_7_, ...), custom_call_target="tpu_custom_call", output_to_operand_aliasing={{0}: (3, {}), {1}: (4, {}), {2}: (5, {})} | custom-call | flops 536870912 | bytes 1048576 | tf_op jit(solution)/shard_map/pallas_call | solution.py:67
  81.1 3.9 %shard_map.168 = (f32[512,128]{1,0:T(8,128)S(1)}, f32[512,128]{1,0:T(8,128)S(1)}, f32[512,128]{1,0:T(8,128)S(1)}) custom-call(bf16[544,256]{1,0:T(8,128)(2,1)S(1)} %collective-permute-done.14.refs_0_.refs_11_, bf16[544,256]{1,0:T(8,128)(2,1)S(1)} %collective-permute-done.18.refs_1_.refs_8_, ...), custom_call_target="tpu_custom_call", output_to_operand_aliasing={{0}: (3, {}), {1}: (4, {}), {2}: (5, {})} | custom-call | flops 536870912 | bytes 1048576 | tf_op jit(solution)/shard_map/pallas_call | solution.py:67
  85.0 3.7 %shard_map.169 = (f32[512,128]{1,0:T(8,128)S(1)}, f32[512,128]{1,0:T(8,128)S(1)}, f32[512,128]{1,0:T(8,128)S(1)}) custom-call(bf16[544,256]{1,0:T(8,128)(2,1)S(1)} %collective-permute-done.15.refs_0_.refs_10_, bf16[544,256]{1,0:T(8,128)(2,1)S(1)} %collective-permute-done.19.refs_1_.refs_9_, ...), custom_call_target="tpu_custom_call", output_to_operand_aliasing={{0}: (3, {}), {1}: (4, {}), {2}: (5, {})} | custom-call | flops 536870912 | bytes 1048576 | tf_op jit(solution)/shard_map/pallas_call | solution.py:67
  88.7 0.0 collective-permute-done.16.refs_0_
  88.7 2.7 %shard_map.170 = (bf16[128,256]{1,0:T(8,128)(2,1)S(1)}, bf16[128,256]{1,0:T(8,128)(2,1)S(1)}, bf16[128,256]{1,0:T(8,128)(2,1)S(1)}, bf16[128,256]{1,0:T(8,128)(2,1)S(1)}) custom-call(bf16[544,256]{1,0:T(8,128)(2,1)S(1)} %collective-permute-done.16.refs_0_, f32[512,128]{1,0:T(8,128)} %get-tuple-element.64.refs_1_, f32[512,128]{1,0:T(8,128)} %get-tuple-element.65.refs_2_, ...), custom_call_target="tpu_custom_call" | custom-call | flops 536870912 | bytes 1048576 | tf_op jit(solution)/shard_map/pallas_call | solution.py:67
  91.5 0.3 collective-permute-start.20
  91.8 0.0 collective-permute-done.11.refs_6_
  91.8 2.4 %collective-permute-start.21 = (bf16[128,256]{1,0:T(8,128)(2,1)S(1)}, bf16[128,256]{1,0:T(8,128)(2,1)S(1)}, u32[]{:S(2)}, u32[]{:S(2)}) collective-permute-start(bf16[128,256]{1,0:T(8,128)(2,1)S(1)} %get-tuple-element.83), channel_id=1, source_target_pairs={{0,24},{8,0},{16,8},{24,16},{1,25},{9,1},{17,9},{25,17},{2,26},{10... | collective-permute-start | bytes 196616 | tf_op jit(solution)/shard_map/ppermute | solution.py:574
  94.2 0.0 collective-permute-done.8.refs_2_
  94.2 0.0 collective-permute-start.22
  94.2 0.0 collective-permute-done.12.refs_7_
  94.2 0.5 collective-permute-done.9.refs_3_
  94.8 1.4 %collective-permute-done.20.refs_9_ = bf16[128,256]{1,0:T(8,128)(2,1)S(1)} collective-permute-done((bf16[128,256]{1,0:T(8,128)(2,1)S(1)}, bf16[128,256]{1,0:T(8,128)(2,1)S(1)}, u32[]{:S(2)}, u32[]{:S(2)}) %collective-permute-start.20) | collective-permute-done | bytes 65568 | tf_op jit(solution)/shard_map/ppermute | solution.py:574
  96.2 0.0 collective-permute-done.21.refs_10_
  96.2 2.7 %collective-permute-done.22.refs_11_ = bf16[128,256]{1,0:T(8,128)(2,1)S(1)} collective-permute-done((bf16[128,256]{1,0:T(8,128)(2,1)S(1)}, bf16[128,256]{1,0:T(8,128)(2,1)S(1)}, u32[]{:S(2)}, u32[]{:S(2)}) %collective-permute-start.22) | collective-permute-done | bytes 65568 | tf_op jit(solution)/shard_map/ppermute | solution.py:574
  98.8 2.8 %shard_map.171 = (bf16[64,2048]{1,0:T(8,128)(2,1)}, f32[64,2048]{1,0:T(8,128)S(1)}) custom-call(bf16[512,512]{1,0:T(8,128)(2,1)} %refs_0_.2, bf16[512,512]{1,0:T(8,128)(2,1)S(1)} %collective-permute-done.7.refs_1_, bf16[512,512]{1,0:T(8,128)(2,1)S(1)} %collective-permute-done.8.refs_2_, bf16[512,512]{1,0:T(8,128)(2,1)S(1)} %collective-permute-done.9.refs_3_, ...), custom_call_target="tpu_custom_call" | custom-call | flops 536870912 | bytes 1048576 | tf_op jit(solution)/shard_map/pallas_call | solution.py:67
  101.6 6.4 %collective-permute-start.23 = (bf16[64,2048]{1,0:T(8,128)(2,1)}, bf16[64,2048]{1,0:T(8,128)(2,1)S(1)}, u32[]{:S(2)}, u32[]{:S(2)}) collective-permute-start(bf16[64,2048]{1,0:T(8,128)(2,1)} %get-tuple-element.86), channel_id=1, source_target_pairs={{0,1},{1,0},{2,3},{3,2},{4,5},{5,4},{6,7},{7,6},{8,9},{9,8},{10,11... | collective-permute-start | bytes 786440 | tf_op jit(solution)/shard_map/ppermute | solution.py:574
  108.0 1.4 %collective-permute-done.23 = bf16[64,2048]{1,0:T(8,128)(2,1)S(1)} collective-permute-done((bf16[64,2048]{1,0:T(8,128)(2,1)}, bf16[64,2048]{1,0:T(8,128)(2,1)S(1)}, u32[]{:S(2)}, u32[]{:S(2)}) %collective-permute-start.23) | collective-permute-done | bytes 262176 | tf_op jit(solution)/shard_map/ppermute | solution.py:574
  109.4 0.8 fusion
  (6 shorter events, 0.0 us)
Async XLA Ops:
  2.5 21.8 %copy-start = (bf16[512,256]{1,0:T(8,128)(2,1)S(1)}, bf16[512,256]{1,0:T(8,128)(2,1)}, u32[]{:S(2)}) copy-start(bf16[512,256]{1,0:T(8,128)(2,1)} %get-tuple-element.54.refs_2_) | copy-start | bytes 786436
  2.5 23.0 %copy-start.1 = (bf16[512,256]{1,0:T(8,128)(2,1)S(1)}, bf16[512,256]{1,0:T(8,128)(2,1)}, u32[]{:S(2)}) copy-start(bf16[512,256]{1,0:T(8,128)(2,1)} %get-tuple-element.55.refs_6_) | copy-start | bytes 786436
  2.5 33.6 %copy-start.4 = (f32[32]{0:T(128)S(1)}, f32[32]{0:T(128)}, u32[]{:S(2)}) copy-start(f32[32]{0:T(128)} %param.24) | copy-start | bytes 388
  22.5 18.1 %collective-permute-start = (bf16[4,72,2048]{2,1,0:T(8,128)(2,1)S(1)}, bf16[4,72,2048]{2,1,0:T(8,128)(2,1)S(1)}, u32[]{:S(2)}, u32[]{:S(2)}) collective-permute-start(bf16[4,72,2048]{2,1,0:T(8,128)(2,1)S(1)} %all_to_all.5.refs_0_), channel_id=1, source_target_pairs={{0,1},{1,0},{2,3},{3,2},{4,5},{5,4},{6,7},{7,6},{8,9},{9,8},{10,11... | collective-permute-start | bytes 3538952 | tf_op jit(solution)/shard_map/ppermute | solution.py:574
  24.3 9.1 %collective-permute-start.1 = (bf16[512,256]{1,0:T(8,128)(2,1)S(1)}, bf16[512,256]{1,0:T(8,128)(2,1)S(1)}, u32[]{:S(2)}, u32[]{:S(2)}) collective-permute-start(bf16[512,256]{1,0:T(8,128)(2,1)S(1)} %copy-done), channel_id=1, source_target_pairs={{0,2},{2,4},{4,6},{6,0},{1,3},{3,5},{5,7},{7,1},{8,10},{10,12},{12... | collective-permute-start | bytes 786440 | tf_op jit(solution)/shard_map/ppermute | solution.py:574
  25.5 7.9 %collective-permute-start.5 = (bf16[512,256]{1,0:T(8,128)(2,1)S(1)}, bf16[512,256]{1,0:T(8,128)(2,1)S(1)}, u32[]{:S(2)}, u32[]{:S(2)}) collective-permute-start(bf16[512,256]{1,0:T(8,128)(2,1)S(1)} %copy-done.1), channel_id=1, source_target_pairs={{0,6},{2,0},{4,2},{6,4},{1,7},{3,1},{5,3},{7,5},{8,14},{10,8},{12,... | collective-permute-start | bytes 786440 | tf_op jit(solution)/shard_map/ppermute | solution.py:574
  27.0 13.6 %collective-permute-start.2 = (bf16[512,256]{1,0:T(8,128)(2,1)S(1)}, bf16[512,256]{1,0:T(8,128)(2,1)S(1)}, u32[]{:S(2)}, u32[]{:S(2)}) collective-permute-start(bf16[512,256]{1,0:T(8,128)(2,1)S(1)} %copy-done), channel_id=1, source_target_pairs={{0,6},{2,0},{4,2},{6,4},{1,7},{3,1},{5,3},{7,5},{8,14},{10,8},{12,... | collective-permute-start | bytes 786440 | tf_op jit(solution)/shard_map/ppermute | solution.py:574
  28.2 12.3 %collective-permute-start.4 = (bf16[512,256]{1,0:T(8,128)(2,1)S(1)}, bf16[512,256]{1,0:T(8,128)(2,1)S(1)}, u32[]{:S(2)}, u32[]{:S(2)}) collective-permute-start(bf16[512,256]{1,0:T(8,128)(2,1)S(1)} %copy-done.1), channel_id=1, source_target_pairs={{0,2},{2,4},{4,6},{6,0},{1,3},{3,5},{5,7},{7,1},{8,10},{10,12},{12... | collective-permute-start | bytes 786440 | tf_op jit(solution)/shard_map/ppermute | solution.py:574
  33.4 11.2 %collective-permute-start.3 = (bf16[512,256]{1,0:T(8,128)(2,1)S(1)}, bf16[512,256]{1,0:T(8,128)(2,1)S(1)}, u32[]{:S(2)}, u32[]{:S(2)}) collective-permute-start(bf16[512,256]{1,0:T(8,128)(2,1)S(1)} %collective-permute-done.1.refs_3_), channel_id=1, source_target_pairs={{0,2},{2,4},{4,6},{6,0},{1,3},{3,5},{5,7},{7,1},{8,10},{10,12},{12... | collective-permute-start | bytes 786440 | tf_op jit(solution)/shard_map/ppermute | solution.py:574
  33.4 11.2 %collective-permute-start.6 = (bf16[512,256]{1,0:T(8,128)(2,1)S(1)}, bf16[512,256]{1,0:T(8,128)(2,1)S(1)}, u32[]{:S(2)}, u32[]{:S(2)}) collective-permute-start(bf16[512,256]{1,0:T(8,128)(2,1)S(1)} %collective-permute-done.5.refs_8_), channel_id=1, source_target_pairs={{0,6},{2,0},{4,2},{6,4},{1,7},{3,1},{5,3},{7,5},{8,14},{10,8},{12,... | collective-permute-start | bytes 786440 | tf_op jit(solution)/shard_map/ppermute | solution.py:574
  40.5 11.2 %copy-start.3 = (bf16[512,512]{1,0:T(8,128)(2,1)S(1)}, bf16[512,512]{1,0:T(8,128)(2,1)}, u32[]{:S(2)}) copy-start(bf16[512,512]{1,0:T(8,128)(2,1)} %refs_4_.2) | copy-start | bytes 1572868
  40.5 18.8 %copy-start.2 = (bf16[512,512]{1,0:T(8,128)(2,1)S(1)}, bf16[512,512]{1,0:T(8,128)(2,1)}, u32[]{:S(2)}) copy-start(bf16[512,512]{1,0:T(8,128)(2,1)} %refs_0_.2) | copy-start | bytes 1572868
  50.2 7.7 %collective-permute-start.13 = (bf16[544,256]{1,0:T(8,128)(2,1)}, bf16[544,256]{1,0:T(8,128)(2,1)S(1)}, u32[]{:S(2)}, u32[]{:S(2)}) collective-permute-start(bf16[544,256]{1,0:T(8,128)(2,1)} %get-tuple-element.61.refs_0_), channel_id=1, source_target_pairs={{0,32},{32,64},{64,96},{96,128},{128,160},{160,192},{192,224},{224... | collective-permute-start | bytes 835592 | tf_op jit(solution)/shard_map/ppermute | solution.py:574
  50.3 9.7 %collective-permute-start.17 = (bf16[544,256]{1,0:T(8,128)(2,1)}, bf16[544,256]{1,0:T(8,128)(2,1)S(1)}, u32[]{:S(2)}, u32[]{:S(2)}) collective-permute-start(bf16[544,256]{1,0:T(8,128)(2,1)} %get-tuple-element.61.refs_0_), channel_id=1, source_target_pairs={{0,224},{32,0},{64,32},{96,64},{128,96},{160,128},{192,160},{224,1... | collective-permute-start | bytes 835592 | tf_op jit(solution)/shard_map/ppermute | solution.py:574
  51.7 16.3 %collective-permute-start.10 = (bf16[512,512]{1,0:T(8,128)(2,1)S(1)}, bf16[512,512]{1,0:T(8,128)(2,1)S(1)}, u32[]{:S(2)}, u32[]{:S(2)}) collective-permute-start(bf16[512,512]{1,0:T(8,128)(2,1)S(1)} %copy-done.3), channel_id=1, source_target_pairs={{0,6},{2,0},{4,2},{6,4},{1,7},{3,1},{5,3},{7,5},{8,14},{10,8},{12,... | collective-permute-start | bytes 1572872 | tf_op jit(solution)/shard_map/ppermute | solution.py:574
  57.8 6.5 %collective-permute-start.14 = (bf16[544,256]{1,0:T(8,128)(2,1)S(1)}, bf16[544,256]{1,0:T(8,128)(2,1)S(1)}, u32[]{:S(2)}, u32[]{:S(2)}) collective-permute-start(bf16[544,256]{1,0:T(8,128)(2,1)S(1)} %collective-permute-done.13.refs_0_.refs_12_), channel_id=1, source_target_pairs={{0,32},{32,64},{64,96},{96,128},{128,160},{160,192},{192,224},{224... | collective-permute-start | bytes 835592 | tf_op jit(solution)/shard_map/ppermute | solution.py:574
  59.3 13.0 %collective-permute-start.7 = (bf16[512,512]{1,0:T(8,128)(2,1)S(1)}, bf16[512,512]{1,0:T(8,128)(2,1)S(1)}, u32[]{:S(2)}, u32[]{:S(2)}) collective-permute-start(bf16[512,512]{1,0:T(8,128)(2,1)S(1)} %copy-done.2), channel_id=1, source_target_pairs={{0,2},{2,4},{4,6},{6,0},{1,3},{3,5},{5,7},{7,1},{8,10},{10,12},{12... | collective-permute-start | bytes 1572872 | tf_op jit(solution)/shard_map/ppermute | solution.py:574
  60.0 7.4 %collective-permute-start.18 = (bf16[544,256]{1,0:T(8,128)(2,1)S(1)}, bf16[544,256]{1,0:T(8,128)(2,1)S(1)}, u32[]{:S(2)}, u32[]{:S(2)}) collective-permute-start(bf16[544,256]{1,0:T(8,128)(2,1)S(1)} %collective-permute-done.17.refs_1_.refs_7_), channel_id=1, source_target_pairs={{0,224},{32,0},{64,32},{96,64},{128,96},{160,128},{192,160},{224,1... | collective-permute-start | bytes 835592 | tf_op jit(solution)/shard_map/ppermute | solution.py:574
  64.3 8.6 %collective-permute-start.15 = (bf16[544,256]{1,0:T(8,128)(2,1)S(1)}, bf16[544,256]{1,0:T(8,128)(2,1)S(1)}, u32[]{:S(2)}, u32[]{:S(2)}) collective-permute-start(bf16[544,256]{1,0:T(8,128)(2,1)S(1)} %collective-permute-done.14.refs_0_.refs_11_), channel_id=1, source_target_pairs={{0,32},{32,64},{64,96},{96,128},{128,160},{160,192},{192,224},{224... | collective-permute-start | bytes 835592 | tf_op jit(solution)/shard_map/ppermute | solution.py:574
  67.3 6.9 %collective-permute-start.19 = (bf16[544,256]{1,0:T(8,128)(2,1)S(1)}, bf16[544,256]{1,0:T(8,128)(2,1)S(1)}, u32[]{:S(2)}, u32[]{:S(2)}) collective-permute-start(bf16[544,256]{1,0:T(8,128)(2,1)S(1)} %collective-permute-done.18.refs_1_.refs_8_), channel_id=1, source_target_pairs={{0,224},{32,0},{64,32},{96,64},{128,96},{160,128},{192,160},{224,1... | collective-permute-start | bytes 835592 | tf_op jit(solution)/shard_map/ppermute | solution.py:574
  67.3 24.5 %collective-permute-start.11 = (bf16[512,512]{1,0:T(8,128)(2,1)S(1)}, bf16[512,512]{1,0:T(8,128)(2,1)S(1)}, u32[]{:S(2)}, u32[]{:S(2)}) collective-permute-start(bf16[512,512]{1,0:T(8,128)(2,1)S(1)} %copy-done.3), channel_id=1, source_target_pairs={{0,2},{2,4},{4,6},{6,0},{1,3},{3,5},{5,7},{7,1},{8,10},{10,12},{12... | collective-permute-start | bytes 1572872 | tf_op jit(solution)/shard_map/ppermute | solution.py:574
  68.0 26.2 %collective-permute-start.8 = (bf16[512,512]{1,0:T(8,128)(2,1)S(1)}, bf16[512,512]{1,0:T(8,128)(2,1)S(1)}, u32[]{:S(2)}, u32[]{:S(2)}) collective-permute-start(bf16[512,512]{1,0:T(8,128)(2,1)S(1)} %copy-done.2), channel_id=1, source_target_pairs={{0,6},{2,0},{4,2},{6,4},{1,7},{3,1},{5,3},{7,5},{8,14},{10,8},{12,... | collective-permute-start | bytes 1572872 | tf_op jit(solution)/shard_map/ppermute | solution.py:574
  72.3 21.9 %collective-permute-start.12 = (bf16[512,512]{1,0:T(8,128)(2,1)S(1)}, bf16[512,512]{1,0:T(8,128)(2,1)S(1)}, u32[]{:S(2)}, u32[]{:S(2)}) collective-permute-start(bf16[512,512]{1,0:T(8,128)(2,1)S(1)} %collective-permute-done.10.refs_5_), channel_id=1, source_target_pairs={{0,6},{2,0},{4,2},{6,4},{1,7},{3,1},{5,3},{7,5},{8,14},{10,8},{12,... | collective-permute-start | bytes 1572872 | tf_op jit(solution)/shard_map/ppermute | solution.py:574
  72.9 21.9 %collective-permute-start.9 = (bf16[512,512]{1,0:T(8,128)(2,1)S(1)}, bf16[512,512]{1,0:T(8,128)(2,1)S(1)}, u32[]{:S(2)}, u32[]{:S(2)}) collective-permute-start(bf16[512,512]{1,0:T(8,128)(2,1)S(1)} %collective-permute-done.7.refs_1_), channel_id=1, source_target_pairs={{0,2},{2,4},{4,6},{6,0},{1,3},{3,5},{5,7},{7,1},{8,10},{10,12},{12... | collective-permute-start | bytes 1572872 | tf_op jit(solution)/shard_map/ppermute | solution.py:574
  74.2 14.5 %collective-permute-start.16 = (bf16[544,256]{1,0:T(8,128)(2,1)S(1)}, bf16[544,256]{1,0:T(8,128)(2,1)S(1)}, u32[]{:S(2)}, u32[]{:S(2)}) collective-permute-start(bf16[544,256]{1,0:T(8,128)(2,1)S(1)} %collective-permute-done.15.refs_0_.refs_10_), channel_id=1, source_target_pairs={{0,32},{32,64},{64,96},{96,128},{128,160},{160,192},{192,224},{224... | collective-permute-start | bytes 835592 | tf_op jit(solution)/shard_map/ppermute | solution.py:574
  91.5 4.7 %collective-permute-start.20 = (bf16[128,256]{1,0:T(8,128)(2,1)S(1)}, bf16[128,256]{1,0:T(8,128)(2,1)S(1)}, u32[]{:S(2)}, u32[]{:S(2)}) collective-permute-start(bf16[128,256]{1,0:T(8,128)(2,1)S(1)} %get-tuple-element.82), channel_id=1, source_target_pairs={{0,8},{8,16},{16,24},{24,0},{1,9},{9,17},{17,25},{25,1},{2,10},{10... | collective-permute-start | bytes 196616 | tf_op jit(solution)/shard_map/ppermute | solution.py:574
  91.8 4.4 %collective-permute-start.21 = (bf16[128,256]{1,0:T(8,128)(2,1)S(1)}, bf16[128,256]{1,0:T(8,128)(2,1)S(1)}, u32[]{:S(2)}, u32[]{:S(2)}) collective-permute-start(bf16[128,256]{1,0:T(8,128)(2,1)S(1)} %get-tuple-element.83), channel_id=1, source_target_pairs={{0,24},{8,0},{16,8},{24,16},{1,25},{9,1},{17,9},{25,17},{2,26},{10... | collective-permute-start | bytes 196616 | tf_op jit(solution)/shard_map/ppermute | solution.py:574
  94.2 4.6 %collective-permute-start.22 = (bf16[128,256]{1,0:T(8,128)(2,1)S(1)}, bf16[128,256]{1,0:T(8,128)(2,1)S(1)}, u32[]{:S(2)}, u32[]{:S(2)}) collective-permute-start(bf16[128,256]{1,0:T(8,128)(2,1)S(1)} %get-tuple-element.84), channel_id=1, source_target_pairs={{0,16},{8,24},{16,0},{24,8},{1,17},{9,25},{17,1},{25,9},{2,18},{10... | collective-permute-start | bytes 196616 | tf_op jit(solution)/shard_map/ppermute | solution.py:574
  101.6 7.8 %collective-permute-start.23 = (bf16[64,2048]{1,0:T(8,128)(2,1)}, bf16[64,2048]{1,0:T(8,128)(2,1)S(1)}, u32[]{:S(2)}, u32[]{:S(2)}) collective-permute-start(bf16[64,2048]{1,0:T(8,128)(2,1)} %get-tuple-element.86), channel_id=1, source_target_pairs={{0,1},{1,0},{2,3},{3,2},{4,5},{5,4},{6,7},{7,6},{8,9},{9,8},{10,11... | collective-permute-start | bytes 786440 | tf_op jit(solution)/shard_map/ppermute | solution.py:574

commit v3 on v2

--- a/solution.py
+++ b/solution.py
@@ -399,12 +399,11 @@
 def project_body(
     ready, send, mine, theirs, a0, a3, a1, a2, b0, b3, b1, b2, pow_ref, inv_ref, b_ref, ct_ref, skip_ref,
     kv_ref, y_ref, ef_ref, hop_ref, q_ref,
-    rows, sems, more, u_ref, f_ref, x_ref, st_ref, w_ref,
+    rows, sems, more, u_ref, x_ref, st_ref, w_ref,
 ):
     c = lax.axis_index("c")
     x = lax.axis_index("x")
     copies = []
-    both = None
     for n, (step, ref) in enumerate(((0, a0), (3, a3), (1, a1), (2, a2), (0, b0), (3, b3), (1, b1), (2, b2))):
         at = pl.multiple_of(((x + step) % 4) * ROWS, ROWS)
         to = w_ref.at[pl.ds(at, ROWS), pl.ds(256 * (n // 4), 256)]
@@ -419,26 +418,15 @@
         copies.append(
             pltpu.make_async_copy(mine.at[b, pl.ds(64, MORE)], more.at[b], sems.at[8 + b])
         )
-    for copy in copies:
+    for copy in copies[-4:] + copies[:-4]:
         copy.start()
-    for copy in copies:
+    for copy in copies[-4:]:
         copy.wait()
-    both = mm(rows[...], w_ref[...])
-    kv_ref[:ROWS, :] = both[:, :256].astype(bf16)
-    q_ref[...] = both[:, 256:384].astype(bf16)
-    u_ref[...] = both[:, 384:].astype(bf16)
     offs = [more[b].astype(f32)[1:2, :BLOCK] for b in range(4)]
     row0 = jnp.concatenate(offs[:2], axis=1)
     row1 = jnp.concatenate(offs[2:], axis=1)
     tail = jnp.concatenate([row0, row1, jnp.zeros((EXTRA - 2, 256), f32)], axis=0)
     kv_ref[ROWS : ROWS + EXTRA, :] = tail.astype(bf16)
-    for b in range(4):
-        part = more[b].astype(f32)
-        part = part[0:1, : 8 * BLOCK] + part[0:1, 8 * BLOCK :]
-        f_ref[:, b * BLOCK : (b + 1) * BLOCK] = jnp.concatenate(
-            [part[:, g * BLOCK : (g + 1) * BLOCK] for g in range(8)], axis=0
-        )
-    ready(10, 11, 12, 13, 14)
     row = lax.broadcasted_iota(jnp.int32, (BLOCK, BLOCK), 0)
     col = lax.broadcasted_iota(jnp.int32, (BLOCK, BLOCK), 1)
     low = (col <= row).astype(bf16)
@@ -446,14 +434,16 @@
     even = lax.broadcasted_iota(jnp.int32, (1, BLOCK), 1) < 64
     keeps = []
     blocks = [slice(b * BLOCK, (b + 1) * BLOCK) for b in range(4)]
-    for at in blocks:
-        f = f_ref[:, at]
+    for b, at in enumerate(blocks):
+        part = more[b].astype(f32)
+        part = part[0:1, : 8 * BLOCK] + part[0:1, 8 * BLOCK :]
+        f = jnp.concatenate([part[:, g * BLOCK : (g + 1) * BLOCK] for g in range(8)], axis=0)
         f_all = jnp.concatenate([jnp.broadcast_to(f[g : g + 1], (16, BLOCK)) for g in range(8)], axis=0)
         cum_f = lax.dot_general(
             low32, f_all, (((1,), (1,)), ((), ())), precision=lax.Precision.HIGHEST, preferred_element_type=f32
         )
         ef_ref[at, :] = jnp.exp(cum_f)
-        x_ref[at, :BLOCK] = u_ref[at, :].astype(f32) * jnp.exp(-cum_f)
+        x_ref[at, :BLOCK] = jnp.exp(-cum_f)
         total = jnp.exp(jnp.broadcast_to(jnp.sum(f, axis=1, keepdims=True), (8, BLOCK)))
         keeps.append(
             jnp.concatenate(
@@ -461,6 +451,14 @@
                 axis=1,
             )
         )
+    for copy in copies[:-4]:
+        copy.wait()
+    both = mm(rows[...], w_ref[...])
+    kv_ref[:ROWS, :] = both[:, :256].astype(bf16)
+    q_ref[...] = both[:, 256:384].astype(bf16)
+    u_ref[...] = both[:, 384:].astype(bf16)
+    x_ref[:, :BLOCK] = x_ref[:, :BLOCK] * u_ref[...].astype(f32)
+    ready(10, 11, 12, 13, 14)
     x_ref[...] = mm(x_ref[:, :BLOCK].astype(bf16), b_ref[...])
     carry_r = jnp.zeros((1, N), f32)
     carry_i = jnp.zeros((1, N), f32)
@@ -504,7 +502,6 @@
             pltpu.SemaphoreType.DMA((20,)),
             pltpu.VMEM((4, MORE, 2048), bf16),
             pltpu.VMEM((ROWS, BLOCK), bf16),
-            pltpu.VMEM((8, ROWS), f32),
             pltpu.VMEM((ROWS, 2 * N), f32),
             pltpu.VMEM((ROWS, 2 * N), bf16),
             pltpu.VMEM((2048, ROWS), bf16),
@@ -540,14 +537,13 @@
 
 
 def out_body(
-    ready, send, a0, a3, a1, a2, b0, b1, b3, b2, r0, r3, r1, r2, send_ref, keep_ref, lhs_ref, sum_ref
+    a0, a3, a1, a2, b0, b1, b3, b2, r0, r3, r1, r2, send_ref, keep_ref, lhs_ref, sum_ref
 ):
     x, y, c = lax.axis_index("x"), lax.axis_index("y"), lax.axis_index("c")
     for step, ref in ((0, r0), (3, r3), (1, r1), (2, r2)):
         at = pl.multiple_of(((y + step) % 4) * BLOCK, BLOCK)
         lhs_ref[:, pl.ds(at, BLOCK)] = ref[:, :BLOCK]
         lhs_ref[:, pl.ds(ROWS + at, BLOCK)] = ref[:, BLOCK:]
-    ready(*range(8))
     for step, scan_w, attend_w in ((0, a0, b0), (3, a3, b3), (1, a1, b1), (2, a2, b2)):
         total = mm(lhs_ref[:, :ROWS], scan_w[...]) + mm(lhs_ref[:, ROWS:], attend_w[...])
         sum_ref[:, pl.ds(pl.multiple_of(((x + step) % 4) * ROWS, ROWS), ROWS)] = total
@@ -559,12 +555,10 @@
     return staged(
         out_body,
         [shape((64, 2048), bf16)],
-        list(pieces),
+        [],
         [pltpu.VMEM((BLOCK, 1024), bf16), pltpu.VMEM((BLOCK, 2048), f32)],
         flops=BLOCK * 1024 * 2048 * 2,
-        lazy=True,
-        free=(1, 2, 3, 5, 6, 7),
-        vin=tuple(recv),
+        vin=tuple(pieces) + tuple(recv),
         vout=(shape((64, 2048), f32),),
     )
 
@@ -636,9 +630,9 @@
     )
     ups, downs = [kv], [kv]
     for k in range(1, 5):
-        ups.append(shift(ups[-1], "z", 1))
+        ups.append(lax.ppermute(ups[-1], "z", [(i, i + 1) for i in range(k - 1, 7)]))
         if k < 4:
-            downs.append(shift(downs[-1], "z", -1))
+            downs.append(lax.ppermute(downs[-1], "z", [((j - k + 1) % 8, (j - k) % 8) for j in range(3)]))
     out_pieces = []
     for w, way in ((scan_out_weight, 1), (attend_out_weight, -1)):
         w = after(w, kv)

time: 110 us -> 116 us (1.055)
  starting transfers between devices: 31.2 us -> 37 us
  Pallas kernels: 31.6 us -> 30.2 us
    ppermute x0 -> x7, starting transfers between devices: none -> 12 us  [the longest x3 6.87 us: on_device(): lax.ppermute(downs[-1], 'z', [((j - k + 1) % 8, (j - k) % 8) for j in ran...]
    ppermute x0 -> x7, waiting for transfers between devices: none -> 11.4 us  [the longest x4 6.59 us: on_device(): lax.ppermute(ups[-1], 'z', [(i, i + 1) for i in range(k - 1, 7)])]
    ppermute x24 -> x17, waiting for transfers between devices: 25.8 us -> 14.9 us  [shift(): return lax.ppermute(a, axis, [(i, (i + by) % n) for i in range(n)])]
    ppermute x24 -> x17, starting transfers between devices: 31.2 us -> 25 us  [shift(): return lax.ppermute(a, axis, [(i, (i + by) % n) for i in range(n)])]
    pallas_call x9, Pallas kernels: 31.6 us -> 30.2 us  [staged(): pl.pallas_call(kernel, out_shape=tuple((pltpu.HBM(o.shape, o.dtype) for o...]
  transfers between devices with their start and end apart: 24 -> 24, of which waited for: 10 -> 11; matrix products, arithmetic and copies ran while one was open for 1% -> 1% of each run, Pallas kernels for 19% -> 18%
where the time goes in v3:
time: 116 us; the launch traced here: 115 us
  starting transfers between devices  37 us (32%)
  Pallas kernels  30.2 us (26%)
  waiting for transfers between devices  26.4 us (23%)
  blocking collectives  20 us (17%)
    pallas_call x9, Pallas kernels, staged(): pl.pallas_call(kernel, out_shape=tuple((pltpu.HBM(o.shape, o.dtype) for o...  30.2 us
    ppermute x17, starting transfers between devices, shift(): return lax.ppermute(a, axis, [(i, (i + by) % n) for i in range(n)])  25 us
    all_to_all x1, blocking collectives, exchange(): return lax.all_to_all(a, axis, split_axis=0, concat_axis=0, tiled=True)  20 us
    ppermute x17, waiting for transfers between devices, shift(): return lax.ppermute(a, axis, [(i, (i + by) % n) for i in range(n)])  14.9 us
    ppermute x3, starting transfers between devices, on_device(): lax.ppermute(downs[-1], 'z', [((j - k + 1) % 8, (j - k) % 8) for j in ran...  6.87 us
    ppermute x4, waiting for transfers between devices, on_device(): lax.ppermute(ups[-1], 'z', [(i, i + 1) for i in range(k - 1, 7)])  6.59 us
    ppermute x4, starting transfers between devices, on_device(): lax.ppermute(ups[-1], 'z', [(i, i + 1) for i in range(k - 1, 7)])  5.13 us
    ppermute x3, waiting for transfers between devices, on_device(): lax.ppermute(downs[-1], 'z', [((j - k + 1) % 8, (j - k) % 8) for j in ran...  4.84 us
  transfers between devices with their start and end apart: 24, of which 11 were waited for; matrix products, arithmetic and copies ran while one was open for 1% of the time, Pallas kernels for 18%

profile of v3, /device:TPU:225, one launch (start us, length us, event | category | flops | bytes accessed | tf_op | source)
XLA Modules:
  0.0 115.2 jit_solution(6066163937817162573)
XLA Ops:
  0.0 2.5 %shard_map.163 = (bf16[4,72,2048]{2,1,0:T(8,128)(2,1)}, bf16[512,256]{1,0:T(8,128)(2,1)}, bf16[512,256]{1,0:T(8,128)(2,1)}) custom-call(bf16[1,64,2048]{2,1,0:T(8,128)(2,1)} %refs_0_.1, f32[1,2048]{1,0:T(1,128)} %bitcast.8, f32[32,128]{1,0:T(8,128)} %bitcast.7, bf16[4,128]{1,0:T(4,128)(2,1)} %bitcast.9, bf16[512,512]{1,0:T(8,128)(2,1)} %refs_4_.1, ...), custom_call_target="tpu_custom_call" | custom-call | flops 1000000 | bytes 1048576 | tf_op jit(solution)/shard_map/pallas_call | solution.py:67
  2.5 0.0 copy-start.2
  2.5 0.0 copy-start.4
  2.5 20.0 %all_to_all.5.refs_0_ = bf16[4,72,2048]{2,1,0:T(8,128)(2,1)S(1)} all-to-all(bf16[4,72,2048]{2,1,0:T(8,128)(2,1)} %get-tuple-element.46), channel_id=1, replica_groups=mesh['z'=8,'y'=4,'x'=4,'c'=2] {'y'}, dimensions={0} | all-to-all | bytes 2359296 | tf_op jit(solution)/shard_map/all_to_all | solution.py:595
  22.5 1.8 %collective-permute-start = (bf16[4,72,2048]{2,1,0:T(8,128)(2,1)S(1)}, bf16[4,72,2048]{2,1,0:T(8,128)(2,1)S(1)}, u32[]{:S(2)}, u32[]{:S(2)}) collective-permute-start(bf16[4,72,2048]{2,1,0:T(8,128)(2,1)S(1)} %all_to_all.5.refs_0_), channel_id=1, source_target_pairs={{0,1},{1,0},{2,3},{3,2},{4,5},{5,4},{6,7},{7,6},{8,9},{9,8},{10,11... | collective-permute-start | bytes 3538952 | tf_op jit(solution)/shard_map/ppermute | solution.py:568
  24.3 1.2 %collective-permute-start.1 = (bf16[512,256]{1,0:T(8,128)(2,1)S(1)}, bf16[512,256]{1,0:T(8,128)(2,1)S(1)}, u32[]{:S(2)}, u32[]{:S(2)}) collective-permute-start(bf16[512,256]{1,0:T(8,128)(2,1)S(1)} %copy-done.2), channel_id=1, source_target_pairs={{0,2},{2,4},{4,6},{6,0},{1,3},{3,5},{5,7},{7,1},{8,10},{10,12},{12... | collective-permute-start | bytes 786440 | tf_op jit(solution)/shard_map/ppermute | solution.py:568
  25.5 1.5 %collective-permute-start.5 = (bf16[512,256]{1,0:T(8,128)(2,1)S(1)}, bf16[512,256]{1,0:T(8,128)(2,1)S(1)}, u32[]{:S(2)}, u32[]{:S(2)}) collective-permute-start(bf16[512,256]{1,0:T(8,128)(2,1)S(1)} %copy-done.3), channel_id=1, source_target_pairs={{0,6},{2,0},{4,2},{6,4},{1,7},{3,1},{5,3},{7,5},{8,14},{10,8},{12,... | collective-permute-start | bytes 786440 | tf_op jit(solution)/shard_map/ppermute | solution.py:568
  27.0 1.3 %collective-permute-start.2 = (bf16[512,256]{1,0:T(8,128)(2,1)S(1)}, bf16[512,256]{1,0:T(8,128)(2,1)S(1)}, u32[]{:S(2)}, u32[]{:S(2)}) collective-permute-start(bf16[512,256]{1,0:T(8,128)(2,1)S(1)} %copy-done.2), channel_id=1, source_target_pairs={{0,6},{2,0},{4,2},{6,4},{1,7},{3,1},{5,3},{7,5},{8,14},{10,8},{12,... | collective-permute-start | bytes 786440 | tf_op jit(solution)/shard_map/ppermute | solution.py:568
  28.2 0.2 collective-permute-start.4
  28.4 4.9 %collective-permute-done.1.refs_3_ = bf16[512,256]{1,0:T(8,128)(2,1)S(1)} collective-permute-done((bf16[512,256]{1,0:T(8,128)(2,1)S(1)}, bf16[512,256]{1,0:T(8,128)(2,1)S(1)}, u32[]{:S(2)}, u32[]{:S(2)}) %collective-permute-start.1) | collective-permute-done | bytes 262176 | tf_op jit(solution)/shard_map/ppermute | solution.py:568
  33.4 0.0 collective-permute-start.3
  33.4 0.0 collective-permute-done.5.refs_8_
  33.4 2.7 %collective-permute-start.6 = (bf16[512,256]{1,0:T(8,128)(2,1)S(1)}, bf16[512,256]{1,0:T(8,128)(2,1)S(1)}, u32[]{:S(2)}, u32[]{:S(2)}) collective-permute-start(bf16[512,256]{1,0:T(8,128)(2,1)S(1)} %collective-permute-done.5.refs_8_), channel_id=1, source_target_pairs={{0,6},{2,0},{4,2},{6,4},{1,7},{3,1},{5,3},{7,5},{8,14},{10,8},{12,... | collective-permute-start | bytes 786440 | tf_op jit(solution)/shard_map/ppermute | solution.py:568
  36.0 0.7 broadcast_in_dim.4.refs_4_
  36.7 3.8 %shard_map.164 = (f32[256,512]{1,0:T(8,128)}, f32[256,512]{1,0:T(8,128)}, bf16[128,1024]{1,0:T(8,128)(2,1)}, bf16[128,1024]{1,0:T(8,128)(2,1)}, f32[2,512]{1,0:T(2,128)}, /*index=5*/f32[1,128]{1,0:T(1,128)}) custom-call(f32[2,32,16,64]{3,2,1,0:T(8,128)} %bitcast.10, f32[2,32,16,64]{3,2,1,0:T(8,128)} %refs_1_.1, f32[32,64]{1,0:T(8,128)} %refs_2_.1, ...), custom_call_target="tpu_custom_call" | custom-call | flops 1000000000 | bytes 1048576 | tf_op jit(solution)/shard_map/pallas_call | solution.py:67
  40.5 0.0 collective-permute-done.refs_1_
  40.5 0.0 copy-start.1
  40.5 0.0 copy-start
  40.6 0.0 collective-permute-done.2.refs_4_
  40.6 0.0 collective-permute-done.4.refs_7_
  40.6 4.0 %collective-permute-done.3.refs_5_ = bf16[512,256]{1,0:T(8,128)(2,1)S(1)} collective-permute-done((bf16[512,256]{1,0:T(8,128)(2,1)S(1)}, bf16[512,256]{1,0:T(8,128)(2,1)S(1)}, u32[]{:S(2)}, u32[]{:S(2)}) %collective-permute-start.3) | collective-permute-done | bytes 262176 | tf_op jit(solution)/shard_map/ppermute | solution.py:568
  44.6 0.0 collective-permute-done.6.refs_9_
  44.6 5.6 %shard_map.165 = (bf16[544,256]{1,0:T(8,128)(2,1)}, f32[512,128]{1,0:T(8,128)}, f32[512,128]{1,0:T(8,128)}, f32[8,512]{1,0:T(8,128)}, bf16[512,128]{1,0:T(8,128)(2,1)S(1)}) custom-call(bf16[4,72,2048]{2,1,0:T(8,128)(2,1)S(1)} %all_to_all.5.refs_0_, bf16[4,72,2048]{2,1,0:T(8,128)(2,1)S(1)} %collective-permute-done.refs_1_, bf16[512,256]{1,0:T(8,128)(2,1)S(1)} %copy-done.2, ...), custom_call_target="tpu_custom_call" | custom-call | flops 3000000000 | bytes 1048576 | tf_op jit(solution)/shard_map/pallas_call | solution.py:67
  50.2 1.3 %collective-permute-start.13 = (bf16[544,256]{1,0:T(8,128)(2,1)}, bf16[544,256]{1,0:T(8,128)(2,1)S(1)}, u32[]{:S(2)}, u32[]{:S(2)}) collective-permute-start(bf16[544,256]{1,0:T(8,128)(2,1)} %get-tuple-element.61.refs_0_), channel_id=1, source_target_pairs={{0,32},{32,64},{64,96},{96,128},{128,160},{160,192},{192,224},{1,3... | collective-permute-start | bytes 835592 | tf_op jit(solution)/shard_map/ppermute | solution.py:633
  51.5 1.3 %collective-permute-start.17 = (bf16[544,256]{1,0:T(8,128)(2,1)}, bf16[544,256]{1,0:T(8,128)(2,1)S(1)}, u32[]{:S(2)}, u32[]{:S(2)}) collective-permute-start(bf16[544,256]{1,0:T(8,128)(2,1)} %get-tuple-element.61.refs_0_), channel_id=1, source_target_pairs={{0,224},{32,0},{64,32},{1,225},{33,1},{65,33},{2,226},{34,2},{66,3... | collective-permute-start | bytes 835592 | tf_op jit(solution)/shard_map/ppermute | solution.py:635
  52.8 2.5 %collective-permute-start.10 = (bf16[512,512]{1,0:T(8,128)(2,1)S(1)}, bf16[512,512]{1,0:T(8,128)(2,1)S(1)}, u32[]{:S(2)}, u32[]{:S(2)}) collective-permute-start(bf16[512,512]{1,0:T(8,128)(2,1)S(1)} %copy-done.1), channel_id=1, source_target_pairs={{0,6},{2,0},{4,2},{6,4},{1,7},{3,1},{5,3},{7,5},{8,14},{10,8},{12,... | collective-permute-start | bytes 1572872 | tf_op jit(solution)/shard_map/ppermute | solution.py:568
  55.3 4.4 %collective-permute-done.13.refs_0_.refs_12_ = bf16[544,256]{1,0:T(8,128)(2,1)S(1)} collective-permute-done((bf16[544,256]{1,0:T(8,128)(2,1)}, bf16[544,256]{1,0:T(8,128)(2,1)S(1)}, u32[]{:S(2)}, u32[]{:S(2)}) %collective-permute-start.13) | collective-permute-done | bytes 278560 | tf_op jit(solution)/shard_map/ppermute | solution.py:633
  59.7 1.3 %collective-permute-start.14 = (bf16[544,256]{1,0:T(8,128)(2,1)S(1)}, bf16[544,256]{1,0:T(8,128)(2,1)S(1)}, u32[]{:S(2)}, u32[]{:S(2)}) collective-permute-start(bf16[544,256]{1,0:T(8,128)(2,1)S(1)} %collective-permute-done.13.refs_0_.refs_12_), channel_id=1, source_target_pairs={{32,64},{64,96},{96,128},{128,160},{160,192},{192,224},{33,65},{65... | collective-permute-start | bytes 835592 | tf_op jit(solution)/shard_map/ppermute | solution.py:633
  61.0 0.9 collective-permute-start.7
  61.9 0.3 collective-permute-done.17.refs_1_.refs_7_
  62.2 3.7 %collective-permute-start.18 = (bf16[544,256]{1,0:T(8,128)(2,1)S(1)}, bf16[544,256]{1,0:T(8,128)(2,1)S(1)}, u32[]{:S(2)}, u32[]{:S(2)}) collective-permute-start(bf16[544,256]{1,0:T(8,128)(2,1)S(1)} %collective-permute-done.17.refs_1_.refs_7_), channel_id=1, source_target_pairs={{224,192},{0,224},{32,0},{225,193},{1,225},{33,1},{226,194},{2,226... | collective-permute-start | bytes 835592 | tf_op jit(solution)/shard_map/ppermute | solution.py:635
  65.9 2.2 %collective-permute-done.14.refs_0_.refs_11_ = bf16[544,256]{1,0:T(8,128)(2,1)S(1)} collective-permute-done((bf16[544,256]{1,0:T(8,128)(2,1)S(1)}, bf16[544,256]{1,0:T(8,128)(2,1)S(1)}, u32[]{:S(2)}, u32[]{:S(2)}) %collective-permute-start.14) | collective-permute-done | bytes 278560 | tf_op jit(solution)/shard_map/ppermute | solution.py:633
  68.0 1.3 %collective-permute-start.15 = (bf16[544,256]{1,0:T(8,128)(2,1)S(1)}, bf16[544,256]{1,0:T(8,128)(2,1)S(1)}, u32[]{:S(2)}, u32[]{:S(2)}) collective-permute-start(bf16[544,256]{1,0:T(8,128)(2,1)S(1)} %collective-permute-done.14.refs_0_.refs_11_), channel_id=1, source_target_pairs={{64,96},{96,128},{128,160},{160,192},{192,224},{65,97},{97,129},{1... | collective-permute-start | bytes 835592 | tf_op jit(solution)/shard_map/ppermute | solution.py:633
  69.3 2.2 %collective-permute-done.18.refs_1_.refs_8_ = bf16[544,256]{1,0:T(8,128)(2,1)S(1)} collective-permute-done((bf16[544,256]{1,0:T(8,128)(2,1)S(1)}, bf16[544,256]{1,0:T(8,128)(2,1)S(1)}, u32[]{:S(2)}, u32[]{:S(2)}) %collective-permute-start.18) | collective-permute-done | bytes 278560 | tf_op jit(solution)/shard_map/ppermute | solution.py:635
  71.5 1.9 %collective-permute-start.19 = (bf16[544,256]{1,0:T(8,128)(2,1)S(1)}, bf16[544,256]{1,0:T(8,128)(2,1)S(1)}, u32[]{:S(2)}, u32[]{:S(2)}) collective-permute-start(bf16[544,256]{1,0:T(8,128)(2,1)S(1)} %collective-permute-done.18.refs_1_.refs_8_), channel_id=1, source_target_pairs={{192,160},{224,192},{0,224},{193,161},{225,193},{1,225},{194,162},... | collective-permute-start | bytes 835592 | tf_op jit(solution)/shard_map/ppermute | solution.py:635
  73.4 1.0 collective-permute-start.11
  74.4 0.0 collective-permute-done.10.refs_5_
  74.4 1.8 %collective-permute-start.8 = (bf16[512,512]{1,0:T(8,128)(2,1)S(1)}, bf16[512,512]{1,0:T(8,128)(2,1)S(1)}, u32[]{:S(2)}, u32[]{:S(2)}) collective-permute-start(bf16[512,512]{1,0:T(8,128)(2,1)S(1)} %copy-done), channel_id=1, source_target_pairs={{0,6},{2,0},{4,2},{6,4},{1,7},{3,1},{5,3},{7,5},{8,14},{10,8},{12,... | collective-permute-start | bytes 1572872 | tf_op jit(solution)/shard_map/ppermute | solution.py:568
  76.2 0.0 collective-permute-done.7.refs_1_
  76.2 1.1 collective-permute-start.12
  77.3 0.0 collective-permute-done.15.refs_0_.refs_10_
  77.3 0.4 collective-permute-start.9
  77.7 2.3 %collective-permute-done.19.refs_1_.refs_9_ = bf16[544,256]{1,0:T(8,128)(2,1)S(1)} collective-permute-done((bf16[544,256]{1,0:T(8,128)(2,1)S(1)}, bf16[544,256]{1,0:T(8,128)(2,1)S(1)}, u32[]{:S(2)}, u32[]{:S(2)}) %collective-permute-start.19) | collective-permute-done | bytes 278560 | tf_op jit(solution)/shard_map/ppermute | solution.py:635
  80.0 1.3 %collective-permute-start.16 = (bf16[544,256]{1,0:T(8,128)(2,1)S(1)}, bf16[544,256]{1,0:T(8,128)(2,1)S(1)}, u32[]{:S(2)}, u32[]{:S(2)}) collective-permute-start(bf16[544,256]{1,0:T(8,128)(2,1)S(1)} %collective-permute-done.15.refs_0_.refs_10_), channel_id=1, source_target_pairs={{96,128},{128,160},{160,192},{192,224},{97,129},{129,161},{161,193... | collective-permute-start | bytes 835592 | tf_op jit(solution)/shard_map/ppermute | solution.py:633
  81.3 2.9 %shard_map.166 = (f32[512,128]{1,0:T(8,128)S(1)}, f32[512,128]{1,0:T(8,128)S(1)}, f32[512,128]{1,0:T(8,128)S(1)}) custom-call(bf16[544,256]{1,0:T(8,128)(2,1)} %get-tuple-element.61.refs_0_, bf16[512,128]{1,0:T(8,128)(2,1)S(1)} %get-tuple-element.68.refs_1_.refs_2_.refs_13_), custom_call_target="tpu_custom_call" | custom-call | flops 268435456 | bytes 1048576 | tf_op jit(solution)/shard_map/pallas_call | solution.py:67
  84.2 3.7 %shard_map.167 = (f32[512,128]{1,0:T(8,128)S(1)}, f32[512,128]{1,0:T(8,128)S(1)}, f32[512,128]{1,0:T(8,128)S(1)}) custom-call(bf16[544,256]{1,0:T(8,128)(2,1)S(1)} %collective-permute-done.13.refs_0_.refs_12_, bf16[544,256]{1,0:T(8,128)(2,1)S(1)} %collective-permute-done.17.refs_1_.refs_7_, ...), custom_call_target="tpu_custom_call", output_to_operand_aliasing={{0}: (3, {}), {1}: (4, {}), {2}: (5, {})} | custom-call | flops 536870912 | bytes 1048576 | tf_op jit(solution)/shard_map/pallas_call | solution.py:67
  87.9 3.7 %shard_map.168 = (f32[512,128]{1,0:T(8,128)S(1)}, f32[512,128]{1,0:T(8,128)S(1)}, f32[512,128]{1,0:T(8,128)S(1)}) custom-call(bf16[544,256]{1,0:T(8,128)(2,1)S(1)} %collective-permute-done.14.refs_0_.refs_11_, bf16[544,256]{1,0:T(8,128)(2,1)S(1)} %collective-permute-done.18.refs_1_.refs_8_, ...), custom_call_target="tpu_custom_call", output_to_operand_aliasing={{0}: (3, {}), {1}: (4, {}), {2}: (5, {})} | custom-call | flops 536870912 | bytes 1048576 | tf_op jit(solution)/shard_map/pallas_call | solution.py:67
  91.6 3.7 %shard_map.169 = (f32[512,128]{1,0:T(8,128)S(1)}, f32[512,128]{1,0:T(8,128)S(1)}, f32[512,128]{1,0:T(8,128)S(1)}) custom-call(bf16[544,256]{1,0:T(8,128)(2,1)S(1)} %collective-permute-done.15.refs_0_.refs_10_, bf16[544,256]{1,0:T(8,128)(2,1)S(1)} %collective-permute-done.19.refs_1_.refs_9_, ...), custom_call_target="tpu_custom_call", output_to_operand_aliasing={{0}: (3, {}), {1}: (4, {}), {2}: (5, {})} | custom-call | flops 536870912 | bytes 1048576 | tf_op jit(solution)/shard_map/pallas_call | solution.py:67
  95.3 0.0 collective-permute-done.16.refs_0_
  95.3 2.7 %shard_map.170 = (bf16[128,256]{1,0:T(8,128)(2,1)S(1)}, bf16[128,256]{1,0:T(8,128)(2,1)S(1)}, bf16[128,256]{1,0:T(8,128)(2,1)S(1)}, bf16[128,256]{1,0:T(8,128)(2,1)S(1)}) custom-call(bf16[544,256]{1,0:T(8,128)(2,1)S(1)} %collective-permute-done.16.refs_0_, f32[512,128]{1,0:T(8,128)} %get-tuple-element.64.refs_1_, f32[512,128]{1,0:T(8,128)} %get-tuple-element.65.refs_2_, ...), custom_call_target="tpu_custom_call" | custom-call | flops 536870912 | bytes 1048576 | tf_op jit(solution)/shard_map/pallas_call | solution.py:67
  98.1 0.6 collective-permute-start.20
  98.7 0.0 collective-permute-done.11.refs_6_
  98.7 2.4 %collective-permute-start.21 = (bf16[128,256]{1,0:T(8,128)(2,1)S(1)}, bf16[128,256]{1,0:T(8,128)(2,1)S(1)}, u32[]{:S(2)}, u32[]{:S(2)}) collective-permute-start(bf16[128,256]{1,0:T(8,128)(2,1)S(1)} %get-tuple-element.83), channel_id=1, source_target_pairs={{0,24},{8,0},{16,8},{24,16},{1,25},{9,1},{17,9},{25,17},{2,26},{10... | collective-permute-start | bytes 196616 | tf_op jit(solution)/shard_map/ppermute | solution.py:568
  101.1 0.0 collective-permute-done.8.refs_2_
  101.1 0.0 collective-permute-start.22
  101.1 0.0 collective-permute-done.12.refs_7_
  101.1 0.0 collective-permute-done.9.refs_3_
  101.1 1.6 %collective-permute-done.20.refs_9_ = bf16[128,256]{1,0:T(8,128)(2,1)S(1)} collective-permute-done((bf16[128,256]{1,0:T(8,128)(2,1)S(1)}, bf16[128,256]{1,0:T(8,128)(2,1)S(1)}, u32[]{:S(2)}, u32[]{:S(2)}) %collective-permute-start.20) | collective-permute-done | bytes 65568 | tf_op jit(solution)/shard_map/ppermute | solution.py:568
  102.7 0.3 collective-permute-done.21.refs_10_
  103.0 2.7 %collective-permute-done.22.refs_11_ = bf16[128,256]{1,0:T(8,128)(2,1)S(1)} collective-permute-done((bf16[128,256]{1,0:T(8,128)(2,1)S(1)}, bf16[128,256]{1,0:T(8,128)(2,1)S(1)}, u32[]{:S(2)}, u32[]{:S(2)}) %collective-permute-start.22) | collective-permute-done | bytes 65568 | tf_op jit(solution)/shard_map/ppermute | solution.py:568
  105.7 1.5 %shard_map.171 = (bf16[64,2048]{1,0:T(8,128)(2,1)}, f32[64,2048]{1,0:T(8,128)S(1)}) custom-call(bf16[512,512]{1,0:T(8,128)(2,1)S(1)} %copy-done, bf16[512,512]{1,0:T(8,128)(2,1)S(1)} %collective-permute-done.7.refs_1_, bf16[512,512]{1,0:T(8,128)(2,1)S(1)} %collective-permute-done.8.refs_2_, bf16[512,512]{1,0:T(8,128)(2,1)S(1)} %collective-permute-done.9.refs_3_, ...), custom_call_target="tpu_custom_call" | custom-call | flops 536870912 | bytes 1048576 | tf_op jit(solution)/shard_map/pallas_call | solution.py:67
  107.3 5.8 %collective-permute-start.23 = (bf16[64,2048]{1,0:T(8,128)(2,1)}, bf16[64,2048]{1,0:T(8,128)(2,1)S(1)}, u32[]{:S(2)}, u32[]{:S(2)}) collective-permute-start(bf16[64,2048]{1,0:T(8,128)(2,1)} %get-tuple-element.86), channel_id=1, source_target_pairs={{0,1},{1,0},{2,3},{3,2},{4,5},{5,4},{6,7},{7,6},{8,9},{9,8},{10,11... | collective-permute-start | bytes 786440 | tf_op jit(solution)/shard_map/ppermute | solution.py:568
  113.0 1.4 %collective-permute-done.23 = bf16[64,2048]{1,0:T(8,128)(2,1)S(1)} collective-permute-done((bf16[64,2048]{1,0:T(8,128)(2,1)}, bf16[64,2048]{1,0:T(8,128)(2,1)S(1)}, u32[]{:S(2)}, u32[]{:S(2)}) %collective-permute-start.23) | collective-permute-done | bytes 262176 | tf_op jit(solution)/shard_map/ppermute | solution.py:568
  114.4 0.8 fusion
  (6 shorter events, 0.0 us)
Async XLA Ops:
  2.5 21.8 %copy-start.2 = (bf16[512,256]{1,0:T(8,128)(2,1)S(1)}, bf16[512,256]{1,0:T(8,128)(2,1)}, u32[]{:S(2)}) copy-start(bf16[512,256]{1,0:T(8,128)(2,1)} %get-tuple-element.54.refs_2_) | copy-start | bytes 786436
  2.5 23.0 %copy-start.3 = (bf16[512,256]{1,0:T(8,128)(2,1)S(1)}, bf16[512,256]{1,0:T(8,128)(2,1)}, u32[]{:S(2)}) copy-start(bf16[512,256]{1,0:T(8,128)(2,1)} %get-tuple-element.55.refs_6_) | copy-start | bytes 786436
  2.5 33.6 %copy-start.4 = (f32[32]{0:T(128)S(1)}, f32[32]{0:T(128)}, u32[]{:S(2)}) copy-start(f32[32]{0:T(128)} %param.24) | copy-start | bytes 388
  22.5 18.1 %collective-permute-start = (bf16[4,72,2048]{2,1,0:T(8,128)(2,1)S(1)}, bf16[4,72,2048]{2,1,0:T(8,128)(2,1)S(1)}, u32[]{:S(2)}, u32[]{:S(2)}) collective-permute-start(bf16[4,72,2048]{2,1,0:T(8,128)(2,1)S(1)} %all_to_all.5.refs_0_), channel_id=1, source_target_pairs={{0,1},{1,0},{2,3},{3,2},{4,5},{5,4},{6,7},{7,6},{8,9},{9,8},{10,11... | collective-permute-start | bytes 3538952 | tf_op jit(solution)/shard_map/ppermute | solution.py:568
  24.3 9.1 %collective-permute-start.1 = (bf16[512,256]{1,0:T(8,128)(2,1)S(1)}, bf16[512,256]{1,0:T(8,128)(2,1)S(1)}, u32[]{:S(2)}, u32[]{:S(2)}) collective-permute-start(bf16[512,256]{1,0:T(8,128)(2,1)S(1)} %copy-done.2), channel_id=1, source_target_pairs={{0,2},{2,4},{4,6},{6,0},{1,3},{3,5},{5,7},{7,1},{8,10},{10,12},{12... | collective-permute-start | bytes 786440 | tf_op jit(solution)/shard_map/ppermute | solution.py:568
  25.5 7.9 %collective-permute-start.5 = (bf16[512,256]{1,0:T(8,128)(2,1)S(1)}, bf16[512,256]{1,0:T(8,128)(2,1)S(1)}, u32[]{:S(2)}, u32[]{:S(2)}) collective-permute-start(bf16[512,256]{1,0:T(8,128)(2,1)S(1)} %copy-done.3), channel_id=1, source_target_pairs={{0,6},{2,0},{4,2},{6,4},{1,7},{3,1},{5,3},{7,5},{8,14},{10,8},{12,... | collective-permute-start | bytes 786440 | tf_op jit(solution)/shard_map/ppermute | solution.py:568
  27.0 13.6 %collective-permute-start.2 = (bf16[512,256]{1,0:T(8,128)(2,1)S(1)}, bf16[512,256]{1,0:T(8,128)(2,1)S(1)}, u32[]{:S(2)}, u32[]{:S(2)}) collective-permute-start(bf16[512,256]{1,0:T(8,128)(2,1)S(1)} %copy-done.2), channel_id=1, source_target_pairs={{0,6},{2,0},{4,2},{6,4},{1,7},{3,1},{5,3},{7,5},{8,14},{10,8},{12,... | collective-permute-start | bytes 786440 | tf_op jit(solution)/shard_map/ppermute | solution.py:568
  28.2 12.3 %collective-permute-start.4 = (bf16[512,256]{1,0:T(8,128)(2,1)S(1)}, bf16[512,256]{1,0:T(8,128)(2,1)S(1)}, u32[]{:S(2)}, u32[]{:S(2)}) collective-permute-start(bf16[512,256]{1,0:T(8,128)(2,1)S(1)} %copy-done.3), channel_id=1, source_target_pairs={{0,2},{2,4},{4,6},{6,0},{1,3},{3,5},{5,7},{7,1},{8,10},{10,12},{12... | collective-permute-start | bytes 786440 | tf_op jit(solution)/shard_map/ppermute | solution.py:568
  33.4 11.2 %collective-permute-start.3 = (bf16[512,256]{1,0:T(8,128)(2,1)S(1)}, bf16[512,256]{1,0:T(8,128)(2,1)S(1)}, u32[]{:S(2)}, u32[]{:S(2)}) collective-permute-start(bf16[512,256]{1,0:T(8,128)(2,1)S(1)} %collective-permute-done.1.refs_3_), channel_id=1, source_target_pairs={{0,2},{2,4},{4,6},{6,0},{1,3},{3,5},{5,7},{7,1},{8,10},{10,12},{12... | collective-permute-start | bytes 786440 | tf_op jit(solution)/shard_map/ppermute | solution.py:568
  33.4 11.2 %collective-permute-start.6 = (bf16[512,256]{1,0:T(8,128)(2,1)S(1)}, bf16[512,256]{1,0:T(8,128)(2,1)S(1)}, u32[]{:S(2)}, u32[]{:S(2)}) collective-permute-start(bf16[512,256]{1,0:T(8,128)(2,1)S(1)} %collective-permute-done.5.refs_8_), channel_id=1, source_target_pairs={{0,6},{2,0},{4,2},{6,4},{1,7},{3,1},{5,3},{7,5},{8,14},{10,8},{12,... | collective-permute-start | bytes 786440 | tf_op jit(solution)/shard_map/ppermute | solution.py:568
  40.5 12.3 %copy-start.1 = (bf16[512,512]{1,0:T(8,128)(2,1)S(1)}, bf16[512,512]{1,0:T(8,128)(2,1)}, u32[]{:S(2)}) copy-start(bf16[512,512]{1,0:T(8,128)(2,1)} %refs_4_.2) | copy-start | bytes 1572868
  40.5 20.4 %copy-start = (bf16[512,512]{1,0:T(8,128)(2,1)S(1)}, bf16[512,512]{1,0:T(8,128)(2,1)}, u32[]{:S(2)}) copy-start(bf16[512,512]{1,0:T(8,128)(2,1)} %refs_0_.2) | copy-start | bytes 1572868
  50.2 9.5 %collective-permute-start.13 = (bf16[544,256]{1,0:T(8,128)(2,1)}, bf16[544,256]{1,0:T(8,128)(2,1)S(1)}, u32[]{:S(2)}, u32[]{:S(2)}) collective-permute-start(bf16[544,256]{1,0:T(8,128)(2,1)} %get-tuple-element.61.refs_0_), channel_id=1, source_target_pairs={{0,32},{32,64},{64,96},{96,128},{128,160},{160,192},{192,224},{1,3... | collective-permute-start | bytes 835592 | tf_op jit(solution)/shard_map/ppermute | solution.py:633
  51.5 10.7 %collective-permute-start.17 = (bf16[544,256]{1,0:T(8,128)(2,1)}, bf16[544,256]{1,0:T(8,128)(2,1)S(1)}, u32[]{:S(2)}, u32[]{:S(2)}) collective-permute-start(bf16[544,256]{1,0:T(8,128)(2,1)} %get-tuple-element.61.refs_0_), channel_id=1, source_target_pairs={{0,224},{32,0},{64,32},{1,225},{33,1},{65,33},{2,226},{34,2},{66,3... | collective-permute-start | bytes 835592 | tf_op jit(solution)/shard_map/ppermute | solution.py:635
  52.8 21.6 %collective-permute-start.10 = (bf16[512,512]{1,0:T(8,128)(2,1)S(1)}, bf16[512,512]{1,0:T(8,128)(2,1)S(1)}, u32[]{:S(2)}, u32[]{:S(2)}) collective-permute-start(bf16[512,512]{1,0:T(8,128)(2,1)S(1)} %copy-done.1), channel_id=1, source_target_pairs={{0,6},{2,0},{4,2},{6,4},{1,7},{3,1},{5,3},{7,5},{8,14},{10,8},{12,... | collective-permute-start | bytes 1572872 | tf_op jit(solution)/shard_map/ppermute | solution.py:568
  59.7 8.4 %collective-permute-start.14 = (bf16[544,256]{1,0:T(8,128)(2,1)S(1)}, bf16[544,256]{1,0:T(8,128)(2,1)S(1)}, u32[]{:S(2)}, u32[]{:S(2)}) collective-permute-start(bf16[544,256]{1,0:T(8,128)(2,1)S(1)} %collective-permute-done.13.refs_0_.refs_12_), channel_id=1, source_target_pairs={{32,64},{64,96},{96,128},{128,160},{160,192},{192,224},{33,65},{65... | collective-permute-start | bytes 835592 | tf_op jit(solution)/shard_map/ppermute | solution.py:633
  61.0 15.2 %collective-permute-start.7 = (bf16[512,512]{1,0:T(8,128)(2,1)S(1)}, bf16[512,512]{1,0:T(8,128)(2,1)S(1)}, u32[]{:S(2)}, u32[]{:S(2)}) collective-permute-start(bf16[512,512]{1,0:T(8,128)(2,1)S(1)} %copy-done), channel_id=1, source_target_pairs={{0,2},{2,4},{4,6},{6,0},{1,3},{3,5},{5,7},{7,1},{8,10},{10,12},{12... | collective-permute-start | bytes 1572872 | tf_op jit(solution)/shard_map/ppermute | solution.py:568
  62.2 9.3 %collective-permute-start.18 = (bf16[544,256]{1,0:T(8,128)(2,1)S(1)}, bf16[544,256]{1,0:T(8,128)(2,1)S(1)}, u32[]{:S(2)}, u32[]{:S(2)}) collective-permute-start(bf16[544,256]{1,0:T(8,128)(2,1)S(1)} %collective-permute-done.17.refs_1_.refs_7_), channel_id=1, source_target_pairs={{224,192},{0,224},{32,0},{225,193},{1,225},{33,1},{226,194},{2,226... | collective-permute-start | bytes 835592 | tf_op jit(solution)/shard_map/ppermute | solution.py:635
  68.0 9.2 %collective-permute-start.15 = (bf16[544,256]{1,0:T(8,128)(2,1)S(1)}, bf16[544,256]{1,0:T(8,128)(2,1)S(1)}, u32[]{:S(2)}, u32[]{:S(2)}) collective-permute-start(bf16[544,256]{1,0:T(8,128)(2,1)S(1)} %collective-permute-done.14.refs_0_.refs_11_), channel_id=1, source_target_pairs={{64,96},{96,128},{128,160},{160,192},{192,224},{65,97},{97,129},{1... | collective-permute-start | bytes 835592 | tf_op jit(solution)/shard_map/ppermute | solution.py:633
  71.5 8.5 %collective-permute-start.19 = (bf16[544,256]{1,0:T(8,128)(2,1)S(1)}, bf16[544,256]{1,0:T(8,128)(2,1)S(1)}, u32[]{:S(2)}, u32[]{:S(2)}) collective-permute-start(bf16[544,256]{1,0:T(8,128)(2,1)S(1)} %collective-permute-done.18.refs_1_.refs_8_), channel_id=1, source_target_pairs={{192,160},{224,192},{0,224},{193,161},{225,193},{1,225},{194,162},... | collective-permute-start | bytes 835592 | tf_op jit(solution)/shard_map/ppermute | solution.py:635
  73.4 25.2 %collective-permute-start.11 = (bf16[512,512]{1,0:T(8,128)(2,1)S(1)}, bf16[512,512]{1,0:T(8,128)(2,1)S(1)}, u32[]{:S(2)}, u32[]{:S(2)}) collective-permute-start(bf16[512,512]{1,0:T(8,128)(2,1)S(1)} %copy-done.1), channel_id=1, source_target_pairs={{0,2},{2,4},{4,6},{6,0},{1,3},{3,5},{5,7},{7,1},{8,10},{10,12},{12... | collective-permute-start | bytes 1572872 | tf_op jit(solution)/shard_map/ppermute | solution.py:568
  74.4 26.6 %collective-permute-start.8 = (bf16[512,512]{1,0:T(8,128)(2,1)S(1)}, bf16[512,512]{1,0:T(8,128)(2,1)S(1)}, u32[]{:S(2)}, u32[]{:S(2)}) collective-permute-start(bf16[512,512]{1,0:T(8,128)(2,1)S(1)} %copy-done), channel_id=1, source_target_pairs={{0,6},{2,0},{4,2},{6,4},{1,7},{3,1},{5,3},{7,5},{8,14},{10,8},{12,... | collective-permute-start | bytes 1572872 | tf_op jit(solution)/shard_map/ppermute | solution.py:568
  76.2 24.9 %collective-permute-start.12 = (bf16[512,512]{1,0:T(8,128)(2,1)S(1)}, bf16[512,512]{1,0:T(8,128)(2,1)S(1)}, u32[]{:S(2)}, u32[]{:S(2)}) collective-permute-start(bf16[512,512]{1,0:T(8,128)(2,1)S(1)} %collective-permute-done.10.refs_5_), channel_id=1, source_target_pairs={{0,6},{2,0},{4,2},{6,4},{1,7},{3,1},{5,3},{7,5},{8,14},{10,8},{12,... | collective-permute-start | bytes 1572872 | tf_op jit(solution)/shard_map/ppermute | solution.py:568
  77.3 23.8 %collective-permute-start.9 = (bf16[512,512]{1,0:T(8,128)(2,1)S(1)}, bf16[512,512]{1,0:T(8,128)(2,1)S(1)}, u32[]{:S(2)}, u32[]{:S(2)}) collective-permute-start(bf16[512,512]{1,0:T(8,128)(2,1)S(1)} %collective-permute-done.7.refs_1_), channel_id=1, source_target_pairs={{0,2},{2,4},{4,6},{6,0},{1,3},{3,5},{5,7},{7,1},{8,10},{10,12},{12... | collective-permute-start | bytes 1572872 | tf_op jit(solution)/shard_map/ppermute | solution.py:568
  80.0 15.3 %collective-permute-start.16 = (bf16[544,256]{1,0:T(8,128)(2,1)S(1)}, bf16[544,256]{1,0:T(8,128)(2,1)S(1)}, u32[]{:S(2)}, u32[]{:S(2)}) collective-permute-start(bf16[544,256]{1,0:T(8,128)(2,1)S(1)} %collective-permute-done.15.refs_0_.refs_10_), channel_id=1, source_target_pairs={{96,128},{128,160},{160,192},{192,224},{97,129},{129,161},{161,193... | collective-permute-start | bytes 835592 | tf_op jit(solution)/shard_map/ppermute | solution.py:633
  98.1 4.6 %collective-permute-start.20 = (bf16[128,256]{1,0:T(8,128)(2,1)S(1)}, bf16[128,256]{1,0:T(8,128)(2,1)S(1)}, u32[]{:S(2)}, u32[]{:S(2)}) collective-permute-start(bf16[128,256]{1,0:T(8,128)(2,1)S(1)} %get-tuple-element.82), channel_id=1, source_target_pairs={{0,8},{8,16},{16,24},{24,0},{1,9},{9,17},{17,25},{25,1},{2,10},{10... | collective-permute-start | bytes 196616 | tf_op jit(solution)/shard_map/ppermute | solution.py:568
  98.7 4.3 %collective-permute-start.21 = (bf16[128,256]{1,0:T(8,128)(2,1)S(1)}, bf16[128,256]{1,0:T(8,128)(2,1)S(1)}, u32[]{:S(2)}, u32[]{:S(2)}) collective-permute-start(bf16[128,256]{1,0:T(8,128)(2,1)S(1)} %get-tuple-element.83), channel_id=1, source_target_pairs={{0,24},{8,0},{16,8},{24,16},{1,25},{9,1},{17,9},{25,17},{2,26},{10... | collective-permute-start | bytes 196616 | tf_op jit(solution)/shard_map/ppermute | solution.py:568
  101.1 4.6 %collective-permute-start.22 = (bf16[128,256]{1,0:T(8,128)(2,1)S(1)}, bf16[128,256]{1,0:T(8,128)(2,1)S(1)}, u32[]{:S(2)}, u32[]{:S(2)}) collective-permute-start(bf16[128,256]{1,0:T(8,128)(2,1)S(1)} %get-tuple-element.84), channel_id=1, source_target_pairs={{0,16},{8,24},{16,0},{24,8},{1,17},{9,25},{17,1},{25,9},{2,18},{10... | collective-permute-start | bytes 196616 | tf_op jit(solution)/shard_map/ppermute | solution.py:568
  107.3 7.1 %collective-permute-start.23 = (bf16[64,2048]{1,0:T(8,128)(2,1)}, bf16[64,2048]{1,0:T(8,128)(2,1)S(1)}, u32[]{:S(2)}, u32[]{:S(2)}) collective-permute-start(bf16[64,2048]{1,0:T(8,128)(2,1)} %get-tuple-element.86), channel_id=1, source_target_pairs={{0,1},{1,0},{2,3},{3,2},{4,5},{5,4},{6,7},{7,6},{8,9},{9,8},{10,11... | collective-permute-start | bytes 786440 | tf_op jit(solution)/shard_map/ppermute | solution.py:568

commit v4 on v3

--- a/solution.py
+++ b/solution.py
@@ -404,10 +404,14 @@
     c = lax.axis_index("c")
     x = lax.axis_index("x")
     copies = []
-    for n, (step, ref) in enumerate(((0, a0), (3, a3), (1, a1), (2, a2), (0, b0), (3, b3), (1, b1), (2, b2))):
+    arriving = []
+    for n, (step, a_ref, b_ref2) in enumerate(((0, a0, b0), (3, a3, b3), (1, a1, b1), (2, a2, b2))):
         at = pl.multiple_of(((x + step) % 4) * ROWS, ROWS)
-        to = w_ref.at[pl.ds(at, ROWS), pl.ds(256 * (n // 4), 256)]
-        copies.append(pltpu.make_async_copy(ref, to, sems.at[12 + n]))
+        pair = [
+            pltpu.make_async_copy(ref, w_ref.at[n, :, pl.ds(256 * h, 256)], sems.at[12 + 2 * n + h])
+            for h, ref in enumerate((a_ref, b_ref2))
+        ]
+        arriving.append((at, pair))
     for b in range(4):
         for part, ref in enumerate((mine, theirs)):
             at = pl.multiple_of(b * BLOCK + ((c + part) % 2) * 64, 64)
@@ -418,7 +422,7 @@
         copies.append(
             pltpu.make_async_copy(mine.at[b, pl.ds(64, MORE)], more.at[b], sems.at[8 + b])
         )
-    for copy in copies[-4:] + copies[:-4]:
+    for copy in copies[-4:] + copies[:-4] + [copy for _, pair in arriving for copy in pair]:
         copy.start()
     for copy in copies[-4:]:
         copy.wait()
@@ -453,7 +457,12 @@
         )
     for copy in copies[:-4]:
         copy.wait()
-    both = mm(rows[...], w_ref[...])
+    both = None
+    for n, (at, pair) in enumerate(arriving):
+        for copy in pair:
+            copy.wait()
+        part = mm(rows[:, pl.ds(at, ROWS)], w_ref[n])
+        both = part if both is None else both + part
     kv_ref[:ROWS, :] = both[:, :256].astype(bf16)
     q_ref[...] = both[:, 256:384].astype(bf16)
     u_ref[...] = both[:, 384:].astype(bf16)
@@ -504,7 +513,7 @@
             pltpu.VMEM((ROWS, BLOCK), bf16),
             pltpu.VMEM((ROWS, 2 * N), f32),
             pltpu.VMEM((ROWS, 2 * N), bf16),
-            pltpu.VMEM((2048, ROWS), bf16),
+            pltpu.VMEM((4, ROWS, ROWS), bf16),
         ],
         flops=3 * 10**9,
         lazy=True,
@@ -630,9 +639,9 @@
     )
     ups, downs = [kv], [kv]
     for k in range(1, 5):
-        ups.append(lax.ppermute(ups[-1], "z", [(i, i + 1) for i in range(k - 1, 7)]))
+        ups.append(shift(ups[-1], "z", 1))
         if k < 4:
-            downs.append(lax.ppermute(downs[-1], "z", [((j - k + 1) % 8, (j - k) % 8) for j in range(3)]))
+            downs.append(shift(downs[-1], "z", -1))
     out_pieces = []
     for w, way in ((scan_out_weight, 1), (attend_out_weight, -1)):
         w = after(w, kv)

time: 116 us -> 109 us (0.940)
  starting transfers between devices: 37 us -> 31.2 us
    ppermute x7 -> x0, starting transfers between devices: 12 us -> none  [the longest x3 6.87 us: on_device(): lax.ppermute(downs[-1], 'z', [((j - k + 1) % 8, (j - k) % 8) for j in ran...]
    ppermute x7 -> x0, waiting for transfers between devices: 11.4 us -> none  [the longest x4 6.59 us: on_device(): lax.ppermute(ups[-1], 'z', [(i, i + 1) for i in range(k - 1, 7)])]
    ppermute x17 -> x24, waiting for transfers between devices: 14.9 us -> 25.8 us  [shift(): return lax.ppermute(a, axis, [(i, (i + by) % n) for i in range(n)])]
    ppermute x17 -> x24, starting transfers between devices: 25 us -> 31.2 us  [shift(): return lax.ppermute(a, axis, [(i, (i + by) % n) for i in range(n)])]
  transfers between devices with their start and end apart: 24 -> 24, of which waited for: 11 -> 10; matrix products, arithmetic and copies ran while one was open for 1% -> 1% of each run, Pallas kernels for 18% -> 19%
where the time goes in v4:
time: 109 us
  starting transfers between devices  31.2 us (29%)
  Pallas kernels  30.5 us (28%)
  waiting for transfers between devices  25.8 us (24%)
  blocking collectives  20 us (18%)
    ppermute x24, starting transfers between devices, shift(): return lax.ppermute(a, axis, [(i, (i + by) % n) for i in range(n)])  31.2 us
    pallas_call x9, Pallas kernels, staged(): pl.pallas_call(kernel, out_shape=tuple((pltpu.HBM(o.shape, o.dtype) for o...  30.5 us
    ppermute x24, waiting for transfers between devices, shift(): return lax.ppermute(a, axis, [(i, (i + by) % n) for i in range(n)])  25.8 us
    all_to_all x1, blocking collectives, exchange(): return lax.all_to_all(a, axis, split_axis=0, concat_axis=0, tiled=True)  20 us
  transfers between devices with their start and end apart: 24, of which 10 were waited for; matrix products, arithmetic and copies ran while one was open for 1% of the time, Pallas kernels for 19%

profile of v4, /device:TPU:225, one launch (start us, length us, event | category | flops | bytes accessed | tf_op | source)
XLA Modules:
  0.0 109.1 jit_solution(13669307947818870665)
XLA Ops:
  0.0 2.5 %shard_map.163 = (bf16[4,72,2048]{2,1,0:T(8,128)(2,1)}, bf16[512,256]{1,0:T(8,128)(2,1)}, bf16[512,256]{1,0:T(8,128)(2,1)}) custom-call(bf16[1,64,2048]{2,1,0:T(8,128)(2,1)} %refs_0_.1, f32[1,2048]{1,0:T(1,128)} %bitcast.8, f32[32,128]{1,0:T(8,128)} %bitcast.7, bf16[4,128]{1,0:T(4,128)(2,1)} %bitcast.9, bf16[512,512]{1,0:T(8,128)(2,1)} %refs_4_.1, ...), custom_call_target="tpu_custom_call" | custom-call | flops 1000000 | bytes 1048576 | tf_op jit(solution)/shard_map/pallas_call | solution.py:67
  2.5 0.0 copy-start.2
  2.5 0.0 copy-start.4
  2.5 20.0 %all_to_all.5.refs_0_ = bf16[4,72,2048]{2,1,0:T(8,128)(2,1)S(1)} all-to-all(bf16[4,72,2048]{2,1,0:T(8,128)(2,1)} %get-tuple-element.46), channel_id=1, replica_groups=mesh['z'=8,'y'=4,'x'=4,'c'=2] {'y'}, dimensions={0} | all-to-all | bytes 2359296 | tf_op jit(solution)/shard_map/all_to_all | solution.py:604
  22.5 1.8 %collective-permute-start = (bf16[4,72,2048]{2,1,0:T(8,128)(2,1)S(1)}, bf16[4,72,2048]{2,1,0:T(8,128)(2,1)S(1)}, u32[]{:S(2)}, u32[]{:S(2)}) collective-permute-start(bf16[4,72,2048]{2,1,0:T(8,128)(2,1)S(1)} %all_to_all.5.refs_0_), channel_id=1, source_target_pairs={{0,1},{1,0},{2,3},{3,2},{4,5},{5,4},{6,7},{7,6},{8,9},{9,8},{10,11... | collective-permute-start | bytes 3538952 | tf_op jit(solution)/shard_map/ppermute | solution.py:577
  24.3 1.2 %collective-permute-start.1 = (bf16[512,256]{1,0:T(8,128)(2,1)S(1)}, bf16[512,256]{1,0:T(8,128)(2,1)S(1)}, u32[]{:S(2)}, u32[]{:S(2)}) collective-permute-start(bf16[512,256]{1,0:T(8,128)(2,1)S(1)} %copy-done.2), channel_id=1, source_target_pairs={{0,2},{2,4},{4,6},{6,0},{1,3},{3,5},{5,7},{7,1},{8,10},{10,12},{12... | collective-permute-start | bytes 786440 | tf_op jit(solution)/shard_map/ppermute | solution.py:577
  25.5 1.5 %collective-permute-start.5 = (bf16[512,256]{1,0:T(8,128)(2,1)S(1)}, bf16[512,256]{1,0:T(8,128)(2,1)S(1)}, u32[]{:S(2)}, u32[]{:S(2)}) collective-permute-start(bf16[512,256]{1,0:T(8,128)(2,1)S(1)} %copy-done.3), channel_id=1, source_target_pairs={{0,6},{2,0},{4,2},{6,4},{1,7},{3,1},{5,3},{7,5},{8,14},{10,8},{12,... | collective-permute-start | bytes 786440 | tf_op jit(solution)/shard_map/ppermute | solution.py:577
  27.0 1.3 %collective-permute-start.2 = (bf16[512,256]{1,0:T(8,128)(2,1)S(1)}, bf16[512,256]{1,0:T(8,128)(2,1)S(1)}, u32[]{:S(2)}, u32[]{:S(2)}) collective-permute-start(bf16[512,256]{1,0:T(8,128)(2,1)S(1)} %copy-done.2), channel_id=1, source_target_pairs={{0,6},{2,0},{4,2},{6,4},{1,7},{3,1},{5,3},{7,5},{8,14},{10,8},{12,... | collective-permute-start | bytes 786440 | tf_op jit(solution)/shard_map/ppermute | solution.py:577
  28.2 0.2 collective-permute-start.4
  28.4 4.9 %collective-permute-done.1.refs_3_ = bf16[512,256]{1,0:T(8,128)(2,1)S(1)} collective-permute-done((bf16[512,256]{1,0:T(8,128)(2,1)S(1)}, bf16[512,256]{1,0:T(8,128)(2,1)S(1)}, u32[]{:S(2)}, u32[]{:S(2)}) %collective-permute-start.1) | collective-permute-done | bytes 262176 | tf_op jit(solution)/shard_map/ppermute | solution.py:577
  33.4 0.0 collective-permute-start.3
  33.4 0.0 collective-permute-done.5.refs_8_
  33.4 2.7 %collective-permute-start.6 = (bf16[512,256]{1,0:T(8,128)(2,1)S(1)}, bf16[512,256]{1,0:T(8,128)(2,1)S(1)}, u32[]{:S(2)}, u32[]{:S(2)}) collective-permute-start(bf16[512,256]{1,0:T(8,128)(2,1)S(1)} %collective-permute-done.5.refs_8_), channel_id=1, source_target_pairs={{0,6},{2,0},{4,2},{6,4},{1,7},{3,1},{5,3},{7,5},{8,14},{10,8},{12,... | collective-permute-start | bytes 786440 | tf_op jit(solution)/shard_map/ppermute | solution.py:577
  36.0 0.7 broadcast_in_dim.4.refs_4_
  36.7 3.8 %shard_map.164 = (f32[256,512]{1,0:T(8,128)}, f32[256,512]{1,0:T(8,128)}, bf16[128,1024]{1,0:T(8,128)(2,1)}, bf16[128,1024]{1,0:T(8,128)(2,1)}, f32[2,512]{1,0:T(2,128)}, /*index=5*/f32[1,128]{1,0:T(1,128)}) custom-call(f32[2,32,16,64]{3,2,1,0:T(8,128)} %bitcast.10, f32[2,32,16,64]{3,2,1,0:T(8,128)} %refs_1_.1, f32[32,64]{1,0:T(8,128)} %refs_2_.1, ...), custom_call_target="tpu_custom_call" | custom-call | flops 1000000000 | bytes 1048576 | tf_op jit(solution)/shard_map/pallas_call | solution.py:67
  40.5 0.0 collective-permute-done.refs_1_
  40.5 0.0 copy-start.1
  40.5 0.0 copy-start
  40.6 0.0 collective-permute-done.2.refs_4_
  40.6 0.0 collective-permute-done.4.refs_7_
  40.6 4.0 %collective-permute-done.3.refs_5_ = bf16[512,256]{1,0:T(8,128)(2,1)S(1)} collective-permute-done((bf16[512,256]{1,0:T(8,128)(2,1)S(1)}, bf16[512,256]{1,0:T(8,128)(2,1)S(1)}, u32[]{:S(2)}, u32[]{:S(2)}) %collective-permute-start.3) | collective-permute-done | bytes 262176 | tf_op jit(solution)/shard_map/ppermute | solution.py:577
  44.6 0.0 collective-permute-done.6.refs_9_
  44.6 5.7 %shard_map.165 = (bf16[544,256]{1,0:T(8,128)(2,1)}, f32[512,128]{1,0:T(8,128)}, f32[512,128]{1,0:T(8,128)}, f32[8,512]{1,0:T(8,128)}, bf16[512,128]{1,0:T(8,128)(2,1)S(1)}) custom-call(bf16[4,72,2048]{2,1,0:T(8,128)(2,1)S(1)} %all_to_all.5.refs_0_, bf16[4,72,2048]{2,1,0:T(8,128)(2,1)S(1)} %collective-permute-done.refs_1_, bf16[512,256]{1,0:T(8,128)(2,1)S(1)} %copy-done.2, ...), custom_call_target="tpu_custom_call" | custom-call | flops 3000000000 | bytes 1048576 | tf_op jit(solution)/shard_map/pallas_call | solution.py:67
  50.3 0.1 collective-permute-start.13
  50.4 1.5 %collective-permute-start.17 = (bf16[544,256]{1,0:T(8,128)(2,1)}, bf16[544,256]{1,0:T(8,128)(2,1)S(1)}, u32[]{:S(2)}, u32[]{:S(2)}) collective-permute-start(bf16[544,256]{1,0:T(8,128)(2,1)} %get-tuple-element.61.refs_0_), channel_id=1, source_target_pairs={{0,224},{32,0},{64,32},{96,64},{128,96},{160,128},{192,160},{224,1... | collective-permute-start | bytes 835592 | tf_op jit(solution)/shard_map/ppermute | solution.py:577
  51.9 2.4 %collective-permute-start.10 = (bf16[512,512]{1,0:T(8,128)(2,1)S(1)}, bf16[512,512]{1,0:T(8,128)(2,1)S(1)}, u32[]{:S(2)}, u32[]{:S(2)}) collective-permute-start(bf16[512,512]{1,0:T(8,128)(2,1)S(1)} %copy-done.1), channel_id=1, source_target_pairs={{0,6},{2,0},{4,2},{6,4},{1,7},{3,1},{5,3},{7,5},{8,14},{10,8},{12,... | collective-permute-start | bytes 1572872 | tf_op jit(solution)/shard_map/ppermute | solution.py:577
  54.3 3.7 %collective-permute-done.13.refs_0_.refs_12_ = bf16[544,256]{1,0:T(8,128)(2,1)S(1)} collective-permute-done((bf16[544,256]{1,0:T(8,128)(2,1)}, bf16[544,256]{1,0:T(8,128)(2,1)S(1)}, u32[]{:S(2)}, u32[]{:S(2)}) %collective-permute-start.13) | collective-permute-done | bytes 278560 | tf_op jit(solution)/shard_map/ppermute | solution.py:577
  58.0 1.5 %collective-permute-start.14 = (bf16[544,256]{1,0:T(8,128)(2,1)S(1)}, bf16[544,256]{1,0:T(8,128)(2,1)S(1)}, u32[]{:S(2)}, u32[]{:S(2)}) collective-permute-start(bf16[544,256]{1,0:T(8,128)(2,1)S(1)} %collective-permute-done.13.refs_0_.refs_12_), channel_id=1, source_target_pairs={{0,32},{32,64},{64,96},{96,128},{128,160},{160,192},{192,224},{224... | collective-permute-start | bytes 835592 | tf_op jit(solution)/shard_map/ppermute | solution.py:577
  59.5 0.6 collective-permute-start.7
  60.1 0.0 collective-permute-done.17.refs_1_.refs_7_
  60.1 0.0 collective-permute-start.18
  60.1 4.4 %collective-permute-done.14.refs_0_.refs_11_ = bf16[544,256]{1,0:T(8,128)(2,1)S(1)} collective-permute-done((bf16[544,256]{1,0:T(8,128)(2,1)S(1)}, bf16[544,256]{1,0:T(8,128)(2,1)S(1)}, u32[]{:S(2)}, u32[]{:S(2)}) %collective-permute-start.14) | collective-permute-done | bytes 278560 | tf_op jit(solution)/shard_map/ppermute | solution.py:577
  64.5 3.0 %collective-permute-start.15 = (bf16[544,256]{1,0:T(8,128)(2,1)S(1)}, bf16[544,256]{1,0:T(8,128)(2,1)S(1)}, u32[]{:S(2)}, u32[]{:S(2)}) collective-permute-start(bf16[544,256]{1,0:T(8,128)(2,1)S(1)} %collective-permute-done.14.refs_0_.refs_11_), channel_id=1, source_target_pairs={{0,32},{32,64},{64,96},{96,128},{128,160},{160,192},{192,224},{224... | collective-permute-start | bytes 835592 | tf_op jit(solution)/shard_map/ppermute | solution.py:577
  67.5 0.0 collective-permute-done.18.refs_1_.refs_8_
  67.5 0.0 collective-permute-start.19
  67.5 0.7 collective-permute-start.11
  68.2 0.0 collective-permute-done.10.refs_5_
  68.2 2.0 %collective-permute-start.8 = (bf16[512,512]{1,0:T(8,128)(2,1)S(1)}, bf16[512,512]{1,0:T(8,128)(2,1)S(1)}, u32[]{:S(2)}, u32[]{:S(2)}) collective-permute-start(bf16[512,512]{1,0:T(8,128)(2,1)S(1)} %copy-done), channel_id=1, source_target_pairs={{0,6},{2,0},{4,2},{6,4},{1,7},{3,1},{5,3},{7,5},{8,14},{10,8},{12,... | collective-permute-start | bytes 1572872 | tf_op jit(solution)/shard_map/ppermute | solution.py:577
  70.2 2.3 %collective-permute-done.7.refs_1_ = bf16[512,512]{1,0:T(8,128)(2,1)S(1)} collective-permute-done((bf16[512,512]{1,0:T(8,128)(2,1)S(1)}, bf16[512,512]{1,0:T(8,128)(2,1)S(1)}, u32[]{:S(2)}, u32[]{:S(2)}) %collective-permute-start.7) | collective-permute-done | bytes 524320 | tf_op jit(solution)/shard_map/ppermute | solution.py:577
  72.5 0.6 collective-permute-start.12
  73.1 0.0 collective-permute-done.15.refs_0_.refs_10_
  73.1 0.9 collective-permute-start.9
  73.9 0.4 collective-permute-done.19.refs_1_.refs_9_
  74.4 0.2 collective-permute-start.16
  74.6 2.9 %shard_map.166 = (f32[512,128]{1,0:T(8,128)S(1)}, f32[512,128]{1,0:T(8,128)S(1)}, f32[512,128]{1,0:T(8,128)S(1)}) custom-call(bf16[544,256]{1,0:T(8,128)(2,1)} %get-tuple-element.61.refs_0_, bf16[512,128]{1,0:T(8,128)(2,1)S(1)} %get-tuple-element.68.refs_1_.refs_2_.refs_13_), custom_call_target="tpu_custom_call" | custom-call | flops 268435456 | bytes 1048576 | tf_op jit(solution)/shard_map/pallas_call | solution.py:67
  77.5 3.7 %shard_map.167 = (f32[512,128]{1,0:T(8,128)S(1)}, f32[512,128]{1,0:T(8,128)S(1)}, f32[512,128]{1,0:T(8,128)S(1)}) custom-call(bf16[544,256]{1,0:T(8,128)(2,1)S(1)} %collective-permute-done.13.refs_0_.refs_12_, bf16[544,256]{1,0:T(8,128)(2,1)S(1)} %collective-permute-done.17.refs_1_.refs_7_, ...), custom_call_target="tpu_custom_call", output_to_operand_aliasing={{0}: (3, {}), {1}: (4, {}), {2}: (5, {})} | custom-call | flops 536870912 | bytes 1048576 | tf_op jit(solution)/shard_map/pallas_call | solution.py:67
  81.2 3.9 %shard_map.168 = (f32[512,128]{1,0:T(8,128)S(1)}, f32[512,128]{1,0:T(8,128)S(1)}, f32[512,128]{1,0:T(8,128)S(1)}) custom-call(bf16[544,256]{1,0:T(8,128)(2,1)S(1)} %collective-permute-done.14.refs_0_.refs_11_, bf16[544,256]{1,0:T(8,128)(2,1)S(1)} %collective-permute-done.18.refs_1_.refs_8_, ...), custom_call_target="tpu_custom_call", output_to_operand_aliasing={{0}: (3, {}), {1}: (4, {}), {2}: (5, {})} | custom-call | flops 536870912 | bytes 1048576 | tf_op jit(solution)/shard_map/pallas_call | solution.py:67
  85.1 3.7 %shard_map.169 = (f32[512,128]{1,0:T(8,128)S(1)}, f32[512,128]{1,0:T(8,128)S(1)}, f32[512,128]{1,0:T(8,128)S(1)}) custom-call(bf16[544,256]{1,0:T(8,128)(2,1)S(1)} %collective-permute-done.15.refs_0_.refs_10_, bf16[544,256]{1,0:T(8,128)(2,1)S(1)} %collective-permute-done.19.refs_1_.refs_9_, ...), custom_call_target="tpu_custom_call", output_to_operand_aliasing={{0}: (3, {}), {1}: (4, {}), {2}: (5, {})} | custom-call | flops 536870912 | bytes 1048576 | tf_op jit(solution)/shard_map/pallas_call | solution.py:67
  88.9 0.0 collective-permute-done.16.refs_0_
  88.9 2.7 %shard_map.170 = (bf16[128,256]{1,0:T(8,128)(2,1)S(1)}, bf16[128,256]{1,0:T(8,128)(2,1)S(1)}, bf16[128,256]{1,0:T(8,128)(2,1)S(1)}, bf16[128,256]{1,0:T(8,128)(2,1)S(1)}) custom-call(bf16[544,256]{1,0:T(8,128)(2,1)S(1)} %collective-permute-done.16.refs_0_, f32[512,128]{1,0:T(8,128)} %get-tuple-element.64.refs_1_, f32[512,128]{1,0:T(8,128)} %get-tuple-element.65.refs_2_, ...), custom_call_target="tpu_custom_call" | custom-call | flops 536870912 | bytes 1048576 | tf_op jit(solution)/shard_map/pallas_call | solution.py:67
  91.6 0.4 collective-permute-start.20
  92.0 0.0 collective-permute-done.11.refs_6_
  92.0 2.4 %collective-permute-start.21 = (bf16[128,256]{1,0:T(8,128)(2,1)S(1)}, bf16[128,256]{1,0:T(8,128)(2,1)S(1)}, u32[]{:S(2)}, u32[]{:S(2)}) collective-permute-start(bf16[128,256]{1,0:T(8,128)(2,1)S(1)} %get-tuple-element.83), channel_id=1, source_target_pairs={{0,24},{8,0},{16,8},{24,16},{1,25},{9,1},{17,9},{25,17},{2,26},{10... | collective-permute-start | bytes 196616 | tf_op jit(solution)/shard_map/ppermute | solution.py:577
  94.4 0.0 collective-permute-done.8.refs_2_
  94.4 0.0 collective-permute-start.22
  94.4 0.0 collective-permute-done.12.refs_7_
  94.4 0.5 collective-permute-done.9.refs_3_
  94.9 1.4 %collective-permute-done.20.refs_9_ = bf16[128,256]{1,0:T(8,128)(2,1)S(1)} collective-permute-done((bf16[128,256]{1,0:T(8,128)(2,1)S(1)}, bf16[128,256]{1,0:T(8,128)(2,1)S(1)}, u32[]{:S(2)}, u32[]{:S(2)}) %collective-permute-start.20) | collective-permute-done | bytes 65568 | tf_op jit(solution)/shard_map/ppermute | solution.py:577
  96.3 0.0 collective-permute-done.21.refs_10_
  96.3 2.7 %collective-permute-done.22.refs_11_ = bf16[128,256]{1,0:T(8,128)(2,1)S(1)} collective-permute-done((bf16[128,256]{1,0:T(8,128)(2,1)S(1)}, bf16[128,256]{1,0:T(8,128)(2,1)S(1)}, u32[]{:S(2)}, u32[]{:S(2)}) %collective-permute-start.22) | collective-permute-done | bytes 65568 | tf_op jit(solution)/shard_map/ppermute | solution.py:577
  99.0 1.5 %shard_map.171 = (bf16[64,2048]{1,0:T(8,128)(2,1)}, f32[64,2048]{1,0:T(8,128)S(1)}) custom-call(bf16[512,512]{1,0:T(8,128)(2,1)S(1)} %copy-done, bf16[512,512]{1,0:T(8,128)(2,1)S(1)} %collective-permute-done.7.refs_1_, bf16[512,512]{1,0:T(8,128)(2,1)S(1)} %collective-permute-done.8.refs_2_, bf16[512,512]{1,0:T(8,128)(2,1)S(1)} %collective-permute-done.9.refs_3_, ...), custom_call_target="tpu_custom_call" | custom-call | flops 536870912 | bytes 1048576 | tf_op jit(solution)/shard_map/pallas_call | solution.py:67
  100.6 6.4 %collective-permute-start.23 = (bf16[64,2048]{1,0:T(8,128)(2,1)}, bf16[64,2048]{1,0:T(8,128)(2,1)S(1)}, u32[]{:S(2)}, u32[]{:S(2)}) collective-permute-start(bf16[64,2048]{1,0:T(8,128)(2,1)} %get-tuple-element.86), channel_id=1, source_target_pairs={{0,1},{1,0},{2,3},{3,2},{4,5},{5,4},{6,7},{7,6},{8,9},{9,8},{10,11... | collective-permute-start | bytes 786440 | tf_op jit(solution)/shard_map/ppermute | solution.py:577
  107.0 1.4 %collective-permute-done.23 = bf16[64,2048]{1,0:T(8,128)(2,1)S(1)} collective-permute-done((bf16[64,2048]{1,0:T(8,128)(2,1)}, bf16[64,2048]{1,0:T(8,128)(2,1)S(1)}, u32[]{:S(2)}, u32[]{:S(2)}) %collective-permute-start.23) | collective-permute-done | bytes 262176 | tf_op jit(solution)/shard_map/ppermute | solution.py:577
  108.4 0.8 fusion
  (6 shorter events, 0.0 us)
Async XLA Ops:
  2.5 21.8 %copy-start.2 = (bf16[512,256]{1,0:T(8,128)(2,1)S(1)}, bf16[512,256]{1,0:T(8,128)(2,1)}, u32[]{:S(2)}) copy-start(bf16[512,256]{1,0:T(8,128)(2,1)} %get-tuple-element.54.refs_2_) | copy-start | bytes 786436
  2.5 23.0 %copy-start.3 = (bf16[512,256]{1,0:T(8,128)(2,1)S(1)}, bf16[512,256]{1,0:T(8,128)(2,1)}, u32[]{:S(2)}) copy-start(bf16[512,256]{1,0:T(8,128)(2,1)} %get-tuple-element.55.refs_6_) | copy-start | bytes 786436
  2.5 33.6 %copy-start.4 = (f32[32]{0:T(128)S(1)}, f32[32]{0:T(128)}, u32[]{:S(2)}) copy-start(f32[32]{0:T(128)} %param.24) | copy-start | bytes 388
  22.5 18.1 %collective-permute-start = (bf16[4,72,2048]{2,1,0:T(8,128)(2,1)S(1)}, bf16[4,72,2048]{2,1,0:T(8,128)(2,1)S(1)}, u32[]{:S(2)}, u32[]{:S(2)}) collective-permute-start(bf16[4,72,2048]{2,1,0:T(8,128)(2,1)S(1)} %all_to_all.5.refs_0_), channel_id=1, source_target_pairs={{0,1},{1,0},{2,3},{3,2},{4,5},{5,4},{6,7},{7,6},{8,9},{9,8},{10,11... | collective-permute-start | bytes 3538952 | tf_op jit(solution)/shard_map/ppermute | solution.py:577
  24.3 9.1 %collective-permute-start.1 = (bf16[512,256]{1,0:T(8,128)(2,1)S(1)}, bf16[512,256]{1,0:T(8,128)(2,1)S(1)}, u32[]{:S(2)}, u32[]{:S(2)}) collective-permute-start(bf16[512,256]{1,0:T(8,128)(2,1)S(1)} %copy-done.2), channel_id=1, source_target_pairs={{0,2},{2,4},{4,6},{6,0},{1,3},{3,5},{5,7},{7,1},{8,10},{10,12},{12... | collective-permute-start | bytes 786440 | tf_op jit(solution)/shard_map/ppermute | solution.py:577
  25.5 7.9 %collective-permute-start.5 = (bf16[512,256]{1,0:T(8,128)(2,1)S(1)}, bf16[512,256]{1,0:T(8,128)(2,1)S(1)}, u32[]{:S(2)}, u32[]{:S(2)}) collective-permute-start(bf16[512,256]{1,0:T(8,128)(2,1)S(1)} %copy-done.3), channel_id=1, source_target_pairs={{0,6},{2,0},{4,2},{6,4},{1,7},{3,1},{5,3},{7,5},{8,14},{10,8},{12,... | collective-permute-start | bytes 786440 | tf_op jit(solution)/shard_map/ppermute | solution.py:577
  27.0 13.6 %collective-permute-start.2 = (bf16[512,256]{1,0:T(8,128)(2,1)S(1)}, bf16[512,256]{1,0:T(8,128)(2,1)S(1)}, u32[]{:S(2)}, u32[]{:S(2)}) collective-permute-start(bf16[512,256]{1,0:T(8,128)(2,1)S(1)} %copy-done.2), channel_id=1, source_target_pairs={{0,6},{2,0},{4,2},{6,4},{1,7},{3,1},{5,3},{7,5},{8,14},{10,8},{12,... | collective-permute-start | bytes 786440 | tf_op jit(solution)/shard_map/ppermute | solution.py:577
  28.2 12.3 %collective-permute-start.4 = (bf16[512,256]{1,0:T(8,128)(2,1)S(1)}, bf16[512,256]{1,0:T(8,128)(2,1)S(1)}, u32[]{:S(2)}, u32[]{:S(2)}) collective-permute-start(bf16[512,256]{1,0:T(8,128)(2,1)S(1)} %copy-done.3), channel_id=1, source_target_pairs={{0,2},{2,4},{4,6},{6,0},{1,3},{3,5},{5,7},{7,1},{8,10},{10,12},{12... | collective-permute-start | bytes 786440 | tf_op jit(solution)/shard_map/ppermute | solution.py:577
  33.4 11.2 %collective-permute-start.3 = (bf16[512,256]{1,0:T(8,128)(2,1)S(1)}, bf16[512,256]{1,0:T(8,128)(2,1)S(1)}, u32[]{:S(2)}, u32[]{:S(2)}) collective-permute-start(bf16[512,256]{1,0:T(8,128)(2,1)S(1)} %collective-permute-done.1.refs_3_), channel_id=1, source_target_pairs={{0,2},{2,4},{4,6},{6,0},{1,3},{3,5},{5,7},{7,1},{8,10},{10,12},{12... | collective-permute-start | bytes 786440 | tf_op jit(solution)/shard_map/ppermute | solution.py:577
  33.4 11.2 %collective-permute-start.6 = (bf16[512,256]{1,0:T(8,128)(2,1)S(1)}, bf16[512,256]{1,0:T(8,128)(2,1)S(1)}, u32[]{:S(2)}, u32[]{:S(2)}) collective-permute-start(bf16[512,256]{1,0:T(8,128)(2,1)S(1)} %collective-permute-done.5.refs_8_), channel_id=1, source_target_pairs={{0,6},{2,0},{4,2},{6,4},{1,7},{3,1},{5,3},{7,5},{8,14},{10,8},{12,... | collective-permute-start | bytes 786440 | tf_op jit(solution)/shard_map/ppermute | solution.py:577
  40.5 11.4 %copy-start.1 = (bf16[512,512]{1,0:T(8,128)(2,1)S(1)}, bf16[512,512]{1,0:T(8,128)(2,1)}, u32[]{:S(2)}) copy-start(bf16[512,512]{1,0:T(8,128)(2,1)} %refs_4_.2) | copy-start | bytes 1572868
  40.5 18.9 %copy-start = (bf16[512,512]{1,0:T(8,128)(2,1)S(1)}, bf16[512,512]{1,0:T(8,128)(2,1)}, u32[]{:S(2)}) copy-start(bf16[512,512]{1,0:T(8,128)(2,1)} %refs_0_.2) | copy-start | bytes 1572868
  50.3 7.6 %collective-permute-start.13 = (bf16[544,256]{1,0:T(8,128)(2,1)}, bf16[544,256]{1,0:T(8,128)(2,1)S(1)}, u32[]{:S(2)}, u32[]{:S(2)}) collective-permute-start(bf16[544,256]{1,0:T(8,128)(2,1)} %get-tuple-element.61.refs_0_), channel_id=1, source_target_pairs={{0,32},{32,64},{64,96},{96,128},{128,160},{160,192},{192,224},{224... | collective-permute-start | bytes 835592 | tf_op jit(solution)/shard_map/ppermute | solution.py:577
  50.4 9.7 %collective-permute-start.17 = (bf16[544,256]{1,0:T(8,128)(2,1)}, bf16[544,256]{1,0:T(8,128)(2,1)S(1)}, u32[]{:S(2)}, u32[]{:S(2)}) collective-permute-start(bf16[544,256]{1,0:T(8,128)(2,1)} %get-tuple-element.61.refs_0_), channel_id=1, source_target_pairs={{0,224},{32,0},{64,32},{96,64},{128,96},{160,128},{192,160},{224,1... | collective-permute-start | bytes 835592 | tf_op jit(solution)/shard_map/ppermute | solution.py:577
  51.9 16.3 %collective-permute-start.10 = (bf16[512,512]{1,0:T(8,128)(2,1)S(1)}, bf16[512,512]{1,0:T(8,128)(2,1)S(1)}, u32[]{:S(2)}, u32[]{:S(2)}) collective-permute-start(bf16[512,512]{1,0:T(8,128)(2,1)S(1)} %copy-done.1), channel_id=1, source_target_pairs={{0,6},{2,0},{4,2},{6,4},{1,7},{3,1},{5,3},{7,5},{8,14},{10,8},{12,... | collective-permute-start | bytes 1572872 | tf_op jit(solution)/shard_map/ppermute | solution.py:577
  58.0 6.5 %collective-permute-start.14 = (bf16[544,256]{1,0:T(8,128)(2,1)S(1)}, bf16[544,256]{1,0:T(8,128)(2,1)S(1)}, u32[]{:S(2)}, u32[]{:S(2)}) collective-permute-start(bf16[544,256]{1,0:T(8,128)(2,1)S(1)} %collective-permute-done.13.refs_0_.refs_12_), channel_id=1, source_target_pairs={{0,32},{32,64},{64,96},{96,128},{128,160},{160,192},{192,224},{224... | collective-permute-start | bytes 835592 | tf_op jit(solution)/shard_map/ppermute | solution.py:577
  59.5 13.0 %collective-permute-start.7 = (bf16[512,512]{1,0:T(8,128)(2,1)S(1)}, bf16[512,512]{1,0:T(8,128)(2,1)S(1)}, u32[]{:S(2)}, u32[]{:S(2)}) collective-permute-start(bf16[512,512]{1,0:T(8,128)(2,1)S(1)} %copy-done), channel_id=1, source_target_pairs={{0,2},{2,4},{4,6},{6,0},{1,3},{3,5},{5,7},{7,1},{8,10},{10,12},{12... | collective-permute-start | bytes 1572872 | tf_op jit(solution)/shard_map/ppermute | solution.py:577
  60.1 7.3 %collective-permute-start.18 = (bf16[544,256]{1,0:T(8,128)(2,1)S(1)}, bf16[544,256]{1,0:T(8,128)(2,1)S(1)}, u32[]{:S(2)}, u32[]{:S(2)}) collective-permute-start(bf16[544,256]{1,0:T(8,128)(2,1)S(1)} %collective-permute-done.17.refs_1_.refs_7_), channel_id=1, source_target_pairs={{0,224},{32,0},{64,32},{96,64},{128,96},{160,128},{192,160},{224,1... | collective-permute-start | bytes 835592 | tf_op jit(solution)/shard_map/ppermute | solution.py:577
  64.5 8.6 %collective-permute-start.15 = (bf16[544,256]{1,0:T(8,128)(2,1)S(1)}, bf16[544,256]{1,0:T(8,128)(2,1)S(1)}, u32[]{:S(2)}, u32[]{:S(2)}) collective-permute-start(bf16[544,256]{1,0:T(8,128)(2,1)S(1)} %collective-permute-done.14.refs_0_.refs_11_), channel_id=1, source_target_pairs={{0,32},{32,64},{64,96},{96,128},{128,160},{160,192},{192,224},{224... | collective-permute-start | bytes 835592 | tf_op jit(solution)/shard_map/ppermute | solution.py:577
  67.5 6.9 %collective-permute-start.19 = (bf16[544,256]{1,0:T(8,128)(2,1)S(1)}, bf16[544,256]{1,0:T(8,128)(2,1)S(1)}, u32[]{:S(2)}, u32[]{:S(2)}) collective-permute-start(bf16[544,256]{1,0:T(8,128)(2,1)S(1)} %collective-permute-done.18.refs_1_.refs_8_), channel_id=1, source_target_pairs={{0,224},{32,0},{64,32},{96,64},{128,96},{160,128},{192,160},{224,1... | collective-permute-start | bytes 835592 | tf_op jit(solution)/shard_map/ppermute | solution.py:577
  67.5 24.5 %collective-permute-start.11 = (bf16[512,512]{1,0:T(8,128)(2,1)S(1)}, bf16[512,512]{1,0:T(8,128)(2,1)S(1)}, u32[]{:S(2)}, u32[]{:S(2)}) collective-permute-start(bf16[512,512]{1,0:T(8,128)(2,1)S(1)} %copy-done.1), channel_id=1, source_target_pairs={{0,2},{2,4},{4,6},{6,0},{1,3},{3,5},{5,7},{7,1},{8,10},{10,12},{12... | collective-permute-start | bytes 1572872 | tf_op jit(solution)/shard_map/ppermute | solution.py:577
  68.2 26.2 %collective-permute-start.8 = (bf16[512,512]{1,0:T(8,128)(2,1)S(1)}, bf16[512,512]{1,0:T(8,128)(2,1)S(1)}, u32[]{:S(2)}, u32[]{:S(2)}) collective-permute-start(bf16[512,512]{1,0:T(8,128)(2,1)S(1)} %copy-done), channel_id=1, source_target_pairs={{0,6},{2,0},{4,2},{6,4},{1,7},{3,1},{5,3},{7,5},{8,14},{10,8},{12,... | collective-permute-start | bytes 1572872 | tf_op jit(solution)/shard_map/ppermute | solution.py:577
  72.5 21.9 %collective-permute-start.12 = (bf16[512,512]{1,0:T(8,128)(2,1)S(1)}, bf16[512,512]{1,0:T(8,128)(2,1)S(1)}, u32[]{:S(2)}, u32[]{:S(2)}) collective-permute-start(bf16[512,512]{1,0:T(8,128)(2,1)S(1)} %collective-permute-done.10.refs_5_), channel_id=1, source_target_pairs={{0,6},{2,0},{4,2},{6,4},{1,7},{3,1},{5,3},{7,5},{8,14},{10,8},{12,... | collective-permute-start | bytes 1572872 | tf_op jit(solution)/shard_map/ppermute | solution.py:577
  73.1 21.9 %collective-permute-start.9 = (bf16[512,512]{1,0:T(8,128)(2,1)S(1)}, bf16[512,512]{1,0:T(8,128)(2,1)S(1)}, u32[]{:S(2)}, u32[]{:S(2)}) collective-permute-start(bf16[512,512]{1,0:T(8,128)(2,1)S(1)} %collective-permute-done.7.refs_1_), channel_id=1, source_target_pairs={{0,2},{2,4},{4,6},{6,0},{1,3},{3,5},{5,7},{7,1},{8,10},{10,12},{12... | collective-permute-start | bytes 1572872 | tf_op jit(solution)/shard_map/ppermute | solution.py:577
  74.4 14.5 %collective-permute-start.16 = (bf16[544,256]{1,0:T(8,128)(2,1)S(1)}, bf16[544,256]{1,0:T(8,128)(2,1)S(1)}, u32[]{:S(2)}, u32[]{:S(2)}) collective-permute-start(bf16[544,256]{1,0:T(8,128)(2,1)S(1)} %collective-permute-done.15.refs_0_.refs_10_), channel_id=1, source_target_pairs={{0,32},{32,64},{64,96},{96,128},{128,160},{160,192},{192,224},{224... | collective-permute-start | bytes 835592 | tf_op jit(solution)/shard_map/ppermute | solution.py:577
  91.6 4.7 %collective-permute-start.20 = (bf16[128,256]{1,0:T(8,128)(2,1)S(1)}, bf16[128,256]{1,0:T(8,128)(2,1)S(1)}, u32[]{:S(2)}, u32[]{:S(2)}) collective-permute-start(bf16[128,256]{1,0:T(8,128)(2,1)S(1)} %get-tuple-element.82), channel_id=1, source_target_pairs={{0,8},{8,16},{16,24},{24,0},{1,9},{9,17},{17,25},{25,1},{2,10},{10... | collective-permute-start | bytes 196616 | tf_op jit(solution)/shard_map/ppermute | solution.py:577
  92.0 4.3 %collective-permute-start.21 = (bf16[128,256]{1,0:T(8,128)(2,1)S(1)}, bf16[128,256]{1,0:T(8,128)(2,1)S(1)}, u32[]{:S(2)}, u32[]{:S(2)}) collective-permute-start(bf16[128,256]{1,0:T(8,128)(2,1)S(1)} %get-tuple-element.83), channel_id=1, source_target_pairs={{0,24},{8,0},{16,8},{24,16},{1,25},{9,1},{17,9},{25,17},{2,26},{10... | collective-permute-start | bytes 196616 | tf_op jit(solution)/shard_map/ppermute | solution.py:577
  94.4 4.6 %collective-permute-start.22 = (bf16[128,256]{1,0:T(8,128)(2,1)S(1)}, bf16[128,256]{1,0:T(8,128)(2,1)S(1)}, u32[]{:S(2)}, u32[]{:S(2)}) collective-permute-start(bf16[128,256]{1,0:T(8,128)(2,1)S(1)} %get-tuple-element.84), channel_id=1, source_target_pairs={{0,16},{8,24},{16,0},{24,8},{1,17},{9,25},{17,1},{25,9},{2,18},{10... | collective-permute-start | bytes 196616 | tf_op jit(solution)/shard_map/ppermute | solution.py:577
  100.6 7.8 %collective-permute-start.23 = (bf16[64,2048]{1,0:T(8,128)(2,1)}, bf16[64,2048]{1,0:T(8,128)(2,1)S(1)}, u32[]{:S(2)}, u32[]{:S(2)}) collective-permute-start(bf16[64,2048]{1,0:T(8,128)(2,1)} %get-tuple-element.86), channel_id=1, source_target_pairs={{0,1},{1,0},{2,3},{3,2},{4,5},{5,4},{6,7},{7,6},{8,9},{9,8},{10,11... | collective-permute-start | bytes 786440 | tf_op jit(solution)/shard_map/ppermute | solution.py:577

commit v5 on v2

--- a/solution.py
+++ b/solution.py
@@ -540,14 +540,13 @@
 
 
 def out_body(
-    ready, send, a0, a3, a1, a2, b0, b1, b3, b2, r0, r3, r1, r2, send_ref, keep_ref, lhs_ref, sum_ref
+    a0, a3, a1, a2, b0, b1, b3, b2, r0, r3, r1, r2, send_ref, keep_ref, lhs_ref, sum_ref
 ):
     x, y, c = lax.axis_index("x"), lax.axis_index("y"), lax.axis_index("c")
     for step, ref in ((0, r0), (3, r3), (1, r1), (2, r2)):
         at = pl.multiple_of(((y + step) % 4) * BLOCK, BLOCK)
         lhs_ref[:, pl.ds(at, BLOCK)] = ref[:, :BLOCK]
         lhs_ref[:, pl.ds(ROWS + at, BLOCK)] = ref[:, BLOCK:]
-    ready(*range(8))
     for step, scan_w, attend_w in ((0, a0, b0), (3, a3, b3), (1, a1, b1), (2, a2, b2)):
         total = mm(lhs_ref[:, :ROWS], scan_w[...]) + mm(lhs_ref[:, ROWS:], attend_w[...])
         sum_ref[:, pl.ds(pl.multiple_of(((x + step) % 4) * ROWS, ROWS), ROWS)] = total
@@ -559,12 +558,10 @@
     return staged(
         out_body,
         [shape((64, 2048), bf16)],
-        list(pieces),
+        [],
         [pltpu.VMEM((BLOCK, 1024), bf16), pltpu.VMEM((BLOCK, 2048), f32)],
         flops=BLOCK * 1024 * 2048 * 2,
-        lazy=True,
-        free=(1, 2, 3, 5, 6, 7),
-        vin=tuple(recv),
+        vin=tuple(pieces) + tuple(recv),
         vout=(shape((64, 2048), f32),),
     )
 

time: 110 us -> 109 us (level)
  Pallas kernels: 31.6 us -> 30.3 us
    pallas_call x9, Pallas kernels: 31.6 us -> 30.3 us  [staged(): pl.pallas_call(kernel, out_shape=tuple((pltpu.HBM(o.shape, o.dtype) for o...]
where the time goes in v5:
time: 109 us
  starting transfers between devices  31.2 us (29%)
  Pallas kernels  30.3 us (28%)
  waiting for transfers between devices  25.8 us (24%)
  blocking collectives  20 us (18%)
    ppermute x24, starting transfers between devices, shift(): return lax.ppermute(a, axis, [(i, (i + by) % n) for i in range(n)])  31.2 us
    pallas_call x9, Pallas kernels, staged(): pl.pallas_call(kernel, out_shape=tuple((pltpu.HBM(o.shape, o.dtype) for o...  30.3 us
    ppermute x24, waiting for transfers between devices, shift(): return lax.ppermute(a, axis, [(i, (i + by) % n) for i in range(n)])  25.8 us
    all_to_all x1, blocking collectives, exchange(): return lax.all_to_all(a, axis, split_axis=0, concat_axis=0, tiled=True)  20 us
  transfers between devices with their start and end apart: 24, of which 10 were waited for; matrix products, arithmetic and copies ran while one was open for 1% of the time, Pallas kernels for 19%

profile of v5, /device:TPU:225, one launch (start us, length us, event | category | flops | bytes accessed | tf_op | source)
XLA Modules:
  0.0 108.9 jit_solution(8248879048105786722)
XLA Ops:
  0.0 2.5 %shard_map.163 = (bf16[4,72,2048]{2,1,0:T(8,128)(2,1)}, bf16[512,256]{1,0:T(8,128)(2,1)}, bf16[512,256]{1,0:T(8,128)(2,1)}) custom-call(bf16[1,64,2048]{2,1,0:T(8,128)(2,1)} %refs_0_.1, f32[1,2048]{1,0:T(1,128)} %bitcast.8, f32[32,128]{1,0:T(8,128)} %bitcast.7, bf16[4,128]{1,0:T(4,128)(2,1)} %bitcast.9, bf16[512,512]{1,0:T(8,128)(2,1)} %refs_4_.1, ...), custom_call_target="tpu_custom_call" | custom-call | flops 1000000 | bytes 1048576 | tf_op jit(solution)/shard_map/pallas_call | solution.py:67
  2.5 0.0 copy-start.2
  2.5 0.0 copy-start.4
  2.5 20.0 %all_to_all.5.refs_0_ = bf16[4,72,2048]{2,1,0:T(8,128)(2,1)S(1)} all-to-all(bf16[4,72,2048]{2,1,0:T(8,128)(2,1)} %get-tuple-element.46), channel_id=1, replica_groups=mesh['z'=8,'y'=4,'x'=4,'c'=2] {'y'}, dimensions={0} | all-to-all | bytes 2359296 | tf_op jit(solution)/shard_map/all_to_all | solution.py:598
  22.5 1.8 %collective-permute-start = (bf16[4,72,2048]{2,1,0:T(8,128)(2,1)S(1)}, bf16[4,72,2048]{2,1,0:T(8,128)(2,1)S(1)}, u32[]{:S(2)}, u32[]{:S(2)}) collective-permute-start(bf16[4,72,2048]{2,1,0:T(8,128)(2,1)S(1)} %all_to_all.5.refs_0_), channel_id=1, source_target_pairs={{0,1},{1,0},{2,3},{3,2},{4,5},{5,4},{6,7},{7,6},{8,9},{9,8},{10,11... | collective-permute-start | bytes 3538952 | tf_op jit(solution)/shard_map/ppermute | solution.py:571
  24.3 1.2 %collective-permute-start.1 = (bf16[512,256]{1,0:T(8,128)(2,1)S(1)}, bf16[512,256]{1,0:T(8,128)(2,1)S(1)}, u32[]{:S(2)}, u32[]{:S(2)}) collective-permute-start(bf16[512,256]{1,0:T(8,128)(2,1)S(1)} %copy-done.2), channel_id=1, source_target_pairs={{0,2},{2,4},{4,6},{6,0},{1,3},{3,5},{5,7},{7,1},{8,10},{10,12},{12... | collective-permute-start | bytes 786440 | tf_op jit(solution)/shard_map/ppermute | solution.py:571
  25.5 1.5 %collective-permute-start.5 = (bf16[512,256]{1,0:T(8,128)(2,1)S(1)}, bf16[512,256]{1,0:T(8,128)(2,1)S(1)}, u32[]{:S(2)}, u32[]{:S(2)}) collective-permute-start(bf16[512,256]{1,0:T(8,128)(2,1)S(1)} %copy-done.3), channel_id=1, source_target_pairs={{0,6},{2,0},{4,2},{6,4},{1,7},{3,1},{5,3},{7,5},{8,14},{10,8},{12,... | collective-permute-start | bytes 786440 | tf_op jit(solution)/shard_map/ppermute | solution.py:571
  27.0 1.3 %collective-permute-start.2 = (bf16[512,256]{1,0:T(8,128)(2,1)S(1)}, bf16[512,256]{1,0:T(8,128)(2,1)S(1)}, u32[]{:S(2)}, u32[]{:S(2)}) collective-permute-start(bf16[512,256]{1,0:T(8,128)(2,1)S(1)} %copy-done.2), channel_id=1, source_target_pairs={{0,6},{2,0},{4,2},{6,4},{1,7},{3,1},{5,3},{7,5},{8,14},{10,8},{12,... | collective-permute-start | bytes 786440 | tf_op jit(solution)/shard_map/ppermute | solution.py:571
  28.2 0.2 collective-permute-start.4
  28.4 4.9 %collective-permute-done.1.refs_3_ = bf16[512,256]{1,0:T(8,128)(2,1)S(1)} collective-permute-done((bf16[512,256]{1,0:T(8,128)(2,1)S(1)}, bf16[512,256]{1,0:T(8,128)(2,1)S(1)}, u32[]{:S(2)}, u32[]{:S(2)}) %collective-permute-start.1) | collective-permute-done | bytes 262176 | tf_op jit(solution)/shard_map/ppermute | solution.py:571
  33.4 0.0 collective-permute-start.3
  33.4 0.0 collective-permute-done.5.refs_8_
  33.4 2.7 %collective-permute-start.6 = (bf16[512,256]{1,0:T(8,128)(2,1)S(1)}, bf16[512,256]{1,0:T(8,128)(2,1)S(1)}, u32[]{:S(2)}, u32[]{:S(2)}) collective-permute-start(bf16[512,256]{1,0:T(8,128)(2,1)S(1)} %collective-permute-done.5.refs_8_), channel_id=1, source_target_pairs={{0,6},{2,0},{4,2},{6,4},{1,7},{3,1},{5,3},{7,5},{8,14},{10,8},{12,... | collective-permute-start | bytes 786440 | tf_op jit(solution)/shard_map/ppermute | solution.py:571
  36.0 0.7 broadcast_in_dim.4.refs_4_
  36.7 3.8 %shard_map.164 = (f32[256,512]{1,0:T(8,128)}, f32[256,512]{1,0:T(8,128)}, bf16[128,1024]{1,0:T(8,128)(2,1)}, bf16[128,1024]{1,0:T(8,128)(2,1)}, f32[2,512]{1,0:T(2,128)}, /*index=5*/f32[1,128]{1,0:T(1,128)}) custom-call(f32[2,32,16,64]{3,2,1,0:T(8,128)} %bitcast.10, f32[2,32,16,64]{3,2,1,0:T(8,128)} %refs_1_.1, f32[32,64]{1,0:T(8,128)} %refs_2_.1, ...), custom_call_target="tpu_custom_call" | custom-call | flops 1000000000 | bytes 1048576 | tf_op jit(solution)/shard_map/pallas_call | solution.py:67
  40.5 0.0 collective-permute-done.refs_1_
  40.5 0.0 copy-start.1
  40.5 0.0 copy-start
  40.6 0.0 collective-permute-done.2.refs_4_
  40.6 0.0 collective-permute-done.4.refs_7_
  40.6 4.0 %collective-permute-done.3.refs_5_ = bf16[512,256]{1,0:T(8,128)(2,1)S(1)} collective-permute-done((bf16[512,256]{1,0:T(8,128)(2,1)S(1)}, bf16[512,256]{1,0:T(8,128)(2,1)S(1)}, u32[]{:S(2)}, u32[]{:S(2)}) %collective-permute-start.3) | collective-permute-done | bytes 262176 | tf_op jit(solution)/shard_map/ppermute | solution.py:571
  44.6 0.0 collective-permute-done.6.refs_9_
  44.6 5.6 %shard_map.165 = (bf16[544,256]{1,0:T(8,128)(2,1)}, f32[512,128]{1,0:T(8,128)}, f32[512,128]{1,0:T(8,128)}, f32[8,512]{1,0:T(8,128)}, bf16[512,128]{1,0:T(8,128)(2,1)S(1)}) custom-call(bf16[4,72,2048]{2,1,0:T(8,128)(2,1)S(1)} %all_to_all.5.refs_0_, bf16[4,72,2048]{2,1,0:T(8,128)(2,1)S(1)} %collective-permute-done.refs_1_, bf16[512,256]{1,0:T(8,128)(2,1)S(1)} %copy-done.2, ...), custom_call_target="tpu_custom_call" | custom-call | flops 3000000000 | bytes 1048576 | tf_op jit(solution)/shard_map/pallas_call | solution.py:67
  50.2 0.1 collective-permute-start.13
  50.3 1.5 %collective-permute-start.17 = (bf16[544,256]{1,0:T(8,128)(2,1)}, bf16[544,256]{1,0:T(8,128)(2,1)S(1)}, u32[]{:S(2)}, u32[]{:S(2)}) collective-permute-start(bf16[544,256]{1,0:T(8,128)(2,1)} %get-tuple-element.61.refs_0_), channel_id=1, source_target_pairs={{0,224},{32,0},{64,32},{96,64},{128,96},{160,128},{192,160},{224,1... | collective-permute-start | bytes 835592 | tf_op jit(solution)/shard_map/ppermute | solution.py:571
  51.7 2.4 %collective-permute-start.10 = (bf16[512,512]{1,0:T(8,128)(2,1)S(1)}, bf16[512,512]{1,0:T(8,128)(2,1)S(1)}, u32[]{:S(2)}, u32[]{:S(2)}) collective-permute-start(bf16[512,512]{1,0:T(8,128)(2,1)S(1)} %copy-done.1), channel_id=1, source_target_pairs={{0,6},{2,0},{4,2},{6,4},{1,7},{3,1},{5,3},{7,5},{8,14},{10,8},{12,... | collective-permute-start | bytes 1572872 | tf_op jit(solution)/shard_map/ppermute | solution.py:571
  54.1 3.7 %collective-permute-done.13.refs_0_.refs_12_ = bf16[544,256]{1,0:T(8,128)(2,1)S(1)} collective-permute-done((bf16[544,256]{1,0:T(8,128)(2,1)}, bf16[544,256]{1,0:T(8,128)(2,1)S(1)}, u32[]{:S(2)}, u32[]{:S(2)}) %collective-permute-start.13) | collective-permute-done | bytes 278560 | tf_op jit(solution)/shard_map/ppermute | solution.py:571
  57.8 1.5 %collective-permute-start.14 = (bf16[544,256]{1,0:T(8,128)(2,1)S(1)}, bf16[544,256]{1,0:T(8,128)(2,1)S(1)}, u32[]{:S(2)}, u32[]{:S(2)}) collective-permute-start(bf16[544,256]{1,0:T(8,128)(2,1)S(1)} %collective-permute-done.13.refs_0_.refs_12_), channel_id=1, source_target_pairs={{0,32},{32,64},{64,96},{96,128},{128,160},{160,192},{192,224},{224... | collective-permute-start | bytes 835592 | tf_op jit(solution)/shard_map/ppermute | solution.py:571
  59.3 0.6 collective-permute-start.7
  60.0 0.0 collective-permute-done.17.refs_1_.refs_7_
  60.0 0.0 collective-permute-start.18
  60.0 4.4 %collective-permute-done.14.refs_0_.refs_11_ = bf16[544,256]{1,0:T(8,128)(2,1)S(1)} collective-permute-done((bf16[544,256]{1,0:T(8,128)(2,1)S(1)}, bf16[544,256]{1,0:T(8,128)(2,1)S(1)}, u32[]{:S(2)}, u32[]{:S(2)}) %collective-permute-start.14) | collective-permute-done | bytes 278560 | tf_op jit(solution)/shard_map/ppermute | solution.py:571
  64.3 3.0 %collective-permute-start.15 = (bf16[544,256]{1,0:T(8,128)(2,1)S(1)}, bf16[544,256]{1,0:T(8,128)(2,1)S(1)}, u32[]{:S(2)}, u32[]{:S(2)}) collective-permute-start(bf16[544,256]{1,0:T(8,128)(2,1)S(1)} %collective-permute-done.14.refs_0_.refs_11_), channel_id=1, source_target_pairs={{0,32},{32,64},{64,96},{96,128},{128,160},{160,192},{192,224},{224... | collective-permute-start | bytes 835592 | tf_op jit(solution)/shard_map/ppermute | solution.py:571
  67.3 0.0 collective-permute-done.18.refs_1_.refs_8_
  67.3 0.0 collective-permute-start.19
  67.3 0.7 collective-permute-start.11
  68.0 0.0 collective-permute-done.10.refs_5_
  68.0 2.0 %collective-permute-start.8 = (bf16[512,512]{1,0:T(8,128)(2,1)S(1)}, bf16[512,512]{1,0:T(8,128)(2,1)S(1)}, u32[]{:S(2)}, u32[]{:S(2)}) collective-permute-start(bf16[512,512]{1,0:T(8,128)(2,1)S(1)} %copy-done), channel_id=1, source_target_pairs={{0,6},{2,0},{4,2},{6,4},{1,7},{3,1},{5,3},{7,5},{8,14},{10,8},{12,... | collective-permute-start | bytes 1572872 | tf_op jit(solution)/shard_map/ppermute | solution.py:571
  70.0 2.3 %collective-permute-done.7.refs_1_ = bf16[512,512]{1,0:T(8,128)(2,1)S(1)} collective-permute-done((bf16[512,512]{1,0:T(8,128)(2,1)S(1)}, bf16[512,512]{1,0:T(8,128)(2,1)S(1)}, u32[]{:S(2)}, u32[]{:S(2)}) %collective-permute-start.7) | collective-permute-done | bytes 524320 | tf_op jit(solution)/shard_map/ppermute | solution.py:571
  72.3 0.6 collective-permute-start.12
  72.9 0.0 collective-permute-done.15.refs_0_.refs_10_
  72.9 0.9 collective-permute-start.9
  73.8 0.4 collective-permute-done.19.refs_1_.refs_9_
  74.2 0.2 collective-permute-start.16
  74.5 2.9 %shard_map.166 = (f32[512,128]{1,0:T(8,128)S(1)}, f32[512,128]{1,0:T(8,128)S(1)}, f32[512,128]{1,0:T(8,128)S(1)}) custom-call(bf16[544,256]{1,0:T(8,128)(2,1)} %get-tuple-element.61.refs_0_, bf16[512,128]{1,0:T(8,128)(2,1)S(1)} %get-tuple-element.68.refs_1_.refs_2_.refs_13_), custom_call_target="tpu_custom_call" | custom-call | flops 268435456 | bytes 1048576 | tf_op jit(solution)/shard_map/pallas_call | solution.py:67
  77.4 3.7 %shard_map.167 = (f32[512,128]{1,0:T(8,128)S(1)}, f32[512,128]{1,0:T(8,128)S(1)}, f32[512,128]{1,0:T(8,128)S(1)}) custom-call(bf16[544,256]{1,0:T(8,128)(2,1)S(1)} %collective-permute-done.13.refs_0_.refs_12_, bf16[544,256]{1,0:T(8,128)(2,1)S(1)} %collective-permute-done.17.refs_1_.refs_7_, ...), custom_call_target="tpu_custom_call", output_to_operand_aliasing={{0}: (3, {}), {1}: (4, {}), {2}: (5, {})} | custom-call | flops 536870912 | bytes 1048576 | tf_op jit(solution)/shard_map/pallas_call | solution.py:67
  81.1 3.9 %shard_map.168 = (f32[512,128]{1,0:T(8,128)S(1)}, f32[512,128]{1,0:T(8,128)S(1)}, f32[512,128]{1,0:T(8,128)S(1)}) custom-call(bf16[544,256]{1,0:T(8,128)(2,1)S(1)} %collective-permute-done.14.refs_0_.refs_11_, bf16[544,256]{1,0:T(8,128)(2,1)S(1)} %collective-permute-done.18.refs_1_.refs_8_, ...), custom_call_target="tpu_custom_call", output_to_operand_aliasing={{0}: (3, {}), {1}: (4, {}), {2}: (5, {})} | custom-call | flops 536870912 | bytes 1048576 | tf_op jit(solution)/shard_map/pallas_call | solution.py:67
  85.0 3.7 %shard_map.169 = (f32[512,128]{1,0:T(8,128)S(1)}, f32[512,128]{1,0:T(8,128)S(1)}, f32[512,128]{1,0:T(8,128)S(1)}) custom-call(bf16[544,256]{1,0:T(8,128)(2,1)S(1)} %collective-permute-done.15.refs_0_.refs_10_, bf16[544,256]{1,0:T(8,128)(2,1)S(1)} %collective-permute-done.19.refs_1_.refs_9_, ...), custom_call_target="tpu_custom_call", output_to_operand_aliasing={{0}: (3, {}), {1}: (4, {}), {2}: (5, {})} | custom-call | flops 536870912 | bytes 1048576 | tf_op jit(solution)/shard_map/pallas_call | solution.py:67
  88.7 0.0 collective-permute-done.16.refs_0_
  88.7 2.7 %shard_map.170 = (bf16[128,256]{1,0:T(8,128)(2,1)S(1)}, bf16[128,256]{1,0:T(8,128)(2,1)S(1)}, bf16[128,256]{1,0:T(8,128)(2,1)S(1)}, bf16[128,256]{1,0:T(8,128)(2,1)S(1)}) custom-call(bf16[544,256]{1,0:T(8,128)(2,1)S(1)} %collective-permute-done.16.refs_0_, f32[512,128]{1,0:T(8,128)} %get-tuple-element.64.refs_1_, f32[512,128]{1,0:T(8,128)} %get-tuple-element.65.refs_2_, ...), custom_call_target="tpu_custom_call" | custom-call | flops 536870912 | bytes 1048576 | tf_op jit(solution)/shard_map/pallas_call | solution.py:67
  91.5 0.3 collective-permute-start.20
  91.8 0.0 collective-permute-done.11.refs_6_
  91.8 2.4 %collective-permute-start.21 = (bf16[128,256]{1,0:T(8,128)(2,1)S(1)}, bf16[128,256]{1,0:T(8,128)(2,1)S(1)}, u32[]{:S(2)}, u32[]{:S(2)}) collective-permute-start(bf16[128,256]{1,0:T(8,128)(2,1)S(1)} %get-tuple-element.83), channel_id=1, source_target_pairs={{0,24},{8,0},{16,8},{24,16},{1,25},{9,1},{17,9},{25,17},{2,26},{10... | collective-permute-start | bytes 196616 | tf_op jit(solution)/shard_map/ppermute | solution.py:571
  94.2 0.0 collective-permute-done.8.refs_2_
  94.2 0.0 collective-permute-start.22
  94.2 0.0 collective-permute-done.12.refs_7_
  94.2 0.5 collective-permute-done.9.refs_3_
  94.8 1.4 %collective-permute-done.20.refs_9_ = bf16[128,256]{1,0:T(8,128)(2,1)S(1)} collective-permute-done((bf16[128,256]{1,0:T(8,128)(2,1)S(1)}, bf16[128,256]{1,0:T(8,128)(2,1)S(1)}, u32[]{:S(2)}, u32[]{:S(2)}) %collective-permute-start.20) | collective-permute-done | bytes 65568 | tf_op jit(solution)/shard_map/ppermute | solution.py:571
  96.2 0.0 collective-permute-done.21.refs_10_
  96.2 2.7 %collective-permute-done.22.refs_11_ = bf16[128,256]{1,0:T(8,128)(2,1)S(1)} collective-permute-done((bf16[128,256]{1,0:T(8,128)(2,1)S(1)}, bf16[128,256]{1,0:T(8,128)(2,1)S(1)}, u32[]{:S(2)}, u32[]{:S(2)}) %collective-permute-start.22) | collective-permute-done | bytes 65568 | tf_op jit(solution)/shard_map/ppermute | solution.py:571
  98.8 1.5 %shard_map.171 = (bf16[64,2048]{1,0:T(8,128)(2,1)}, f32[64,2048]{1,0:T(8,128)S(1)}) custom-call(bf16[512,512]{1,0:T(8,128)(2,1)S(1)} %copy-done, bf16[512,512]{1,0:T(8,128)(2,1)S(1)} %collective-permute-done.7.refs_1_, bf16[512,512]{1,0:T(8,128)(2,1)S(1)} %collective-permute-done.8.refs_2_, bf16[512,512]{1,0:T(8,128)(2,1)S(1)} %collective-permute-done.9.refs_3_, ...), custom_call_target="tpu_custom_call" | custom-call | flops 536870912 | bytes 1048576 | tf_op jit(solution)/shard_map/pallas_call | solution.py:67
  100.4 6.4 %collective-permute-start.23 = (bf16[64,2048]{1,0:T(8,128)(2,1)}, bf16[64,2048]{1,0:T(8,128)(2,1)S(1)}, u32[]{:S(2)}, u32[]{:S(2)}) collective-permute-start(bf16[64,2048]{1,0:T(8,128)(2,1)} %get-tuple-element.86), channel_id=1, source_target_pairs={{0,1},{1,0},{2,3},{3,2},{4,5},{5,4},{6,7},{7,6},{8,9},{9,8},{10,11... | collective-permute-start | bytes 786440 | tf_op jit(solution)/shard_map/ppermute | solution.py:571
  106.8 1.4 %collective-permute-done.23 = bf16[64,2048]{1,0:T(8,128)(2,1)S(1)} collective-permute-done((bf16[64,2048]{1,0:T(8,128)(2,1)}, bf16[64,2048]{1,0:T(8,128)(2,1)S(1)}, u32[]{:S(2)}, u32[]{:S(2)}) %collective-permute-start.23) | collective-permute-done | bytes 262176 | tf_op jit(solution)/shard_map/ppermute | solution.py:571
  108.2 0.8 fusion
  (6 shorter events, 0.0 us)
Async XLA Ops:
  2.5 21.8 %copy-start.2 = (bf16[512,256]{1,0:T(8,128)(2,1)S(1)}, bf16[512,256]{1,0:T(8,128)(2,1)}, u32[]{:S(2)}) copy-start(bf16[512,256]{1,0:T(8,128)(2,1)} %get-tuple-element.54.refs_2_) | copy-start | bytes 786436
  2.5 23.0 %copy-start.3 = (bf16[512,256]{1,0:T(8,128)(2,1)S(1)}, bf16[512,256]{1,0:T(8,128)(2,1)}, u32[]{:S(2)}) copy-start(bf16[512,256]{1,0:T(8,128)(2,1)} %get-tuple-element.55.refs_6_) | copy-start | bytes 786436
  2.5 33.6 %copy-start.4 = (f32[32]{0:T(128)S(1)}, f32[32]{0:T(128)}, u32[]{:S(2)}) copy-start(f32[32]{0:T(128)} %param.24) | copy-start | bytes 388
  22.5 18.1 %collective-permute-start = (bf16[4,72,2048]{2,1,0:T(8,128)(2,1)S(1)}, bf16[4,72,2048]{2,1,0:T(8,128)(2,1)S(1)}, u32[]{:S(2)}, u32[]{:S(2)}) collective-permute-start(bf16[4,72,2048]{2,1,0:T(8,128)(2,1)S(1)} %all_to_all.5.refs_0_), channel_id=1, source_target_pairs={{0,1},{1,0},{2,3},{3,2},{4,5},{5,4},{6,7},{7,6},{8,9},{9,8},{10,11... | collective-permute-start | bytes 3538952 | tf_op jit(solution)/shard_map/ppermute | solution.py:571
  24.3 9.1 %collective-permute-start.1 = (bf16[512,256]{1,0:T(8,128)(2,1)S(1)}, bf16[512,256]{1,0:T(8,128)(2,1)S(1)}, u32[]{:S(2)}, u32[]{:S(2)}) collective-permute-start(bf16[512,256]{1,0:T(8,128)(2,1)S(1)} %copy-done.2), channel_id=1, source_target_pairs={{0,2},{2,4},{4,6},{6,0},{1,3},{3,5},{5,7},{7,1},{8,10},{10,12},{12... | collective-permute-start | bytes 786440 | tf_op jit(solution)/shard_map/ppermute | solution.py:571
  25.5 7.9 %collective-permute-start.5 = (bf16[512,256]{1,0:T(8,128)(2,1)S(1)}, bf16[512,256]{1,0:T(8,128)(2,1)S(1)}, u32[]{:S(2)}, u32[]{:S(2)}) collective-permute-start(bf16[512,256]{1,0:T(8,128)(2,1)S(1)} %copy-done.3), channel_id=1, source_target_pairs={{0,6},{2,0},{4,2},{6,4},{1,7},{3,1},{5,3},{7,5},{8,14},{10,8},{12,... | collective-permute-start | bytes 786440 | tf_op jit(solution)/shard_map/ppermute | solution.py:571
  27.0 13.6 %collective-permute-start.2 = (bf16[512,256]{1,0:T(8,128)(2,1)S(1)}, bf16[512,256]{1,0:T(8,128)(2,1)S(1)}, u32[]{:S(2)}, u32[]{:S(2)}) collective-permute-start(bf16[512,256]{1,0:T(8,128)(2,1)S(1)} %copy-done.2), channel_id=1, source_target_pairs={{0,6},{2,0},{4,2},{6,4},{1,7},{3,1},{5,3},{7,5},{8,14},{10,8},{12,... | collective-permute-start | bytes 786440 | tf_op jit(solution)/shard_map/ppermute | solution.py:571
  28.2 12.3 %collective-permute-start.4 = (bf16[512,256]{1,0:T(8,128)(2,1)S(1)}, bf16[512,256]{1,0:T(8,128)(2,1)S(1)}, u32[]{:S(2)}, u32[]{:S(2)}) collective-permute-start(bf16[512,256]{1,0:T(8,128)(2,1)S(1)} %copy-done.3), channel_id=1, source_target_pairs={{0,2},{2,4},{4,6},{6,0},{1,3},{3,5},{5,7},{7,1},{8,10},{10,12},{12... | collective-permute-start | bytes 786440 | tf_op jit(solution)/shard_map/ppermute | solution.py:571
  33.4 11.2 %collective-permute-start.3 = (bf16[512,256]{1,0:T(8,128)(2,1)S(1)}, bf16[512,256]{1,0:T(8,128)(2,1)S(1)}, u32[]{:S(2)}, u32[]{:S(2)}) collective-permute-start(bf16[512,256]{1,0:T(8,128)(2,1)S(1)} %collective-permute-done.1.refs_3_), channel_id=1, source_target_pairs={{0,2},{2,4},{4,6},{6,0},{1,3},{3,5},{5,7},{7,1},{8,10},{10,12},{12... | collective-permute-start | bytes 786440 | tf_op jit(solution)/shard_map/ppermute | solution.py:571
  33.4 11.2 %collective-permute-start.6 = (bf16[512,256]{1,0:T(8,128)(2,1)S(1)}, bf16[512,256]{1,0:T(8,128)(2,1)S(1)}, u32[]{:S(2)}, u32[]{:S(2)}) collective-permute-start(bf16[512,256]{1,0:T(8,128)(2,1)S(1)} %collective-permute-done.5.refs_8_), channel_id=1, source_target_pairs={{0,6},{2,0},{4,2},{6,4},{1,7},{3,1},{5,3},{7,5},{8,14},{10,8},{12,... | collective-permute-start | bytes 786440 | tf_op jit(solution)/shard_map/ppermute | solution.py:571
  40.5 11.2 %copy-start.1 = (bf16[512,512]{1,0:T(8,128)(2,1)S(1)}, bf16[512,512]{1,0:T(8,128)(2,1)}, u32[]{:S(2)}) copy-start(bf16[512,512]{1,0:T(8,128)(2,1)} %refs_4_.2) | copy-start | bytes 1572868
  40.5 18.8 %copy-start = (bf16[512,512]{1,0:T(8,128)(2,1)S(1)}, bf16[512,512]{1,0:T(8,128)(2,1)}, u32[]{:S(2)}) copy-start(bf16[512,512]{1,0:T(8,128)(2,1)} %refs_0_.2) | copy-start | bytes 1572868
  50.2 7.7 %collective-permute-start.13 = (bf16[544,256]{1,0:T(8,128)(2,1)}, bf16[544,256]{1,0:T(8,128)(2,1)S(1)}, u32[]{:S(2)}, u32[]{:S(2)}) collective-permute-start(bf16[544,256]{1,0:T(8,128)(2,1)} %get-tuple-element.61.refs_0_), channel_id=1, source_target_pairs={{0,32},{32,64},{64,96},{96,128},{128,160},{160,192},{192,224},{224... | collective-permute-start | bytes 835592 | tf_op jit(solution)/shard_map/ppermute | solution.py:571
  50.3 9.7 %collective-permute-start.17 = (bf16[544,256]{1,0:T(8,128)(2,1)}, bf16[544,256]{1,0:T(8,128)(2,1)S(1)}, u32[]{:S(2)}, u32[]{:S(2)}) collective-permute-start(bf16[544,256]{1,0:T(8,128)(2,1)} %get-tuple-element.61.refs_0_), channel_id=1, source_target_pairs={{0,224},{32,0},{64,32},{96,64},{128,96},{160,128},{192,160},{224,1... | collective-permute-start | bytes 835592 | tf_op jit(solution)/shard_map/ppermute | solution.py:571
  51.7 16.3 %collective-permute-start.10 = (bf16[512,512]{1,0:T(8,128)(2,1)S(1)}, bf16[512,512]{1,0:T(8,128)(2,1)S(1)}, u32[]{:S(2)}, u32[]{:S(2)}) collective-permute-start(bf16[512,512]{1,0:T(8,128)(2,1)S(1)} %copy-done.1), channel_id=1, source_target_pairs={{0,6},{2,0},{4,2},{6,4},{1,7},{3,1},{5,3},{7,5},{8,14},{10,8},{12,... | collective-permute-start | bytes 1572872 | tf_op jit(solution)/shard_map/ppermute | solution.py:571
  57.8 6.5 %collective-permute-start.14 = (bf16[544,256]{1,0:T(8,128)(2,1)S(1)}, bf16[544,256]{1,0:T(8,128)(2,1)S(1)}, u32[]{:S(2)}, u32[]{:S(2)}) collective-permute-start(bf16[544,256]{1,0:T(8,128)(2,1)S(1)} %collective-permute-done.13.refs_0_.refs_12_), channel_id=1, source_target_pairs={{0,32},{32,64},{64,96},{96,128},{128,160},{160,192},{192,224},{224... | collective-permute-start | bytes 835592 | tf_op jit(solution)/shard_map/ppermute | solution.py:571
  59.3 13.0 %collective-permute-start.7 = (bf16[512,512]{1,0:T(8,128)(2,1)S(1)}, bf16[512,512]{1,0:T(8,128)(2,1)S(1)}, u32[]{:S(2)}, u32[]{:S(2)}) collective-permute-start(bf16[512,512]{1,0:T(8,128)(2,1)S(1)} %copy-done), channel_id=1, source_target_pairs={{0,2},{2,4},{4,6},{6,0},{1,3},{3,5},{5,7},{7,1},{8,10},{10,12},{12... | collective-permute-start | bytes 1572872 | tf_op jit(solution)/shard_map/ppermute | solution.py:571
  60.0 7.4 %collective-permute-start.18 = (bf16[544,256]{1,0:T(8,128)(2,1)S(1)}, bf16[544,256]{1,0:T(8,128)(2,1)S(1)}, u32[]{:S(2)}, u32[]{:S(2)}) collective-permute-start(bf16[544,256]{1,0:T(8,128)(2,1)S(1)} %collective-permute-done.17.refs_1_.refs_7_), channel_id=1, source_target_pairs={{0,224},{32,0},{64,32},{96,64},{128,96},{160,128},{192,160},{224,1... | collective-permute-start | bytes 835592 | tf_op jit(solution)/shard_map/ppermute | solution.py:571
  64.3 8.6 %collective-permute-start.15 = (bf16[544,256]{1,0:T(8,128)(2,1)S(1)}, bf16[544,256]{1,0:T(8,128)(2,1)S(1)}, u32[]{:S(2)}, u32[]{:S(2)}) collective-permute-start(bf16[544,256]{1,0:T(8,128)(2,1)S(1)} %collective-permute-done.14.refs_0_.refs_11_), channel_id=1, source_target_pairs={{0,32},{32,64},{64,96},{96,128},{128,160},{160,192},{192,224},{224... | collective-permute-start | bytes 835592 | tf_op jit(solution)/shard_map/ppermute | solution.py:571
  67.3 6.9 %collective-permute-start.19 = (bf16[544,256]{1,0:T(8,128)(2,1)S(1)}, bf16[544,256]{1,0:T(8,128)(2,1)S(1)}, u32[]{:S(2)}, u32[]{:S(2)}) collective-permute-start(bf16[544,256]{1,0:T(8,128)(2,1)S(1)} %collective-permute-done.18.refs_1_.refs_8_), channel_id=1, source_target_pairs={{0,224},{32,0},{64,32},{96,64},{128,96},{160,128},{192,160},{224,1... | collective-permute-start | bytes 835592 | tf_op jit(solution)/shard_map/ppermute | solution.py:571
  67.3 24.5 %collective-permute-start.11 = (bf16[512,512]{1,0:T(8,128)(2,1)S(1)}, bf16[512,512]{1,0:T(8,128)(2,1)S(1)}, u32[]{:S(2)}, u32[]{:S(2)}) collective-permute-start(bf16[512,512]{1,0:T(8,128)(2,1)S(1)} %copy-done.1), channel_id=1, source_target_pairs={{0,2},{2,4},{4,6},{6,0},{1,3},{3,5},{5,7},{7,1},{8,10},{10,12},{12... | collective-permute-start | bytes 1572872 | tf_op jit(solution)/shard_map/ppermute | solution.py:571
  68.0 26.2 %collective-permute-start.8 = (bf16[512,512]{1,0:T(8,128)(2,1)S(1)}, bf16[512,512]{1,0:T(8,128)(2,1)S(1)}, u32[]{:S(2)}, u32[]{:S(2)}) collective-permute-start(bf16[512,512]{1,0:T(8,128)(2,1)S(1)} %copy-done), channel_id=1, source_target_pairs={{0,6},{2,0},{4,2},{6,4},{1,7},{3,1},{5,3},{7,5},{8,14},{10,8},{12,... | collective-permute-start | bytes 1572872 | tf_op jit(solution)/shard_map/ppermute | solution.py:571
  72.3 21.9 %collective-permute-start.12 = (bf16[512,512]{1,0:T(8,128)(2,1)S(1)}, bf16[512,512]{1,0:T(8,128)(2,1)S(1)}, u32[]{:S(2)}, u32[]{:S(2)}) collective-permute-start(bf16[512,512]{1,0:T(8,128)(2,1)S(1)} %collective-permute-done.10.refs_5_), channel_id=1, source_target_pairs={{0,6},{2,0},{4,2},{6,4},{1,7},{3,1},{5,3},{7,5},{8,14},{10,8},{12,... | collective-permute-start | bytes 1572872 | tf_op jit(solution)/shard_map/ppermute | solution.py:571
  72.9 21.9 %collective-permute-start.9 = (bf16[512,512]{1,0:T(8,128)(2,1)S(1)}, bf16[512,512]{1,0:T(8,128)(2,1)S(1)}, u32[]{:S(2)}, u32[]{:S(2)}) collective-permute-start(bf16[512,512]{1,0:T(8,128)(2,1)S(1)} %collective-permute-done.7.refs_1_), channel_id=1, source_target_pairs={{0,2},{2,4},{4,6},{6,0},{1,3},{3,5},{5,7},{7,1},{8,10},{10,12},{12... | collective-permute-start | bytes 1572872 | tf_op jit(solution)/shard_map/ppermute | solution.py:571
  74.2 14.5 %collective-permute-start.16 = (bf16[544,256]{1,0:T(8,128)(2,1)S(1)}, bf16[544,256]{1,0:T(8,128)(2,1)S(1)}, u32[]{:S(2)}, u32[]{:S(2)}) collective-permute-start(bf16[544,256]{1,0:T(8,128)(2,1)S(1)} %collective-permute-done.15.refs_0_.refs_10_), channel_id=1, source_target_pairs={{0,32},{32,64},{64,96},{96,128},{128,160},{160,192},{192,224},{224... | collective-permute-start | bytes 835592 | tf_op jit(solution)/shard_map/ppermute | solution.py:571
  91.5 4.7 %collective-permute-start.20 = (bf16[128,256]{1,0:T(8,128)(2,1)S(1)}, bf16[128,256]{1,0:T(8,128)(2,1)S(1)}, u32[]{:S(2)}, u32[]{:S(2)}) collective-permute-start(bf16[128,256]{1,0:T(8,128)(2,1)S(1)} %get-tuple-element.82), channel_id=1, source_target_pairs={{0,8},{8,16},{16,24},{24,0},{1,9},{9,17},{17,25},{25,1},{2,10},{10... | collective-permute-start | bytes 196616 | tf_op jit(solution)/shard_map/ppermute | solution.py:571
  91.8 4.4 %collective-permute-start.21 = (bf16[128,256]{1,0:T(8,128)(2,1)S(1)}, bf16[128,256]{1,0:T(8,128)(2,1)S(1)}, u32[]{:S(2)}, u32[]{:S(2)}) collective-permute-start(bf16[128,256]{1,0:T(8,128)(2,1)S(1)} %get-tuple-element.83), channel_id=1, source_target_pairs={{0,24},{8,0},{16,8},{24,16},{1,25},{9,1},{17,9},{25,17},{2,26},{10... | collective-permute-start | bytes 196616 | tf_op jit(solution)/shard_map/ppermute | solution.py:571
  94.2 4.6 %collective-permute-start.22 = (bf16[128,256]{1,0:T(8,128)(2,1)S(1)}, bf16[128,256]{1,0:T(8,128)(2,1)S(1)}, u32[]{:S(2)}, u32[]{:S(2)}) collective-permute-start(bf16[128,256]{1,0:T(8,128)(2,1)S(1)} %get-tuple-element.84), channel_id=1, source_target_pairs={{0,16},{8,24},{16,0},{24,8},{1,17},{9,25},{17,1},{25,9},{2,18},{10... | collective-permute-start | bytes 196616 | tf_op jit(solution)/shard_map/ppermute | solution.py:571
  100.4 7.8 %collective-permute-start.23 = (bf16[64,2048]{1,0:T(8,128)(2,1)}, bf16[64,2048]{1,0:T(8,128)(2,1)S(1)}, u32[]{:S(2)}, u32[]{:S(2)}) collective-permute-start(bf16[64,2048]{1,0:T(8,128)(2,1)} %get-tuple-element.86), channel_id=1, source_target_pairs={{0,1},{1,0},{2,3},{3,2},{4,5},{5,4},{6,7},{7,6},{8,9},{9,8},{10,11... | collective-permute-start | bytes 786440 | tf_op jit(solution)/shard_map/ppermute | solution.py:571
